TPU v7x, 256 devices: a 4x2x16 block of a 4x16x16 slice. The times are simulated.
256 devices in a mesh: grp: 2 (over y), sp: 32 (over z, core), tp: 4 (over x).
Axes of the slice: x: 4, y: 2, z: 16, core: 2. Of those that a mesh axis runs over, the one named last changes fastest.
The devices are a block of a 4x16x16 slice.
Arguments:
- stream_in: bfloat16 [32768, 2048], P(('grp', 'sp')), parts along dimension 0, may hold values from -6 to 6
- query_wide: bfloat16 [32768, 1024], P(('grp', 'sp'), 'tp'), parts along dimension 0, may hold values from -6 to 6
- key_wide: bfloat16 [32768, 1024], P(('grp', 'sp'), 'tp'), parts along dimension 0, may hold values from -6 to 6
- value_wide: bfloat16 [32768, 2048], P(('grp', 'sp'), 'tp'), parts along dimension 0, may hold values from -6 to 6
- query_narrow: bfloat16 [32768, 512], P(('grp', 'sp'), 'tp'), parts along dimension 0, may hold values from -6 to 6
- key_narrow: bfloat16 [32768, 512], P(('grp', 'sp'), 'tp'), parts along dimension 0, may hold values from -6 to 6
- value_narrow: bfloat16 [32768, 1024], P(('grp', 'sp'), 'tp'), parts along dimension 0, may hold values from -6 to 6
- decay_wide: float32 [4, 32768], P('tp', ('grp', 'sp')), parts along dimension 1, may hold values from -1 to 0
- decay_narrow: float32 [4, 32768], P('tp', ('grp', 'sp')), parts along dimension 1, may hold values from -1 to 0
- gain_wide: float32 [2048], P('tp'), may hold values from 0.1 to 1.9
- gain_narrow: float32 [1024], P('tp'), may hold values from 0.1 to 1.9
- out_wide: bfloat16 [2048, 2048], P('tp'), may hold values from -0.109375 to 0.109375
- out_narrow: bfloat16 [1024, 2048], P('tp'), may hold values from -0.109375 to 0.109375
- mlp_gain: float32 [2048], replicated, may hold values from 0.1 to 1.9
- up_weight: bfloat16 [2048, 8192], P('sp', 'tp'), may hold values from -0.125 to 0.125
- down_weight: bfloat16 [8192, 2048], P('tp', 'sp'), may hold values from -0.0625 to 0.0625
Outputs:
- stream_out: bfloat16 [32768, 2048], P(('grp', 'sp', 'tp')), parts along dimension 0
There are 2 independent parts, one for each index of `grp`. A program takes and returns all parts, laid end to end along the dimension named above; an argument that names none is the same for every part. Nothing has to cross between parts.
All inputs are finite; a program needn't handle non-finite values.
Results may differ from a plain program's by a relative error of at most 0.019.
Values may be sent and summed in bfloat16 or wider, within the bound.
No kernel may reach another device: no remote copies, remote signals or barrier semaphores. Data moves between devices by JAX's collectives and lax.ppermute only.
A program may use at most 128 MiB of HBM per device.

v0:
```python
import jax
import jax.numpy as jnp
from jax import lax
from jax.sharding import Mesh
from jax.sharding import PartitionSpec as P

SP = ("sp_0", "sp_1")
GRP_SP = ("grp", "sp_0", "sp_1")
GRP_SP_TP = ("grp", "sp_0", "sp_1", "tp")


EPS = 1e-06


def neutral_like(x, identity):
    return jax.tree.map(
        lambda a, e: jnp.broadcast_to(jnp.asarray(e, a.dtype), a.shape), x, identity
    )


def entering(x, axes, combine, identity):
    before = start = neutral_like(x, identity)
    total = x
    for axis in reversed(axes):
        length, mine = (lax.axis_size(axis), lax.axis_index(axis))
        pieces = jax.tree.map(
            lambda part, kind: lax.all_gather(part.astype(kind), axis),
            total,
            (jnp.bfloat16, jnp.bfloat16, jnp.bfloat16, jnp.bfloat16),
        )
        inside, total = (start, start)
        for k in range(length):
            passed = k < mine
            total = combine(
                total, jax.tree.map(lambda part, own: part[k].astype(own.dtype), pieces, x)
            )
            inside = jax.tree.map(lambda new, old: jnp.where(passed, new, old), total, inside)
        before = combine(inside, before)
    return before


def rows_first(arrays, axis, dims):
    turned = [jnp.moveaxis(a, dim, 0) for a, dim in zip(arrays, dims)]
    both = jnp.concatenate([t.reshape(len(t), -1) for t in turned], axis=1)
    result, at, done = (lax.all_gather(both, axis, axis=0, tiled=True), 0, [])
    for t, dim in zip(turned, dims):
        slab = result[:, at : at + t[0].size].reshape(-1, *t.shape[1:])
        done.append(jnp.moveaxis(slab, 0, dim))
        at += t[0].size
    return tuple(done)


def split_up(x, dim, length):
    before, after = (x.shape[:dim], x.shape[dim + 1 :])
    return jnp.moveaxis(x.reshape(*before, length, -1, *after), dim, 0)


def summed_on_arrival(x, axis, dim):
    parts = split_up(x, dim, lax.axis_size(axis))
    arrived = lax.all_to_all(parts, axis, split_axis=0, concat_axis=0, tiled=True)
    return arrived.astype(jnp.float32).sum(axis=0)


def joined_along(parts, dim):
    parts = jnp.moveaxis(parts, 0, dim)
    lengths = parts.shape
    return parts.reshape(*lengths[:dim], lengths[dim] * lengths[dim + 1], *lengths[dim + 2 :])


def copy_for_each(x, axis):
    length = lax.axis_size(axis)
    return lax.all_to_all(jnp.broadcast_to(x[None], (length, *x.shape)), axis, 0, 0, tiled=True)


def collect(x, axis, dim):
    return joined_along(copy_for_each(x, axis), dim)


def retain_local(queries, key_rows, value_rows, log_decay):
    total_heads = log_decay.shape[0]
    length = queries.shape[0]
    key_width = queries.shape[1] // total_heads
    value_width = value_rows.shape[1] // total_heads
    query_heads = queries.reshape(length, total_heads, key_width)
    key_heads = key_rows.reshape(length, total_heads, key_width)
    value_heads = value_rows.reshape(length, total_heads, value_width)
    cumulative = jnp.cumsum(log_decay, axis=1)
    row_index = lax.broadcasted_iota(jnp.int32, (length, length), 0)
    col_index = lax.broadcasted_iota(jnp.int32, (length, length), 1)
    causal = (row_index >= col_index)[None]
    log_gap = cumulative[:, :, None] - cumulative[:, None, :]
    fading = jnp.where(causal, jnp.exp(jnp.where(causal, log_gap, 0.0)), 0.0)
    scores = jnp.einsum("ihd,jhd->hij", query_heads, key_heads, preferred_element_type=jnp.float32)
    weights_low = (scores * key_width ** (-0.5) * fading).astype(jnp.bfloat16)
    within = jnp.einsum(
        "hij,jhe->ihe", weights_low, value_heads, preferred_element_type=jnp.float32
    )
    to_end = jnp.exp(cumulative[:, -1:] - cumulative)
    keyed = (key_heads.astype(jnp.float32) * key_width ** (-0.5) * to_end.T[:, :, None]).astype(
        jnp.bfloat16
    )
    local_state = jnp.einsum("jhd,jhe->hde", keyed, value_heads, preferred_element_type=jnp.float32)
    overall = jnp.exp(cumulative[:, -1])
    return (query_heads, cumulative, within, overall, local_state)


def finish(query_heads, cumulative, within, incoming, gain_values):
    carried = (
        jnp.einsum(
            "ihd,hde->ihe",
            query_heads.astype(jnp.float32),
            incoming,
            precision=lax.Precision.HIGHEST,
        )
        * jnp.exp(cumulative).T[:, :, None]
    )
    retained = within + carried
    centered = retained - jnp.mean(retained, axis=-1, keepdims=True)
    scaled = centered * lax.rsqrt(jnp.mean(centered * centered, axis=-1, keepdims=True) + EPS)
    return (scaled.reshape(retained.shape[0], -1) * gain_values).astype(jnp.bfloat16)


def normalize(rows, gain_values):
    values = rows.astype(jnp.float32)
    scaled = values * lax.rsqrt(jnp.mean(values * values, axis=-1, keepdims=True) + EPS)
    return (scaled * gain_values).astype(jnp.bfloat16)


def join_states(earlier, latter):
    return (
        earlier[0] * latter[0],
        latter[0][:, None, None] * earlier[1] + latter[1],
        earlier[2] * latter[2],
        latter[2][:, None, None] * earlier[3] + latter[3],
    )


def on_device(
    stream_in,
    query_wide,
    key_wide,
    value_wide,
    query_narrow,
    key_narrow,
    value_narrow,
    decay_wide,
    decay_narrow,
    gain_wide,
    gain_narrow,
    out_wide,
    out_narrow,
    mlp_gain,
    up_weight,
    down_weight,
):
    length = stream_in.shape[0]
    portion = length // lax.axis_size("tp")
    member = lax.axis_index("tp")
    wide_query, wide_cum, wide_within, wide_factor, wide_state = retain_local(
        query_wide, key_wide, value_wide, decay_wide
    )
    thin_query, thin_cum, thin_within, thin_factor, thin_state = retain_local(
        query_narrow, key_narrow, value_narrow, decay_narrow
    )
    identity = (
        jnp.ones_like(wide_factor),
        jnp.zeros_like(wide_state),
        jnp.ones_like(thin_factor),
        jnp.zeros_like(thin_state),
    )
    incoming = entering(
        (wide_factor, wide_state, thin_factor, thin_state), SP, join_states, identity
    )
    normed_wide = finish(wide_query, wide_cum, wide_within, incoming[1], gain_wide)
    normed_thin = finish(thin_query, thin_cum, thin_within, incoming[3], gain_narrow)
    up_full, down_full = rows_first((up_weight, down_weight), SP, (0, 1))
    mixed_heads = summed_on_arrival(
        (
            jnp.dot(normed_wide, out_wide, preferred_element_type=jnp.float32)
            + jnp.dot(normed_thin, out_narrow, preferred_element_type=jnp.float32)
        ).astype(jnp.bfloat16),
        "tp",
        0,
    )
    own_stream = lax.dynamic_slice_in_dim(stream_in, member * portion, portion, 0)
    middle = (own_stream.astype(jnp.float32) + mixed_heads).astype(jnp.bfloat16)
    raised = jax.nn.relu(
        jnp.dot(
            collect(normalize(middle, mlp_gain), "tp", 0),
            up_full,
            preferred_element_type=jnp.float32,
        )
    )
    hidden = (raised * raised).astype(jnp.bfloat16)
    channel = summed_on_arrival(
        jnp.dot(hidden, down_full, preferred_element_type=jnp.float32).astype(jnp.bfloat16), "tp", 0
    )
    return (middle.astype(jnp.float32) + channel).astype(jnp.bfloat16)


def solution(mesh):
    torus = Mesh(
        mesh.devices.reshape(mesh.shape["grp"], 16, 2, mesh.shape["tp"]),
        ("grp", "sp_0", "sp_1", "tp"),
    )
    placed = (
        P(GRP_SP, None),
        P(GRP_SP, "tp"),
        P(GRP_SP, "tp"),
        P(GRP_SP, "tp"),
        P(GRP_SP, "tp"),
        P(GRP_SP, "tp"),
        P(GRP_SP, "tp"),
        P("tp", GRP_SP),
        P("tp", GRP_SP),
        P("tp"),
        P("tp"),
        P("tp", None),
        P("tp", None),
        P(),
        P(SP, "tp"),
        P("tp", SP),
    )
    return jax.shard_map(
        on_device, mesh=torus, in_specs=placed, out_specs=P(GRP_SP_TP, None), check_vma=False
    )
```

profile of v0, /device:TPU:33, one launch (start us, length us, event | category | flops | bytes accessed | tf_op | source)
XLA Modules:
  0.0 342.9 jit_solution(9512883190763255492)
XLA Ops:
  6.5 0.0 copy-start
  6.6 0.1 all-gather.10.cloned.1.call-start
  6.6 1.1 reduce-window.14
  7.8 0.2 slice_reduce_fusion.1
  7.9 0.2 reduce-window.15
  8.1 0.1 broadcast.496
  8.2 0.7 slice.363
  8.9 0.6 slice.362
  10.8 1.0 reduce-window.16
  11.8 0.2 slice_reduce_fusion
  11.9 0.2 reduce-window.19
  12.1 0.1 broadcast.499
  12.2 0.6 slice.383
  12.8 0.6 slice.382
  14.6 0.1 exponential_multiply_fusion
  14.7 1.3 dynamic-slice
  16.0 0.8 dynamic-update-slice
  16.7 0.8 dynamic-update-slice.2
  17.5 1.4 convolution_convert_fusion.1
  18.9 22.0 %all-gather.3 = bf16[256,256]{1,0:T(8,128)(2,1)S(1)} all-gather(bf16[128,256]{1,0:T(8,128)(2,1)S(1)} %convolution_convert_fusion.1), channel_id=5, replica_groups=mesh['grp'=2,'sp_0'=16,'sp_1'=2,'tp'=4] {'sp_1'}, dimensions={0}, use_global_device_ids=true | all-gather | bytes 196608 | tf_op jit(solution)/shard_map/all_gather | solution.py:27
  40.9 2.5 all-reduce.5
  43.4 0.6 slice_convert_fusion.1
  44.6 1.3 fusion.248
  45.8 0.1 all-gather.10.cloned.1.call-update
  45.9 0.1 all-gather.8.cloned.1.call-start
  46.6 0.1 exponential_multiply_fusion.1
  46.7 1.5 convolution_convert_fusion
  48.3 2.2 all-gather.1
  50.5 1.4 fusion.115
  51.9 0.1 all-gather.8.cloned.1.call-update
  52.0 0.1 all-gather.12.cloned.1.call-start
  52.1 0.0 copy-done.4
  52.1 0.0 copy-done.5
  52.1 0.8 pad_maximum_fusion
  52.9 0.1 all-gather.12.cloned.1.call-update
  53.0 1.3 dynamic-slice.1
  54.3 0.7 fusion.317
  54.9 1.3 dynamic-update-slice.1
  56.3 1.3 dynamic-update-slice.3
  57.6 24.1 %all-reduce.4 = (bf16[16]{0:T(256)(128)(2,1)S(1)}, bf16[16]{0:T(256)(128)(2,1)S(1)}) all-reduce(bf16[16]{0:T(256)(128)(2,1)S(1)} %dynamic-update-slice.1, bf16[16]{0:T(256)(128)(2,1)S(1)} %dynamic-update-slice.3), channel_id=2, replica_groups=mesh['grp'=2,'sp_0'=16,'sp_1'=2,'tp'=4] {'sp_0'}, use_global_device_ids=true, to_apply=%add.1 | all-reduce | flops 32 | bytes 128
  82.9 0.7 fusion.315
  93.6 0.7 fusion.316
  105.6 0.0 copy-done.3
  105.6 2.3 fusion.18
  107.9 3.0 convolution_bitcast_fusion.1
  111.0 3.0 fusion.319
  114.0 0.1 multiply_reduce_fusion.1
  114.2 2.8 fusion.116
  117.0 58.9 %all-gather.8.cloned.1.call-done = bf16[16,1,256,512]{3,2,1,0:T(8,128)(2,1)} async-done(((bf16[1,1,256,512]{3,2,1,0:T(8,128)(2,1)}), bf16[16,1,256,512]{3,2,1,0:T(8,128)(2,1)}) %all-gather.8.cloned.1.call-update) | async-done | bytes 4194320 | tf_op jit(solution)/shard_map/all_gather | solution.py:27
  175.9 6.0 %fusion.320 = (f32[512]{0:T(512)S(1)}, f32[1,512,512]{2,1,0:T(8,128)S(1)}) fusion(f32[1,512,512]{2,1,0:T(8,128)} %convolution_bitcast_fusion.1, f32[512]{0:T(512)S(1)} %exp.55, bf16[512,256]{1,0:T(8,128)(2,1)S(1)} %copy-done.9, bf16[16,1,256,512]{3,2,1,0:T(8,128)(2,1)} %all-gather.8.cloned.1.call-done, f32[]{:T(128)} %bitcast.30, f32[]{:T(128)} %bitcast.31, ...), kind=kOutput, calls=%fused_computation.358 | convolution fusion | flops 815529472 | bytes 7082078 | tf_op jit(solution)/shard_map/ihd,hde->ihe/dot_general | solution.py:109
  181.8 0.2 multiply_reduce_fusion
  182.1 2.8 add_convert_fusion
  184.9 4.7 %all-to-all-start = ((bf16[4,128,2048]{2,1,0:T(8,128)(2,1)}), bf16[4,128,2048]{2,1,0:T(8,128)(2,1)}, u32[]{:S(2)}, u32[]{:S(2)}) async-start(bf16[4,128,2048]{2,1,0:T(8,128)(2,1)} %bitcast.179), calls=%async_computation | async-start | bytes 4194304 | tf_op jit(solution)/shard_map/all_to_all | solution.py:60
  189.5 16.5 %all-to-all-done = bf16[4,128,2048]{2,1,0:T(8,128)(2,1)} async-done(((bf16[4,128,2048]{2,1,0:T(8,128)(2,1)}), bf16[4,128,2048]{2,1,0:T(8,128)(2,1)}, u32[]{:S(2)}, u32[]{:S(2)}) %all-to-all-start) | async-done | bytes 2097184 | tf_op jit(solution)/shard_map/all_to_all | solution.py:60
  206.0 2.1 convert_reduce_fusion.1
  208.1 1.4 fusion.21
  209.5 0.2 fusion.23
  209.7 0.2 broadcast_in_dim.16
  209.9 18.6 %all_to_all.15 = bf16[4,128,2048]{2,1,0:T(8,128)(2,1)} all-to-all(bf16[4,128,2048]{2,1,0:T(8,128)(2,1)S(1)} %broadcast_in_dim.16), channel_id=1, replica_groups=mesh['grp'=2,'sp_0'=16,'sp_1'=2,'tp'=4] {'tp'}, dimensions={0} | all-to-all | bytes 4194304 | tf_op jit(solution)/shard_map/all_to_all | solution.py:72
  228.5 60.1 %all-gather.12.cloned.1.call-done = bf16[2048,4096]{1,0:T(8,128)(2,1)} async-done(((bf16[64,4096]{1,0:T(8,128)(2,1)}), bf16[2048,4096]{1,0:T(8,128)(2,1)}) %all-gather.12.cloned.1.call-update) | async-done | bytes 16777232 | tf_op jit(solution)/shard_map/all_gather | solution.py:45
  288.7 16.5 %fusion.6 = bf16[512,2048]{1,0:T(8,128)(2,1)} fusion(bf16[2048,4096]{1,0:T(8,128)(2,1)} %all-gather.12.cloned.1.call-done, bf16[512,2048]{1,0:T(8,128)(2,1)} %bitcast.180), kind=kOutput, calls=%fused_computation.8 | convolution fusion | flops 8594128896 | bytes 20971520 | tf_op jit(solution)/shard_map/dot_general | solution.py:196
  305.2 29.9 %all_to_all.16 = bf16[4,128,2048]{2,1,0:T(8,128)(2,1)S(1)} all-to-all(bf16[4,128,2048]{2,1,0:T(8,128)(2,1)} %bitcast.181), channel_id=1, replica_groups=mesh['grp'=2,'sp_0'=16,'sp_1'=2,'tp'=4] {'tp'}, dimensions={0} | all-to-all | bytes 4194304 | tf_op jit(solution)/shard_map/all_to_all | solution.py:60
  335.0 0.4 convert_reduce_fusion
  335.4 0.9 fusion.24
  (30 shorter events, 0.1 us)
Async XLA Ops:
  6.5 175.5 %copy-start = (bf16[512,2048]{1,0:T(8,128)(2,1)S(1)}, bf16[512,2048]{1,0:T(8,128)(2,1)}, u32[]{:S(2)}) copy-start(bf16[512,2048]{1,0:T(8,128)(2,1)} %param.27) | copy-start | bytes 6291460
  6.6 99.0 %copy-start.3 = (bf16[512,256]{1,0:T(8,128)(2,1)S(1)}, bf16[512,256]{1,0:T(8,128)(2,1)}, u32[]{:S(2)}) copy-start(bf16[512,256]{1,0:T(8,128)(2,1)} %param.22) | copy-start | bytes 786436
  6.6 45.5 %copy-start.4 = (bf16[2048,64]{0,1:T(8,128)(2,1)S(1)}, bf16[2048,64]{0,1:T(8,128)(2,1)}, u32[]{:S(2)}) copy-start(bf16[2048,64]{0,1:T(8,128)(2,1)} %param.31) | copy-start | bytes 786436
  6.6 45.5 %copy-start.5 = (bf16[64,2048]{1,0:T(8,128)(2,1)S(1)}, bf16[64,2048]{1,0:T(8,128)(2,1)}, u32[]{:S(2)}) copy-start(bf16[64,2048]{1,0:T(8,128)(2,1)} %param.30) | copy-start | bytes 786436
  6.6 104.4 %all-gather.10.cloned.1.call-start = ((), (), s32[]{:S(2)}) async-start(), calls=%async_computation.4 | async-start | bytes 1114112 | tf_op jit(solution)/shard_map/all_gather | solution.py:27
  45.9 130.0 %all-gather.8.cloned.1.call-start = ((), (), s32[]{:S(2)}) async-start(), calls=%async_computation.3 | async-start | bytes 4456448 | tf_op jit(solution)/shard_map/all_gather | solution.py:27
  52.0 236.7 %all-gather.12.cloned.1.call-start = ((), (), s32[]{:S(2)}) async-start(), calls=%async_computation.5 | async-start | bytes 17301504 | tf_op jit(solution)/shard_map/all_gather | solution.py:45
  107.9 6.2 %copy-start.7 = (f32[256]{0:T(256)S(1)}, f32[256]{0:T(256)}, u32[]{:S(2)}) copy-start(f32[256]{0:T(256)} %param.26) | copy-start | bytes 3076
  111.0 3.2 copy-start.2
  114.1 61.7 %copy-start.9 = (bf16[512,256]{1,0:T(8,128)(2,1)S(1)}, bf16[512,256]{1,0:T(8,128)(2,1)}, u32[]{:S(2)}) copy-start(bf16[512,256]{1,0:T(8,128)(2,1)} %param.17) | copy-start | bytes 786436
  175.9 6.2 %copy-start.1 = (f32[512,2048]{1,0:T(8,128)S(1)}, f32[512,2048]{1,0:T(8,128)}, u32[]{:S(2)}) copy-start(f32[512,2048]{1,0:T(8,128)} %fusion.116) | copy-start | bytes 12582916
  175.9 6.2 %copy-start.8 = (f32[512]{0:T(512)S(1)}, f32[512]{0:T(512)}, u32[]{:S(2)}) copy-start(f32[512]{0:T(512)} %param.25) | copy-start | bytes 6148
  184.9 24.6 %copy-start.6 = (f32[2048]{0:T(1024)S(1)}, f32[2048]{0:T(1024)}, u32[]{:S(2)}) copy-start(f32[2048]{0:T(1024)} %param.29) | copy-start | bytes 24580
  184.9 21.1 %all-to-all-start = ((bf16[4,128,2048]{2,1,0:T(8,128)(2,1)}), bf16[4,128,2048]{2,1,0:T(8,128)(2,1)}, u32[]{:S(2)}, u32[]{:S(2)}) async-start(bf16[4,128,2048]{2,1,0:T(8,128)(2,1)} %bitcast.179), calls=%async_computation | async-start | bytes 4194304 | tf_op jit(solution)/shard_map/all_to_all | solution.py:60
Sparse Core Ops, SparseCore 0:
  46.0 52.9 all-gather.9
  100.8 74.9 all-gather.7
  177.7 110.9 all-gather.11
where the time goes:
time: 344 us; the launch traced here: 343 us
  waiting for transfers between devices  136 us (40%)
  blocking collectives  99.3 us (29%)
  between operations  39.6 us (12%)
  matrix products  39.3 us (11%)
  other arithmetic  12.7 us (4%)
  local copies, waits for them, and re-layouts  11.4 us (3%)
  starting transfers between devices  4.84 us (1%)
    all_gather x1, waiting for transfers between devices, rows_first(): result, at, done = (lax.all_gather(both, axis, axis=0, tiled=True), 0, [])  60.1 us
    all_gather x2, waiting for transfers between devices, entering(): lax.all_gather(part.astype(kind), axis)  58.9 us
    all_to_all x1, blocking collectives, summed_on_arrival(): lax.all_to_all(parts, axis, split_axis=0, concat_axis=0, tiled=True)  29.9 us
    unnamed x2, blocking collectives  26.6 us
    all_gather x2, blocking collectives, entering(): lax.all_gather(part.astype(kind), axis)  24.2 us
    all_to_all x1, blocking collectives, copy_for_each(): lax.all_to_all(jnp.broadcast_to(x[None], (length, *x.shape)), axis, 0, 0,...  18.6 us
    dot_general x1, matrix products, on_device(): jnp.dot(hidden, down_full, preferred_element_type=jnp.float32)  16.5 us
    all_to_all x1, waiting for transfers between devices, summed_on_arrival(): lax.all_to_all(parts, axis, split_axis=0, concat_axis=0, tiled=True)  16.5 us
  transfers between devices with their start and end apart: 4, of which 3 were waited for; matrix products, arithmetic and copies ran while one was open for 10% of the time, Pallas kernels for 0%

commit v1 on v0

v1 whole, which is shorter than its diff:
```python
import jax
import jax.numpy as jnp
from jax import lax
from jax.experimental import pallas as pl
from jax.experimental.pallas import tpu as pltpu
from jax.sharding import Mesh
from jax.sharding import PartitionSpec as P

EPS = 1e-06
SP = ("za", "zb", "core")
GRP_SP = ("grp", "za", "zb", "core")
GRP_SP_TP = ("grp", "za", "zb", "core", "tp")
F32 = jnp.float32
BF16 = jnp.bfloat16
LANES = 128


def vmem():
    return pl.BlockSpec(memory_space=pltpu.VMEM)


def smem():
    return pl.BlockSpec(memory_space=pltpu.SMEM)


def call(body, outs, *args, scratch=(), flops=0, moved=0):
    specs = [smem() if a.dtype == jnp.int32 else vmem() for a in args]
    many = isinstance(outs, (list, tuple))
    return pl.pallas_call(
        body,
        out_shape=outs,
        in_specs=specs,
        out_specs=[vmem() for _ in outs] if many else vmem(),
        scratch_shapes=list(scratch),
        compiler_params=pltpu.CompilerParams(vmem_limit_bytes=48 * 2**20),
        cost_estimate=pl.CostEstimate(flops=flops, bytes_accessed=moved, transcendentals=0),
        name=body.__name__,
    )(*args)


def shaped(shape, dtype):
    return jax.ShapeDtypeStruct(shape, dtype)


def mm(a, b, dims=((1,), (0,))):
    return lax.dot_general(a, b, (dims, ((), ())), preferred_element_type=F32)


def three(x):
    high = x.astype(BF16).astype(F32)
    mid = (x - high).astype(BF16).astype(F32)
    low = (x - high - mid).astype(BF16).astype(F32)
    return high, mid, low


def pick(index, values):
    out = jnp.zeros_like(index, dtype=F32)
    for n, value in enumerate(values):
        out = jnp.where(index == n, value, out)
    return out


def decay_rows(dw, dn):
    row = lax.broadcasted_iota(jnp.int32, (8, dw.shape[1]), 0)
    return pick(row, three(dw) + three(dn)).astype(BF16)


def columns(table):
    wide = table[:, 0:1] + table[:, 1:2] + table[:, 2:3]
    thin = table[:, 3:4] + table[:, 4:5] + table[:, 5:6]
    return wide, thin


def log_lanes(wide, thin, rows):
    lane = lax.broadcasted_iota(jnp.int32, (rows, LANES), 1)
    return pick(lane, three(wide) + three(thin))


def positions(length):
    row = lax.broadcasted_iota(jnp.int32, (length, length), 0)
    col = lax.broadcasted_iota(jnp.int32, (length, length), 1)
    return row, col


def own_state(kw, vw, dw, kn, vn, dn, out):
    length = kw.shape[0]
    row, col = positions(length)
    later = (col > row).astype(F32).astype(BF16)
    table = decay_rows(dw[...], dn[...])
    end_wide, end_thin = columns(mm(later, table, ((1,), (1,))))
    total_wide = jnp.sum(dw[...], axis=1, keepdims=True)
    total_thin = jnp.sum(dn[...], axis=1, keepdims=True)

    def state(k, v, end):
        keyed = k[...].astype(F32) * k.shape[1] ** (-0.5) * jnp.exp(end)
        return mm(keyed.astype(BF16), v[...], ((0,), (0,))).astype(BF16)

    wide = state(kw, vw, end_wide)
    thin = state(kn, vn, end_thin)
    half_wide, half_thin = wide.shape[0] // 2, thin.shape[0] // 2
    at = wide.shape[1]
    logs = log_lanes(total_wide, total_thin, half_wide).astype(BF16)
    for h in range(2):
        out[h, :, :at] = wide[h * half_wide : (h + 1) * half_wide]
        part = thin[h * half_thin : (h + 1) * half_thin]
        out[h, :half_thin, at : at + LANES] = part[:, :LANES]
        out[h, half_thin:, at : at + LANES] = part[:, LANES:]
        out[h, :, at + LANES :] = logs


def inside(qw, kw, vw, dw, qn, kn, vn, dn, out):
    length = kw.shape[0]
    row, col = positions(length)
    causal = row >= col
    upto = causal.astype(F32).astype(BF16)
    table = decay_rows(dw[...], dn[...])
    col_wide, col_thin = columns(mm(upto, table, ((1,), (1,))))
    rows = mm(table, upto, ((1,), (1,)))
    row_wide = rows[0:1] + rows[1:2] + rows[2:3]
    row_thin = rows[3:4] + rows[4:5] + rows[5:6]

    def within(q, k, v, by_col, by_row):
        gap = jnp.where(causal, by_col - by_row, 0.0)
        fading = jnp.where(causal, jnp.exp(gap), 0.0)
        weights = mm(q[...], k[...], ((1,), (1,))) * k.shape[1] ** (-0.5) * fading
        return mm(weights.astype(BF16), v[...])

    at = vw.shape[1]
    out[:, :at] = within(qw, kw, vw, col_wide, row_wide)
    out[:, at:] = within(qn, kn, vn, col_thin, row_thin)


def unpack(x):
    x = x.astype(F32)
    cut = x.shape[-1] - LANES
    wide, thin = columns(x[:, cut:])
    return x[:, : cut - LANES], x[:, cut - LANES : cut], wide, thin


def after(earlier, latter):
    return (
        jnp.exp(latter[2]) * earlier[0] + latter[0],
        jnp.exp(latter[3]) * earlier[1] + latter[1],
        earlier[2] + latter[2],
        earlier[3] + latter[3],
    )


def put(ref, at, state, logs=True):
    rows, wide, thin = state[0].shape[0], state[0].shape[1], state[1].shape[1]
    ref[at, :, :wide] = state[0].astype(BF16)
    ref[at, :, wide : wide + thin] = state[1].astype(BF16)
    if logs:
        ref[at, :, wide + thin :] = log_lanes(state[2], state[3], rows).astype(BF16)


def of_chip(place, own, sibling, out):
    core, spot = place[0], place[1]
    first_core = core == 0
    pieces, rows = out.shape[0], out.shape[1]
    for d in range(pieces):
        start = pl.multiple_of(lax.rem(spot + d, pieces) * rows, rows)
        mine = own[core, pl.ds(start, rows), :]
        other = sibling[core, pl.ds(start, rows), :]
        first = jnp.where(first_core, mine, other)
        second = jnp.where(first_core, other, mine)
        put(out, d, after(unpack(first), unpack(second)))


def in_order(place, parts, ordered):
    pieces = len(parts)
    for d, part in enumerate(parts):
        ordered[lax.rem(place[1] - d + pieces, pieces)] = part[...]


def of_group(place, a, b, c, d, out, ordered):
    in_order(place, (a, b, c, d), ordered)
    total = unpack(ordered[0])
    for n in range(1, 4):
        total = after(total, unpack(ordered[n]))
    put(out, 0, total)


def before_each(place, a, b, c, d, near, mid, far, out, ordered, found):
    in_order(place, (a, b, c, d), ordered)
    state = after(after(unpack(far[0]), unpack(mid[0])), unpack(near[0]))
    for n in range(4):
        put(found, n, state, logs=False)
        state = after(state, unpack(ordered[n]))
    for n in range(4):
        out[n] = found[lax.rem(place[1] + n, 4)]


def gathered_half(place, a, b, c, d, out):
    parts = (a, b, c, d)
    rows = a.shape[0]
    for n, part in enumerate(parts):
        start = pl.multiple_of(lax.rem(place[1] - n + 4, 4) * rows, rows)
        out[pl.ds(start, rows), :] = part[...]


def heads_out(
    place, own_half, other_half, sibling, qw, qn, dw, dn, within, gw, gn, ow, on, out,
    came_wide, came_thin,
):
    first_core = place[0] == 0
    length = qw.shape[0]
    wide_width, thin_width = gw.shape[1], gn.shape[1]
    half_thin = came_thin.shape[0] // 2
    rows = own_half.shape[0]
    for h in range(2):
        mine = own_half[...] if h == 0 else other_half[...]
        other = other_half[...] if h == 0 else own_half[...]
        before = jnp.where(first_core, mine, other).astype(F32)
        s_wide, s_thin, l_wide, l_thin = unpack(sibling[h])
        b_wide, b_thin = before[:, :wide_width], before[:, wide_width:]
        wide = jnp.where(first_core, b_wide, jnp.exp(l_wide) * b_wide + s_wide)
        thin = jnp.where(first_core, b_thin, jnp.exp(l_thin) * b_thin + s_thin)
        came_wide[h * rows : (h + 1) * rows, :] = wide.astype(BF16)
        low = thin.astype(BF16)
        came_thin[h * half_thin : (h + 1) * half_thin, :LANES] = low[:half_thin]
        came_thin[h * half_thin : (h + 1) * half_thin, LANES:] = low[half_thin:]
    row, col = positions(length)
    upto = (row >= col).astype(F32).astype(BF16)
    cum_wide, cum_thin = columns(mm(upto, decay_rows(dw[...], dn[...]), ((1,), (1,))))

    def normed(q, came, cum, inner, gain):
        kept = inner + mm(q[...], came[...]) * jnp.exp(cum)
        centered = kept - jnp.mean(kept, axis=-1, keepdims=True)
        power = jnp.mean(centered * centered, axis=-1, keepdims=True)
        return (centered * lax.rsqrt(power + EPS) * gain[...]).astype(BF16)

    wide = normed(qw, came_wide, cum_wide, within[:, :wide_width], gw)
    thin = normed(qn, came_thin, cum_thin, within[:, wide_width:], gn)
    step = 512
    for n in range(ow.shape[1] // step):
        cols = slice(n * step, (n + 1) * step)
        out[:, cols] = (mm(wide, ow[:, cols]) + mm(thin, on[:, cols])).astype(BF16)


def rows_mid(parts, stream, gain, middle, normed):
    total = parts[0].astype(F32)
    for n in range(1, parts.shape[0]):
        total = total + parts[n].astype(F32)
    mid = (stream[...].astype(F32) + total).astype(BF16)
    middle[...] = mid
    values = mid.astype(F32)
    power = jnp.mean(values * values, axis=-1, keepdims=True)
    normed[...] = (values * lax.rsqrt(power + EPS) * gain[...]).astype(BF16)


def shift(x, axis, by, size, wrap=True):
    pairs = [(i, (i + by) % size) for i in range(size) if wrap or 0 <= i + by < size]
    return lax.ppermute(x, axis, pairs)


def swap(x):
    return lax.ppermute(x, "core", [(0, 1), (1, 0)])


def among(parts):
    return [parts[0]] + [shift(parts[d], "zb", d, 4) for d in range(1, 4)]


def on_device(
    stream_in, query_wide, key_wide, value_wide, query_narrow, key_narrow, value_narrow,
    decay_wide, decay_narrow, gain_wide, gain_narrow, out_wide, out_narrow, mlp_gain,
    up_weight, down_weight,
):
    members = lax.axis_size("tp")
    length, width = stream_in.shape
    portion = length // members
    member = lax.axis_index("tp")
    place = jnp.stack([lax.axis_index("core"), lax.axis_index("zb")]).astype(jnp.int32)

    both = jnp.concatenate([up_weight, down_weight.T], axis=1)
    weights = lax.all_gather(both, SP, axis=0, tiled=True)

    wide_key, wide_value = key_wide.shape[1], value_wide.shape[1]
    thin_value = value_narrow.shape[1]
    half = wide_key // 2
    lanes = wide_value + 2 * LANES
    own = call(
        own_state, shaped((2, half, lanes), BF16),
        key_wide, value_wide, decay_wide, key_narrow, value_narrow, decay_narrow,
        flops=2 * length * wide_key * wide_value, moved=10**6,
    )
    sibling = swap(own)
    within = call(
        inside, shaped((length, wide_value + thin_value), F32),
        query_wide, key_wide, value_wide, decay_wide,
        query_narrow, key_narrow, value_narrow, decay_narrow,
        flops=6 * length * length * wide_value, moved=4 * 10**6,
    )
    rows = half // 4
    pieces = call(of_chip, shaped((4, rows, lanes), BF16), place, own, sibling)
    got = among([pieces[d] for d in range(4)])
    total = call(
        of_group, shaped((1, rows, lanes), BF16), place, *got,
        scratch=[pltpu.VMEM((4, rows, lanes), BF16)],
    )
    size = lax.axis_size("za")
    near, mid, far = [shift(total, "za", d, size, wrap=False) for d in range(1, 4)]
    found = call(
        before_each, shaped((4, rows, lanes - LANES), BF16), place, *got, near, mid, far,
        scratch=[pltpu.VMEM((4, rows, lanes), BF16), pltpu.VMEM((4, rows, lanes - LANES), BF16)],
    )
    back = among([found[d] for d in range(4)])
    own_half = call(gathered_half, shaped((half, lanes - LANES), BF16), place, *back)
    other_half = swap(own_half)
    partial = call(
        heads_out, shaped((length, width), BF16),
        place, own_half, other_half, sibling, query_wide, query_narrow,
        decay_wide, decay_narrow, within, gain_wide[None], gain_narrow[None],
        out_wide, out_narrow,
        scratch=[
            pltpu.VMEM((wide_key, wide_value), BF16),
            pltpu.VMEM((key_narrow.shape[1], thin_value), BF16),
        ],
        flops=4 * length * wide_value * width, moved=8 * 10**6,
    )
    parts = lax.all_to_all(partial.reshape(members, portion, width), "tp", 0, 0, tiled=True)
    own_stream = lax.dynamic_slice_in_dim(stream_in, member * portion, portion, 0)
    middle, normed = call(
        rows_mid, [shaped((portion, width), BF16)] * 2, parts, own_stream, mlp_gain[None]
    )
    copies = jnp.broadcast_to(normed[None], (members, portion, width))
    everyone = lax.all_to_all(copies, "tp", 0, 0, tiled=True).reshape(length, width)
    units = up_weight.shape[1]
    raised = jax.nn.relu(jnp.dot(everyone, weights[:, :units], preferred_element_type=F32))
    hidden = (raised * raised).astype(BF16)
    channel = lax.dot_general(
        hidden, weights[:, units:], (((1,), (1,)), ((), ())), preferred_element_type=F32
    ).astype(BF16)
    summed = lax.all_to_all(channel.reshape(members, portion, width), "tp", 0, 0, tiled=True)
    return (middle.astype(F32) + summed.astype(F32).sum(axis=0)).astype(BF16)


def solution(mesh):
    grp, sp, tp = mesh.shape["grp"], mesh.shape["sp"], mesh.shape["tp"]
    torus = Mesh(
        mesh.devices.reshape(grp, sp // 8, 4, 2, tp), ("grp", "za", "zb", "core", "tp")
    )
    placed = (
        P(GRP_SP, None),
        P(GRP_SP, "tp"),
        P(GRP_SP, "tp"),
        P(GRP_SP, "tp"),
        P(GRP_SP, "tp"),
        P(GRP_SP, "tp"),
        P(GRP_SP, "tp"),
        P("tp", GRP_SP),
        P("tp", GRP_SP),
        P("tp"),
        P("tp"),
        P("tp", None),
        P("tp", None),
        P(),
        P(SP, "tp"),
        P("tp", SP),
    )
    return jax.shard_map(
        on_device, mesh=torus, in_specs=placed, out_specs=P(GRP_SP_TP, None), check_vma=False
    )
```

time: 344 us -> 206 us (0.60)
  waiting for transfers between devices: 136 us -> 45.4 us
  starting transfers between devices: 4.84 us -> 48.5 us
  blocking collectives: 99.3 us -> 56.9 us
  between operations: 39.6 us -> 13.7 us
  matrix products: 39.3 us -> 16.5 us
  Pallas kernels: 0 us -> 13.1 us
  other arithmetic: 12.7 us -> 3.36 us
  local copies, waits for them, and re-layouts: 11.4 us -> 6.89 us
    all_gather x3 -> x1, waiting for transfers between devices: 119 us -> 0.01 us  [on_device(): weights = lax.all_gather(both, SP, axis=0, tiled=True)]
    ppermute x0 -> x11, starting transfers between devices: none -> 43.7 us  [the longest x2 22.1 us: swap(): return lax.ppermute(x, 'core', [(0, 1), (1, 0)])]
    unnamed x2 -> x0, blocking collectives: 26.6 us -> none
    all_gather x2 -> x0, blocking collectives: 24.2 us -> none  [entering(): lax.all_gather(part.astype(kind), axis)]
    dot_general x9 -> x1, matrix products: 39.3 us -> 16.5 us  [on_device(): lax.dot_general(hidden, weights[:, units:], (((1,), (1,)), ((), ())), pre...]
    ppermute x0 -> x11, waiting for transfers between devices: none -> 18.8 us  [the longest x9 17.4 us: shift(): return lax.ppermute(x, axis, pairs)]
    pallas_call x0 -> x8, Pallas kernels: none -> 13.1 us  [call(): pl.pallas_call(body, out_shape=outs, in_specs=specs, out_specs=[vmem() fo...]
    all_to_all x1, waiting for transfers between devices: 16.5 us -> 26.6 us  [on_device(): lax.all_to_all(partial.reshape(members, portion, width), 'tp', 0, 0, tile...]
  transfers between devices with their start and end apart: 4 -> 13, of which waited for: 3 -> 9; matrix products, arithmetic and copies ran while one was open for 10% -> 0% of each run, Pallas kernels for 0% -> 6%
where the time goes in v1:
time: 206 us; the launch traced here: 204 us
  blocking collectives  56.9 us (28%)
  starting transfers between devices  48.5 us (24%)
  waiting for transfers between devices  45.4 us (22%)
  matrix products  16.5 us (8%)
  between operations  13.7 us (7%)
  Pallas kernels  13.1 us (6%)
  local copies, waits for them, and re-layouts  6.89 us (3%)
  other arithmetic  3.36 us (2%)
    all_to_all x1, blocking collectives, on_device(): lax.all_to_all(copies, 'tp', 0, 0, tiled=True).reshape(length, width)  28.7 us
    all_to_all x1, blocking collectives, on_device(): lax.all_to_all(channel.reshape(members, portion, width), 'tp', 0, 0, tile...  28.2 us
    all_to_all x1, waiting for transfers between devices, on_device(): lax.all_to_all(partial.reshape(members, portion, width), 'tp', 0, 0, tile...  26.6 us
    ppermute x2, starting transfers between devices, swap(): return lax.ppermute(x, 'core', [(0, 1), (1, 0)])  22.1 us
    ppermute x9, starting transfers between devices, shift(): return lax.ppermute(x, axis, pairs)  21.6 us
    ppermute x9, waiting for transfers between devices, shift(): return lax.ppermute(x, axis, pairs)  17.4 us
    dot_general x1, matrix products, on_device(): lax.dot_general(hidden, weights[:, units:], (((1,), (1,)), ((), ())), pre...  16.5 us
    pallas_call x8, Pallas kernels, call(): pl.pallas_call(body, out_shape=outs, in_specs=specs, out_specs=[vmem() fo...  13.1 us
  transfers between devices with their start and end apart: 13, of which 9 were waited for; matrix products, arithmetic and copies ran while one was open for 0% of the time, Pallas kernels for 6%

profile of v1, /device:TPU:33, one launch (start us, length us, event | category | flops | bytes accessed | tf_op | source)
XLA Modules:
  0.0 204.5 jit_solution(6069255689407886354)
XLA Ops:
  6.5 0.0 copy-start
  6.6 0.0 all-gather.2.cloned.1.call-start
  6.6 2.0 pad_maximum_fusion
  8.6 0.1 all-gather.2.cloned.1.call-update
  8.6 0.0 copy-start.2
  8.6 1.0 copy-done.2
  9.7 0.9 copy-done.4
  10.6 0.9 copy-done.6
  11.6 0.9 copy-done.8
  12.5 0.7 copy-done.13
  13.2 0.7 copy-done.15
  13.8 0.0 copy-start.16
  13.9 1.0 own_state.1.own
  14.8 20.5 %collective-permute-start = (bf16[2,128,768]{2,1,0:T(8,128)(2,1)S(1)}, bf16[2,128,768]{2,1,0:T(8,128)(2,1)}, u32[]{:S(2)}, u32[]{:S(2)}) collective-permute-start(bf16[2,128,768]{2,1,0:T(8,128)(2,1)S(1)} %own_state.1.own), channel_id=1, source_target_pairs={{0,4},{4,0},{1,5},{5,1},{2,6},{6,2},{3,7},{7,3},{8,12},{12,8},{9,1... | collective-permute-start | bytes 1179656 | tf_op jit(solution)/shard_map/ppermute | solution.py:258
  35.4 0.1 pad_add_fusion.place
  35.4 1.4 collective-permute-done.sibling
  36.8 1.4 of_chip.1
  38.3 0.1 collective-permute-start.1
  38.4 0.1 collective-permute-start.2
  38.5 3.1 %collective-permute-start.3 = (bf16[32,768]{1,0:T(8,128)(2,1)S(1)}, bf16[32,768]{1,0:T(8,128)(2,1)S(1)}, u32[]{:S(2)}, u32[]{:S(2)}) collective-permute-start(bf16[32,768]{1,0:T(8,128)(2,1)S(1)} %get-tuple-element.9), channel_id=1, source_target_pairs={{0,24},{8,0},{16,8},{24,16},{1,25},{9,1},{17,9},{25,17},{2,26},{10... | collective-permute-start | bytes 147464 | tf_op jit(solution)/shard_map/ppermute | solution.py:254
  41.6 2.9 %collective-permute-done.1.b = bf16[32,768]{1,0:T(8,128)(2,1)S(1)} collective-permute-done((bf16[32,768]{1,0:T(8,128)(2,1)S(1)}, bf16[32,768]{1,0:T(8,128)(2,1)S(1)}, u32[]{:S(2)}, u32[]{:S(2)}) %collective-permute-start.1) | collective-permute-done | bytes 49184 | tf_op jit(solution)/shard_map/ppermute | solution.py:254
  44.5 0.3 collective-permute-done.2.c
  44.8 2.2 %collective-permute-done.3.d = bf16[32,768]{1,0:T(8,128)(2,1)S(1)} collective-permute-done((bf16[32,768]{1,0:T(8,128)(2,1)S(1)}, bf16[32,768]{1,0:T(8,128)(2,1)S(1)}, u32[]{:S(2)}, u32[]{:S(2)}) %collective-permute-start.3) | collective-permute-done | bytes 49184 | tf_op jit(solution)/shard_map/ppermute | solution.py:254
  47.0 0.8 of_group.1
  47.8 0.0 copy-start.17
  47.8 0.0 copy-start.18
  47.8 0.0 copy-start.19
  47.8 1.4 collective-permute-start.4
  49.3 11.0 %collective-permute-start.5 = (bf16[1,32,768]{2,1,0:T(8,128)(2,1)S(1)}, bf16[1,32,768]{2,1,0:T(8,128)(2,1)S(1)}, u32[]{:S(2)}, u32[]{:S(2)}) collective-permute-start(bf16[1,32,768]{2,1,0:T(8,128)(2,1)S(1)} %of_group.1), channel_id=1, source_target_pairs={{0,64},{32,96},{1,65},{33,97},{2,66},{34,98},{3,67},{35,99},{4,68}... | collective-permute-start | bytes 147464 | tf_op jit(solution)/shard_map/ppermute | solution.py:254
  60.3 1.3 collective-permute-start.6
  61.6 0.0 collective-permute-done.4.near
  61.6 0.9 collective-permute-done.5.mid
  62.4 6.9 %collective-permute-done.6.far = bf16[1,32,768]{2,1,0:T(8,128)(2,1)S(1)} collective-permute-done((bf16[1,32,768]{2,1,0:T(8,128)(2,1)S(1)}, bf16[1,32,768]{2,1,0:T(8,128)(2,1)S(1)}, u32[]{:S(2)}, u32[]{:S(2)}) %collective-permute-start.6) | collective-permute-done | bytes 49184 | tf_op jit(solution)/shard_map/ppermute | solution.py:254
  69.4 0.8 before_each.1
  70.2 2.3 %collective-permute-start.7 = (bf16[32,640]{1,0:T(8,128)(2,1)S(1)}, bf16[32,640]{1,0:T(8,128)(2,1)S(1)}, u32[]{:S(2)}, u32[]{:S(2)}) collective-permute-start(bf16[32,640]{1,0:T(8,128)(2,1)S(1)} %get-tuple-element.15), channel_id=1, source_target_pairs={{0,8},{8,16},{16,24},{24,0},{1,9},{9,17},{17,25},{25,1},{2,10},{10... | collective-permute-start | bytes 122888 | tf_op jit(solution)/shard_map/ppermute | solution.py:254
  72.5 0.0 collective-permute-start.8
  72.5 2.2 %collective-permute-start.9 = (bf16[32,640]{1,0:T(8,128)(2,1)S(1)}, bf16[32,640]{1,0:T(8,128)(2,1)S(1)}, u32[]{:S(2)}, u32[]{:S(2)}) collective-permute-start(bf16[32,640]{1,0:T(8,128)(2,1)S(1)} %get-tuple-element.13), channel_id=1, source_target_pairs={{0,24},{8,0},{16,8},{24,16},{1,25},{9,1},{17,9},{25,17},{2,26},{10... | collective-permute-start | bytes 122888 | tf_op jit(solution)/shard_map/ppermute | solution.py:254
  74.7 1.3 collective-permute-done.7.b
  75.9 2.9 %collective-permute-done.8.c = bf16[32,640]{1,0:T(8,128)(2,1)S(1)} collective-permute-done((bf16[32,640]{1,0:T(8,128)(2,1)S(1)}, bf16[32,640]{1,0:T(8,128)(2,1)S(1)}, u32[]{:S(2)}, u32[]{:S(2)}) %collective-permute-start.8) | collective-permute-done | bytes 40992 | tf_op jit(solution)/shard_map/ppermute | solution.py:254
  78.9 0.0 collective-permute-done.9.d
  78.9 0.6 gathered_half.1.own_half
  79.4 1.6 collective-permute-start.10
  81.0 0.0 copy-done.3
  81.0 0.0 copy-done.14
  81.0 0.0 copy-done.16
  81.0 0.0 copy-done.9
  81.0 0.0 copy-done.10
  81.0 0.0 copy-done.11
  81.0 1.2 inside.1.within
  82.2 0.0 collective-permute-done.10.other_half
  82.2 0.0 copy-done.17
  82.3 0.0 copy-done.18
  82.3 0.0 copy-done.19
  82.3 5.3 %heads_out.1 = bf16[512,2048]{1,0:T(8,128)(2,1)S(1)} custom-call(s32[2]{0:T(128)S(1)} %pad_add_fusion.place, bf16[128,640]{1,0:T(8,128)(2,1)S(1)} %gathered_half.1.own_half, bf16[128,640]{1,0:T(8,128)(2,1)S(1)} %collective-permute-done.10.other_half, bf16[2,128,768]{2,1,0:T(8,128)(2,1)} %collective-permute-done.sibling, bf16[512,256]{1,0:T(8,128)(2,1)S(1)} %copy-done.10, ...), custom_call_target="tpu_custom_call" | custom-call | flops 2147483648 | bytes 8000000 | tf_op jit(solution)/shard_map/heads_out/pallas_call | solution.py:29
  87.6 1.3 copy-done.1
  88.9 4.8 %all-to-all-start = ((bf16[4,128,2048]{2,1,0:T(8,128)(2,1)}), bf16[4,128,2048]{2,1,0:T(8,128)(2,1)}, u32[]{:S(2)}, u32[]{:S(2)}) async-start(bf16[4,128,2048]{2,1,0:T(8,128)(2,1)} %bitcast.26), calls=%async_computation | async-start | bytes 4194304 | tf_op jit(solution)/shard_map/all_to_all | solution.py:322
  93.8 26.6 %all-to-all-done.parts = bf16[4,128,2048]{2,1,0:T(8,128)(2,1)} async-done(((bf16[4,128,2048]{2,1,0:T(8,128)(2,1)}), bf16[4,128,2048]{2,1,0:T(8,128)(2,1)}, u32[]{:S(2)}, u32[]{:S(2)}) %all-to-all-start) | async-done | bytes 2097184 | tf_op jit(solution)/shard_map/all_to_all | solution.py:322
  120.5 2.2 %rows_mid.1 = (bf16[128,2048]{1,0:T(8,128)(2,1)S(1)}, bf16[128,2048]{1,0:T(8,128)(2,1)S(1)}) custom-call(bf16[4,128,2048]{2,1,0:T(8,128)(2,1)} %all-to-all-done.parts, bf16[128,2048]{1,0:T(8,128)(2,1)S(1)} %constant_dynamic-slice_fusion.stream, f32[1,2048]{1,0:T(1,128)S(1)} %bitcast.27), custom_call_target="tpu_custom_call" | custom-call | tf_op jit(solution)/shard_map/rows_mid/pallas_call | solution.py:29
  122.6 0.2 broadcast_in_dim.18
  122.9 28.7 %all_to_all.15 = bf16[4,128,2048]{2,1,0:T(8,128)(2,1)} all-to-all(bf16[4,128,2048]{2,1,0:T(8,128)(2,1)S(1)} %broadcast_in_dim.18), channel_id=1, replica_groups=mesh['grp'=2,'za'=4,'zb'=4,'core'=2,'tp'=4] {'tp'}, dimensions={0} | all-to-all | bytes 4194304 | tf_op jit(solution)/shard_map/all_to_all | solution.py:328
  151.6 16.5 %fusion.6 = bf16[512,2048]{1,0:T(8,128)(2,1)} fusion(bf16[2048,4096]{1,0:T(8,128)(2,1)} %all-gather.2.cloned.1.call-done, bf16[512,2048]{1,0:T(8,128)(2,1)} %bitcast.30), kind=kOutput, calls=%fused_computation.6 | convolution fusion | flops 8594128896 | bytes 20971520 | tf_op jit(solution)/shard_map/dot_general | solution.py:332
  168.1 28.2 %all_to_all.16 = bf16[4,128,2048]{2,1,0:T(8,128)(2,1)S(1)} all-to-all(bf16[4,128,2048]{2,1,0:T(8,128)(2,1)} %bitcast.31), channel_id=1, replica_groups=mesh['grp'=2,'za'=4,'zb'=4,'core'=2,'tp'=4] {'tp'}, dimensions={0} | all-to-all | bytes 4194304 | tf_op jit(solution)/shard_map/all_to_all | solution.py:335
  196.3 0.4 convert_reduce_fusion
  196.7 0.9 add_convert_fusion
  (22 shorter events, 0.1 us)
Async XLA Ops:
  6.5 87.2 %copy-start = (bf16[512,2048]{1,0:T(8,128)(2,1)S(1)}, bf16[512,2048]{1,0:T(8,128)(2,1)}, u32[]{:S(2)}) copy-start(bf16[512,2048]{1,0:T(8,128)(2,1)} %param.16) | copy-start | bytes 6291460
  6.6 145.1 %all-gather.2.cloned.1.call-start = ((), (), s32[]{:S(2)}) async-start(), calls=%async_computation.3 | async-start | bytes 17301504 | tf_op jit(solution)/shard_map/all_gather | solution.py:277
  8.6 1.0 copy-start.2
  9.7 0.9 copy-start.4
  10.6 0.9 copy-start.6
  11.6 0.9 copy-start.8
  12.5 0.7 copy-start.13
  13.2 0.7 copy-start.15
  13.8 67.1 %copy-start.3 = (bf16[512,512]{1,0:T(8,128)(2,1)S(1)}, bf16[512,512]{1,0:T(8,128)(2,1)}, u32[]{:S(2)}) copy-start(bf16[512,512]{1,0:T(8,128)(2,1)} %vw.3) | copy-start | bytes 1572868
  13.8 67.1 %copy-start.5 = (bf16[512,256]{1,0:T(8,128)(2,1)S(1)}, bf16[512,256]{1,0:T(8,128)(2,1)}, u32[]{:S(2)}) copy-start(bf16[512,256]{1,0:T(8,128)(2,1)} %kw.3) | copy-start | bytes 786436
  13.8 67.1 %copy-start.7 = (bf16[512,256]{1,0:T(8,128)(2,1)S(1)}, bf16[512,256]{1,0:T(8,128)(2,1)}, u32[]{:S(2)}) copy-start(bf16[512,256]{1,0:T(8,128)(2,1)} %vn.3) | copy-start | bytes 786436
  13.8 67.1 %copy-start.14 = (f32[1,512]{1,0:T(1,128)S(1)}, f32[1,512]{1,0:T(1,128)}, u32[]{:S(2)}) copy-start(f32[1,512]{1,0:T(1,128)} %dw.5) | copy-start | bytes 6148
  13.8 67.2 %copy-start.16 = (f32[1,512]{1,0:T(1,128)S(1)}, f32[1,512]{1,0:T(1,128)}, u32[]{:S(2)}) copy-start(f32[1,512]{1,0:T(1,128)} %dn.5) | copy-start | bytes 6148
  14.8 22.0 %collective-permute-start = (bf16[2,128,768]{2,1,0:T(8,128)(2,1)S(1)}, bf16[2,128,768]{2,1,0:T(8,128)(2,1)}, u32[]{:S(2)}, u32[]{:S(2)}) collective-permute-start(bf16[2,128,768]{2,1,0:T(8,128)(2,1)S(1)} %own_state.1.own), channel_id=1, source_target_pairs={{0,4},{4,0},{1,5},{5,1},{2,6},{6,2},{3,7},{7,3},{8,12},{12,8},{9,1... | collective-permute-start | bytes 1179656 | tf_op jit(solution)/shard_map/ppermute | solution.py:258
  35.4 45.6 %copy-start.9 = (bf16[512,128]{1,0:T(8,128)(2,1)S(1)}, bf16[512,128]{1,0:T(8,128)(2,1)}, u32[]{:S(2)}) copy-start(bf16[512,128]{1,0:T(8,128)(2,1)} %kn.3) | copy-start | bytes 393220
  35.4 45.7 %copy-start.10 = (bf16[512,256]{1,0:T(8,128)(2,1)S(1)}, bf16[512,256]{1,0:T(8,128)(2,1)}, u32[]{:S(2)}) copy-start(bf16[512,256]{1,0:T(8,128)(2,1)} %qw.3) | copy-start | bytes 786436
  35.4 45.7 %copy-start.11 = (bf16[512,128]{1,0:T(8,128)(2,1)S(1)}, bf16[512,128]{1,0:T(8,128)(2,1)}, u32[]{:S(2)}) copy-start(bf16[512,128]{1,0:T(8,128)(2,1)} %qn.3) | copy-start | bytes 393220
  38.3 6.3 %collective-permute-start.1 = (bf16[32,768]{1,0:T(8,128)(2,1)S(1)}, bf16[32,768]{1,0:T(8,128)(2,1)S(1)}, u32[]{:S(2)}, u32[]{:S(2)}) collective-permute-start(bf16[32,768]{1,0:T(8,128)(2,1)S(1)} %get-tuple-element.11), channel_id=1, source_target_pairs={{0,8},{8,16},{16,24},{24,0},{1,9},{9,17},{17,25},{25,1},{2,10},{10... | collective-permute-start | bytes 147464 | tf_op jit(solution)/shard_map/ppermute | solution.py:254
  38.4 6.4 %collective-permute-start.2 = (bf16[32,768]{1,0:T(8,128)(2,1)S(1)}, bf16[32,768]{1,0:T(8,128)(2,1)S(1)}, u32[]{:S(2)}, u32[]{:S(2)}) collective-permute-start(bf16[32,768]{1,0:T(8,128)(2,1)S(1)} %get-tuple-element.10), channel_id=1, source_target_pairs={{0,16},{8,24},{16,0},{24,8},{1,17},{9,25},{17,1},{25,9},{2,18},{10... | collective-permute-start | bytes 147464 | tf_op jit(solution)/shard_map/ppermute | solution.py:254
  38.5 8.5 %collective-permute-start.3 = (bf16[32,768]{1,0:T(8,128)(2,1)S(1)}, bf16[32,768]{1,0:T(8,128)(2,1)S(1)}, u32[]{:S(2)}, u32[]{:S(2)}) collective-permute-start(bf16[32,768]{1,0:T(8,128)(2,1)S(1)} %get-tuple-element.9), channel_id=1, source_target_pairs={{0,24},{8,0},{16,8},{24,16},{1,25},{9,1},{17,9},{25,17},{2,26},{10... | collective-permute-start | bytes 147464 | tf_op jit(solution)/shard_map/ppermute | solution.py:254
  47.8 34.4 %copy-start.17 = (bf16[256,2048]{1,0:T(8,128)(2,1)S(1)}, bf16[256,2048]{1,0:T(8,128)(2,1)}, u32[]{:S(2)}) copy-start(bf16[256,2048]{1,0:T(8,128)(2,1)} %on.1) | copy-start | bytes 3145732
  47.8 34.4 %copy-start.18 = (f32[512]{0:T(512)S(1)}, f32[512]{0:T(512)}, u32[]{:S(2)}) copy-start(f32[512]{0:T(512)} %param.25) | copy-start | bytes 6148
  47.8 34.4 %copy-start.19 = (f32[256]{0:T(256)S(1)}, f32[256]{0:T(256)}, u32[]{:S(2)}) copy-start(f32[256]{0:T(256)} %param.26) | copy-start | bytes 3076
  47.8 13.7 %collective-permute-start.4 = (bf16[1,32,768]{2,1,0:T(8,128)(2,1)S(1)}, bf16[1,32,768]{2,1,0:T(8,128)(2,1)S(1)}, u32[]{:S(2)}, u32[]{:S(2)}) collective-permute-start(bf16[1,32,768]{2,1,0:T(8,128)(2,1)S(1)} %of_group.1), channel_id=1, source_target_pairs={{0,32},{32,64},{64,96},{1,33},{33,65},{65,97},{2,34},{34,66},{66,9... | collective-permute-start | bytes 147464 | tf_op jit(solution)/shard_map/ppermute | solution.py:254
  49.3 13.2 %collective-permute-start.5 = (bf16[1,32,768]{2,1,0:T(8,128)(2,1)S(1)}, bf16[1,32,768]{2,1,0:T(8,128)(2,1)S(1)}, u32[]{:S(2)}, u32[]{:S(2)}) collective-permute-start(bf16[1,32,768]{2,1,0:T(8,128)(2,1)S(1)} %of_group.1), channel_id=1, source_target_pairs={{0,64},{32,96},{1,65},{33,97},{2,66},{34,98},{3,67},{35,99},{4,68}... | collective-permute-start | bytes 147464 | tf_op jit(solution)/shard_map/ppermute | solution.py:254
  60.3 9.1 %collective-permute-start.6 = (bf16[1,32,768]{2,1,0:T(8,128)(2,1)S(1)}, bf16[1,32,768]{2,1,0:T(8,128)(2,1)S(1)}, u32[]{:S(2)}, u32[]{:S(2)}) collective-permute-start(bf16[1,32,768]{2,1,0:T(8,128)(2,1)S(1)} %of_group.1), channel_id=1, source_target_pairs={{0,96},{1,97},{2,98},{3,99},{4,100},{5,101},{6,102},{7,103},{8,104... | collective-permute-start | bytes 147464 | tf_op jit(solution)/shard_map/ppermute | solution.py:254
  70.2 5.8 %collective-permute-start.7 = (bf16[32,640]{1,0:T(8,128)(2,1)S(1)}, bf16[32,640]{1,0:T(8,128)(2,1)S(1)}, u32[]{:S(2)}, u32[]{:S(2)}) collective-permute-start(bf16[32,640]{1,0:T(8,128)(2,1)S(1)} %get-tuple-element.15), channel_id=1, source_target_pairs={{0,8},{8,16},{16,24},{24,0},{1,9},{9,17},{17,25},{25,1},{2,10},{10... | collective-permute-start | bytes 122888 | tf_op jit(solution)/shard_map/ppermute | solution.py:254
  72.5 6.4 %collective-permute-start.8 = (bf16[32,640]{1,0:T(8,128)(2,1)S(1)}, bf16[32,640]{1,0:T(8,128)(2,1)S(1)}, u32[]{:S(2)}, u32[]{:S(2)}) collective-permute-start(bf16[32,640]{1,0:T(8,128)(2,1)S(1)} %get-tuple-element.14), channel_id=1, source_target_pairs={{0,16},{8,24},{16,0},{24,8},{1,17},{9,25},{17,1},{25,9},{2,18},{10... | collective-permute-start | bytes 122888 | tf_op jit(solution)/shard_map/ppermute | solution.py:254
  72.5 6.4 %collective-permute-start.9 = (bf16[32,640]{1,0:T(8,128)(2,1)S(1)}, bf16[32,640]{1,0:T(8,128)(2,1)S(1)}, u32[]{:S(2)}, u32[]{:S(2)}) collective-permute-start(bf16[32,640]{1,0:T(8,128)(2,1)S(1)} %get-tuple-element.13), channel_id=1, source_target_pairs={{0,24},{8,0},{16,8},{24,16},{1,25},{9,1},{17,9},{25,17},{2,26},{10... | collective-permute-start | bytes 122888 | tf_op jit(solution)/shard_map/ppermute | solution.py:254
  79.4 2.8 %collective-permute-start.10 = (bf16[128,640]{1,0:T(8,128)(2,1)S(1)}, bf16[128,640]{1,0:T(8,128)(2,1)S(1)}, u32[]{:S(2)}, u32[]{:S(2)}) collective-permute-start(bf16[128,640]{1,0:T(8,128)(2,1)S(1)} %gathered_half.1.own_half), channel_id=1, source_target_pairs={{0,4},{4,0},{1,5},{5,1},{2,6},{6,2},{3,7},{7,3},{8,12},{12,8},{9,1... | collective-permute-start | bytes 491528 | tf_op jit(solution)/shard_map/ppermute | solution.py:258
  87.6 1.3 copy-start.1
  88.9 31.5 %copy-start.12 = (f32[2048]{0:T(1024)S(1)}, f32[2048]{0:T(1024)}, u32[]{:S(2)}) copy-start(f32[2048]{0:T(1024)} %param.29) | copy-start | bytes 24580
  88.9 31.5 %all-to-all-start = ((bf16[4,128,2048]{2,1,0:T(8,128)(2,1)}), bf16[4,128,2048]{2,1,0:T(8,128)(2,1)}, u32[]{:S(2)}, u32[]{:S(2)}) async-start(bf16[4,128,2048]{2,1,0:T(8,128)(2,1)} %bitcast.26), calls=%async_computation | async-start | bytes 4194304 | tf_op jit(solution)/shard_map/all_to_all | solution.py:322
Sparse Core Ops, SparseCore 0:
  9.2 130.6 all-gather.1

commit v2 on v1

--- a/solution.py
+++ b/solution.py
@@ -23,19 +23,48 @@
     return pl.BlockSpec(memory_space=pltpu.SMEM)
 
 
-def call(body, outs, *args, scratch=(), flops=0, moved=0):
-    specs = [smem() if a.dtype == jnp.int32 else vmem() for a in args]
+def whole(a):
+    return pl.BlockSpec(a.shape, lambda *_: (0,) * len(a.shape))
+
+
+def call(body, outs, *args, scratch=(), flops=0, moved=0, pull=False):
     many = isinstance(outs, (list, tuple))
-    return pl.pallas_call(
-        body,
+    outs = list(outs) if many else [outs]
+    inner, pulled = body, []
+    if pull:
+        pulled = [n for n, a in enumerate(args) if a.dtype != jnp.int32]
+
+        def inner(*refs):
+            given = list(refs[: len(args)])
+            kept = refs[len(args) : len(refs) - len(pulled) - 1]
+            held, sems = refs[len(refs) - len(pulled) - 1 : -1], refs[-1]
+            copies = []
+            for k, n in enumerate(pulled):
+                copies.append(pltpu.make_async_copy(given[n], held[k], sems.at[k]))
+                copies[-1].start()
+                given[n] = held[k]
+            for copy in copies:
+                copy.wait()
+            body(*given, *kept)
+
+        far = pl.BlockSpec(memory_space=pltpu.HBM)
+        specs = [smem() if a.dtype == jnp.int32 else far for a in args]
+        scratch = list(scratch) + [pltpu.VMEM(args[n].shape, args[n].dtype) for n in pulled]
+        scratch.append(pltpu.SemaphoreType.DMA((len(pulled),)))
+    else:
+        specs = [smem() if a.dtype == jnp.int32 else vmem() for a in args]
+    result = pl.pallas_call(
+        inner,
+        grid=(1,) if pull else (),
         out_shape=outs,
         in_specs=specs,
-        out_specs=[vmem() for _ in outs] if many else vmem(),
+        out_specs=[whole(o) if pull else vmem() for o in outs],
         scratch_shapes=list(scratch),
         compiler_params=pltpu.CompilerParams(vmem_limit_bytes=48 * 2**20),
         cost_estimate=pl.CostEstimate(flops=flops, bytes_accessed=moved, transcendentals=0),
         name=body.__name__,
     )(*args)
+    return result if many else result[0]
 
 
 def shaped(shape, dtype):
@@ -200,8 +229,9 @@
 
 
 def heads_out(
-    place, own_half, other_half, sibling, qw, qn, dw, dn, within, gw, gn, ow, on, out,
-    came_wide, came_thin,
+    place, own_half, other_half, sibling, qw, qn, dw, dn, within, gw, gn, ow, on,
+    far_a, far_b, right_a, right_b, left_a, left_b, own_a, own_b,
+    came_wide, came_thin, turned_wide, turned_thin,
 ):
     first_core = place[0] == 0
     length = qw.shape[0]
@@ -232,21 +262,108 @@
 
     wide = normed(qw, came_wide, cum_wide, within[:, :wide_width], gw)
     thin = normed(qn, came_thin, cum_thin, within[:, wide_width:], gn)
+    outs = (far_a, far_b, right_a, right_b, left_a, left_b, own_a, own_b)
+    rows, members = far_a.shape[0], length // (2 * far_a.shape[0])
+    for m in range(members):
+        spot = lax.rem(m - place[2] + members, members)
+        order = jnp.where(spot == 2, 0, jnp.where(spot == 1, 1, jnp.where(spot == 3, 2, 3)))
+        start = pl.multiple_of(order * 2 * rows, 2 * rows)
+        turned_wide[pl.ds(start, 2 * rows), :] = wide[m * 2 * rows : (m + 1) * 2 * rows]
+        turned_thin[pl.ds(start, 2 * rows), :] = thin[m * 2 * rows : (m + 1) * 2 * rows]
     step = 512
     for n in range(ow.shape[1] // step):
         cols = slice(n * step, (n + 1) * step)
-        out[:, cols] = (mm(wide, ow[:, cols]) + mm(thin, on[:, cols])).astype(BF16)
-
-
-def rows_mid(parts, stream, gain, middle, normed):
-    total = parts[0].astype(F32)
-    for n in range(1, parts.shape[0]):
-        total = total + parts[n].astype(F32)
-    mid = (stream[...].astype(F32) + total).astype(BF16)
-    middle[...] = mid
-    values = mid.astype(F32)
-    power = jnp.mean(values * values, axis=-1, keepdims=True)
-    normed[...] = (values * lax.rsqrt(power + EPS) * gain[...]).astype(BF16)
+        done = (mm(turned_wide[...], ow[:, cols]) + mm(turned_thin[...], on[:, cols])).astype(BF16)
+        for m, out in enumerate(outs):
+            out[:, cols] = done[m * rows : (m + 1) * rows]
+
+
+def add_two(a, b, c, d, first, second):
+    first[...] = (a[...].astype(F32) + b[...].astype(F32)).astype(BF16)
+    second[...] = (c[...].astype(F32) + d[...].astype(F32)).astype(BF16)
+
+
+def rows_mid(
+    own_a, left_a, right_a, own_b, left_b, right_b, stream, gain,
+    mid_a, mid_b, normed_a, normed_b,
+):
+    rows = own_a.shape[0]
+    halves = ((own_a, left_a, right_a, mid_a, normed_a), (own_b, left_b, right_b, mid_b, normed_b))
+    for n, (own, left, right, middle, normed) in enumerate(halves):
+        total = own[...].astype(F32) + left[...].astype(F32) + right[...].astype(F32)
+        mid = (stream[n * rows : (n + 1) * rows].astype(F32) + total).astype(BF16)
+        middle[...] = mid
+        values = mid.astype(F32)
+        power = jnp.mean(values * values, axis=-1, keepdims=True)
+        normed[...] = (values * lax.rsqrt(power + EPS) * gain[...]).astype(BF16)
+
+
+def hidden_rows(a, b, c, d, up, down, out_a, out_b, out_c, out_d, rows, hidden, sems):
+    step = pl.program_id(0)
+    size, block = a.shape[0], up.shape[1]
+    ups = hidden.shape[1] // block
+
+    @pl.when(step == 0)
+    def _():
+        copies = [
+            pltpu.make_async_copy(part, rows.at[pl.ds(n * size, size), :], sems.at[n])
+            for n, part in enumerate((a, b, c, d))
+        ]
+        for copy in copies:
+            copy.start()
+        for copy in copies:
+            copy.wait()
+
+    @pl.when(step < ups)
+    def _():
+        raised = jnp.maximum(mm(rows[...], up[...]), 0.0)
+        start = pl.multiple_of(step * block, block)
+        hidden[:, pl.ds(start, block)] = (raised * raised).astype(BF16)
+
+    @pl.when(step >= ups)
+    def _():
+        done = mm(hidden[...], down[...], ((1,), (1,))).astype(BF16)
+        for n, out in enumerate((out_a, out_b, out_c, out_d)):
+            out[...] = done[n * size : (n + 1) * size]
+
+
+def feed_forward(parts, weights):
+    size, width = parts[0].shape
+    units = weights.shape[1] // 2
+    block = 256
+    ups, downs = units // block, width // block
+    put_out = pl.BlockSpec((size, block), lambda s: (0, jnp.maximum(s - ups, 0)))
+    return pl.pallas_call(
+        hidden_rows,
+        grid=(ups + downs,),
+        out_shape=[shaped((size, width), BF16)] * 4,
+        in_specs=[pl.BlockSpec(memory_space=pltpu.HBM) for _ in parts]
+        + [
+            pl.BlockSpec((width, block), lambda s: (0, jnp.minimum(s, ups - 1))),
+            pl.BlockSpec((block, units), lambda s: (jnp.maximum(s - ups, 0), 1)),
+        ],
+        out_specs=[put_out] * 4,
+        scratch_shapes=[
+            pltpu.VMEM((4 * size, width), BF16),
+            pltpu.VMEM((4 * size, units), BF16),
+            pltpu.SemaphoreType.DMA((4,)),
+        ],
+        compiler_params=pltpu.CompilerParams(vmem_limit_bytes=48 * 2**20),
+        cost_estimate=pl.CostEstimate(
+            flops=16 * size * width * units, bytes_accessed=4 * units * width, transcendentals=0
+        ),
+        name="hidden_rows",
+    )(*parts, weights, weights)
+
+
+def last_sum(own_a, left_a, right_a, mid_a, own_b, left_b, right_b, mid_b, out):
+    rows = own_a.shape[0]
+    halves = ((own_a, left_a, right_a, mid_a), (own_b, left_b, right_b, mid_b))
+    for n, parts in enumerate(halves):
+        total = parts[3][...].astype(F32)
+        for part in parts[:3]:
+            total = total + part[...].astype(F32)
+        out[n * rows : (n + 1) * rows] = total.astype(BF16)
 
 
 def shift(x, axis, by, size, wrap=True):
@@ -256,6 +373,28 @@
 
 def swap(x):
     return lax.ppermute(x, "core", [(0, 1), (1, 0)])
+
+
+def turn(x, by):
+    return shift(x, "tp", by, lax.axis_size("tp"))
+
+
+def sent_far(far_a, far_b):
+    return turn(far_a, 1), turn(far_b, -1)
+
+
+def reduced(far, right_a, right_b, left_a, left_b):
+    came_right_b, came_left_a = turn(right_b, 1), turn(left_a, -1)
+    like = [shaped(right_a.shape, BF16)] * 2
+    right_sum, left_sum = call(add_two, like, right_a, far[0], left_b, far[1], pull=True)
+    return turn(right_sum, 1), came_right_b, came_left_a, turn(left_sum, -1)
+
+
+def spread(a, b):
+    left_a, right_b = turn(a, 1), turn(b, -1)
+    left_b, right_a = turn(b, 1), turn(a, -1)
+    far_a, far_b = turn(left_a, 1), turn(right_b, -1)
+    return far_a, far_b, right_a, right_b, left_a, left_b
 
 
 def among(parts):
@@ -271,7 +410,7 @@
     length, width = stream_in.shape
     portion = length // members
     member = lax.axis_index("tp")
-    place = jnp.stack([lax.axis_index("core"), lax.axis_index("zb")]).astype(jnp.int32)
+    place = jnp.stack([lax.axis_index(n) for n in ("core", "zb", "tp")]).astype(jnp.int32)
 
     both = jnp.concatenate([up_weight, down_weight.T], axis=1)
     weights = lax.all_gather(both, SP, axis=0, tiled=True)
@@ -283,14 +422,14 @@
     own = call(
         own_state, shaped((2, half, lanes), BF16),
         key_wide, value_wide, decay_wide, key_narrow, value_narrow, decay_narrow,
-        flops=2 * length * wide_key * wide_value, moved=10**6,
+        flops=2 * length * wide_key * wide_value, moved=10**6, pull=True,
     )
     sibling = swap(own)
     within = call(
         inside, shaped((length, wide_value + thin_value), F32),
         query_wide, key_wide, value_wide, decay_wide,
         query_narrow, key_narrow, value_narrow, decay_narrow,
-        flops=6 * length * length * wide_value, moved=4 * 10**6,
+        flops=6 * length * length * wide_value, moved=4 * 10**6, pull=True,
     )
     rows = half // 4
     pieces = call(of_chip, shaped((4, rows, lanes), BF16), place, own, sibling)
@@ -308,32 +447,40 @@
     back = among([found[d] for d in range(4)])
     own_half = call(gathered_half, shaped((half, lanes - LANES), BF16), place, *back)
     other_half = swap(own_half)
-    partial = call(
-        heads_out, shaped((length, width), BF16),
+    quarter = portion // 2
+    far_a, far_b, right_a, right_b, left_a, left_b, own_a, own_b = call(
+        heads_out, [shaped((quarter, width), BF16)] * 8,
         place, own_half, other_half, sibling, query_wide, query_narrow,
         decay_wide, decay_narrow, within, gain_wide[None], gain_narrow[None],
         out_wide, out_narrow,
         scratch=[
             pltpu.VMEM((wide_key, wide_value), BF16),
             pltpu.VMEM((key_narrow.shape[1], thin_value), BF16),
+            pltpu.VMEM((length, wide_value), BF16),
+            pltpu.VMEM((length, thin_value), BF16),
         ],
-        flops=4 * length * wide_value * width, moved=8 * 10**6,
-    )
-    parts = lax.all_to_all(partial.reshape(members, portion, width), "tp", 0, 0, tiled=True)
+        flops=4 * length * wide_value * width, moved=8 * 10**6, pull=True,
+    )
+    from_left_a, from_left_b, from_right_a, from_right_b = reduced(
+        sent_far(far_a, far_b), right_a, right_b, left_a, left_b
+    )
     own_stream = lax.dynamic_slice_in_dim(stream_in, member * portion, portion, 0)
-    middle, normed = call(
-        rows_mid, [shaped((portion, width), BF16)] * 2, parts, own_stream, mlp_gain[None]
-    )
-    copies = jnp.broadcast_to(normed[None], (members, portion, width))
-    everyone = lax.all_to_all(copies, "tp", 0, 0, tiled=True).reshape(length, width)
-    units = up_weight.shape[1]
-    raised = jax.nn.relu(jnp.dot(everyone, weights[:, :units], preferred_element_type=F32))
-    hidden = (raised * raised).astype(BF16)
-    channel = lax.dot_general(
-        hidden, weights[:, units:], (((1,), (1,)), ((), ())), preferred_element_type=F32
-    ).astype(BF16)
-    summed = lax.all_to_all(channel.reshape(members, portion, width), "tp", 0, 0, tiled=True)
-    return (middle.astype(F32) + summed.astype(F32).sum(axis=0)).astype(BF16)
+    mid_a, mid_b, normed_a, normed_b = call(
+        rows_mid, [shaped((quarter, width), BF16)] * 4,
+        own_a, from_left_a, from_right_a, own_b, from_left_b, from_right_b,
+        own_stream, mlp_gain[None], pull=True,
+    )
+    far_a, far_b, right_a, right_b, left_a, left_b = spread(normed_a, normed_b)
+    far_a, far_b, right_a, right_b = feed_forward((far_a, far_b, right_a, right_b), weights)
+    far = sent_far(far_a, far_b)
+    left_a, left_b, own_a, own_b = feed_forward((left_a, left_b, normed_a, normed_b), weights)
+    from_left_a, from_left_b, from_right_a, from_right_b = reduced(
+        far, right_a, right_b, left_a, left_b
+    )
+    return call(
+        last_sum, shaped((portion, width), BF16),
+        own_a, from_left_a, from_right_a, mid_a, own_b, from_left_b, from_right_b, mid_b, pull=True,
+    )
 
 
 def solution(mesh):

time: 206 us -> 199 us (0.966)
  blocking collectives: 56.9 us -> 0 us
  Pallas kernels: 13.1 us -> 47.9 us
  starting transfers between devices: 48.5 us -> 67.2 us
  matrix products: 16.5 us -> 0 us
  local copies, waits for them, and re-layouts: 6.89 us -> 15 us
  waiting for transfers between devices: 45.4 us -> 50.9 us
    all_to_all x2 -> x0, blocking collectives: 56.9 us -> none  [the longest x1 28.7 us: on_device(): lax.all_to_all(copies, 'tp', 0, 0, tiled=True).reshape(length, width)]
    pallas_call x8 -> x13, Pallas kernels: 13.1 us -> 47.9 us  [the longest x2 30.2 us: feed_forward(): pl.pallas_call(hidden_rows, grid=(ups + downs,), out_shape=[shaped((size,...]
    ppermute x9 -> x27, waiting for transfers between devices: 17.4 us -> 44.3 us  [shift(): return lax.ppermute(x, axis, pairs)]
    all_to_all x1 -> x0, waiting for transfers between devices: 26.6 us -> none  [on_device(): lax.all_to_all(partial.reshape(members, portion, width), 'tp', 0, 0, tile...]
    ppermute x9 -> x27, starting transfers between devices: 21.6 us -> 44.3 us  [shift(): return lax.ppermute(x, axis, pairs)]
    dot_general x1 -> x0, matrix products: 16.5 us -> none  [on_device(): lax.dot_general(hidden, weights[:, units:], (((1,), (1,)), ((), ())), pre...]
    unnamed x40 -> x66, local copies, waits for them, and re-layouts: 6.57 us -> 14.9 us
    all_gather x1, waiting for transfers between devices: 0.01 us -> 5.1 us  [on_device(): weights = lax.all_gather(both, SP, axis=0, tiled=True)]
  transfers between devices with their start and end apart: 13 -> 30, of which waited for: 9 -> 19; matrix products, arithmetic and copies ran while one was open for 0% -> 0% of each run, Pallas kernels for 6% -> 24%
where the time goes in v2:
time: 199 us; the launch traced here: 197 us
  starting transfers between devices  67.2 us (34%)
  waiting for transfers between devices  50.9 us (26%)
  Pallas kernels  47.9 us (24%)
  local copies, waits for them, and re-layouts  15 us (8%)
  between operations  13.8 us (7%)
  other arithmetic  2.08 us (1%)
    ppermute x27, waiting for transfers between devices, shift(): return lax.ppermute(x, axis, pairs)  44.3 us
    ppermute x27, starting transfers between devices, shift(): return lax.ppermute(x, axis, pairs)  44.3 us
    pallas_call x2, Pallas kernels, feed_forward(): pl.pallas_call(hidden_rows, grid=(ups + downs,), out_shape=[shaped((size,...  30.2 us
    ppermute x2, starting transfers between devices, swap(): return lax.ppermute(x, 'core', [(0, 1), (1, 0)])  22.9 us
    pallas_call x11, Pallas kernels, call(): pl.pallas_call(inner, grid=(1,) if pull else (), out_shape=outs, in_specs...  17.7 us
    unnamed x66, local copies, waits for them, and re-layouts  14.9 us
    all_gather x1, waiting for transfers between devices, on_device(): weights = lax.all_gather(both, SP, axis=0, tiled=True)  5.1 us
  transfers between devices with their start and end apart: 30, of which 19 were waited for; matrix products, arithmetic and copies ran while one was open for 0% of the time, Pallas kernels for 24%

profile of v2, /device:TPU:33, one launch (start us, length us, event | category | flops | bytes accessed | tf_op | source)
XLA Modules:
  0.0 196.8 jit_solution(14111930853080105507)
XLA Ops:
  6.6 2.0 %pad_maximum_fusion = bf16[64,4096]{1,0:T(8,128)(2,1)} fusion(bf16[64,2048]{1,0:T(8,128)(2,1)} %bitcast.26, bf16[64,2048]{1,0:T(8,128)(2,1)} %param.30), kind=kLoop, calls=%fused_computation | loop fusion | flops 1048576 | bytes 1048576 | tf_op jit(solution)/shard_map/concatenate | solution.py:415
  8.6 1.0 copy-done.1
  9.7 0.9 copy-done.3
  10.6 0.9 copy-done.5
  11.6 0.9 copy-done.7
  13.9 1.3 own_state.1.own
  15.1 20.5 %collective-permute-start = (bf16[2,128,768]{2,1,0:T(8,128)(2,1)S(1)}, bf16[2,128,768]{2,1,0:T(8,128)(2,1)}, u32[]{:S(2)}, u32[]{:S(2)}) collective-permute-start(bf16[2,128,768]{2,1,0:T(8,128)(2,1)S(1)} %own_state.1.own), channel_id=1, source_target_pairs={{0,4},{4,0},{1,5},{5,1},{2,6},{6,2},{3,7},{7,3},{8,12},{12,8},{9,1... | collective-permute-start | bytes 1179656 | tf_op jit(solution)/shard_map/ppermute | solution.py:375
  35.8 1.4 collective-permute-done.sibling.refs_3_
  37.2 1.4 of_chip.1
  38.9 3.1 %collective-permute-start.3 = (bf16[32,768]{1,0:T(8,128)(2,1)S(1)}, bf16[32,768]{1,0:T(8,128)(2,1)S(1)}, u32[]{:S(2)}, u32[]{:S(2)}) collective-permute-start(bf16[32,768]{1,0:T(8,128)(2,1)S(1)} %get-tuple-element.53), channel_id=1, source_target_pairs={{0,24},{8,0},{16,8},{24,16},{1,25},{9,1},{17,9},{25,17},{2,26},{10... | collective-permute-start | bytes 147464 | tf_op jit(solution)/shard_map/ppermute | solution.py:371
  41.9 2.8 %collective-permute-done.1.b = bf16[32,768]{1,0:T(8,128)(2,1)S(1)} collective-permute-done((bf16[32,768]{1,0:T(8,128)(2,1)S(1)}, bf16[32,768]{1,0:T(8,128)(2,1)S(1)}, u32[]{:S(2)}, u32[]{:S(2)}) %collective-permute-start.1) | collective-permute-done | bytes 49184 | tf_op jit(solution)/shard_map/ppermute | solution.py:371
  44.8 2.5 %collective-permute-done.3.d = bf16[32,768]{1,0:T(8,128)(2,1)S(1)} collective-permute-done((bf16[32,768]{1,0:T(8,128)(2,1)S(1)}, bf16[32,768]{1,0:T(8,128)(2,1)S(1)}, u32[]{:S(2)}, u32[]{:S(2)}) %collective-permute-start.3) | collective-permute-done | bytes 49184 | tf_op jit(solution)/shard_map/ppermute | solution.py:371
  47.3 0.8 of_group.1
  48.1 1.4 collective-permute-start.4
  49.6 11.0 %collective-permute-start.5 = (bf16[1,32,768]{2,1,0:T(8,128)(2,1)S(1)}, bf16[1,32,768]{2,1,0:T(8,128)(2,1)S(1)}, u32[]{:S(2)}, u32[]{:S(2)}) collective-permute-start(bf16[1,32,768]{2,1,0:T(8,128)(2,1)S(1)} %of_group.1), channel_id=1, source_target_pairs={{0,64},{32,96},{1,65},{33,97},{2,66},{34,98},{3,67},{35,99},{4,68}... | collective-permute-start | bytes 147464 | tf_op jit(solution)/shard_map/ppermute | solution.py:371
  60.6 1.3 collective-permute-start.6
  61.9 0.9 collective-permute-done.5.mid
  62.8 6.2 %collective-permute-done.6.far = bf16[1,32,768]{2,1,0:T(8,128)(2,1)S(1)} collective-permute-done((bf16[1,32,768]{2,1,0:T(8,128)(2,1)S(1)}, bf16[1,32,768]{2,1,0:T(8,128)(2,1)S(1)}, u32[]{:S(2)}, u32[]{:S(2)}) %collective-permute-start.6) | collective-permute-done | bytes 49184 | tf_op jit(solution)/shard_map/ppermute | solution.py:371
  68.9 0.8 before_each.1
  69.7 2.9 %collective-permute-start.7 = (bf16[32,640]{1,0:T(8,128)(2,1)S(1)}, bf16[32,640]{1,0:T(8,128)(2,1)S(1)}, u32[]{:S(2)}, u32[]{:S(2)}) collective-permute-start(bf16[32,640]{1,0:T(8,128)(2,1)S(1)} %get-tuple-element.59), channel_id=1, source_target_pairs={{0,8},{8,16},{16,24},{24,0},{1,9},{9,17},{17,25},{25,1},{2,10},{10... | collective-permute-start | bytes 122888 | tf_op jit(solution)/shard_map/ppermute | solution.py:371
  72.7 2.2 %collective-permute-start.9 = (bf16[32,640]{1,0:T(8,128)(2,1)S(1)}, bf16[32,640]{1,0:T(8,128)(2,1)S(1)}, u32[]{:S(2)}, u32[]{:S(2)}) collective-permute-start(bf16[32,640]{1,0:T(8,128)(2,1)S(1)} %get-tuple-element.57), channel_id=1, source_target_pairs={{0,24},{8,0},{16,8},{24,16},{1,25},{9,1},{17,9},{25,17},{2,26},{10... | collective-permute-start | bytes 122888 | tf_op jit(solution)/shard_map/ppermute | solution.py:371
  75.5 3.0 %collective-permute-done.8.c = bf16[32,640]{1,0:T(8,128)(2,1)S(1)} collective-permute-done((bf16[32,640]{1,0:T(8,128)(2,1)S(1)}, bf16[32,640]{1,0:T(8,128)(2,1)S(1)}, u32[]{:S(2)}, u32[]{:S(2)}) %collective-permute-start.8) | collective-permute-done | bytes 40992 | tf_op jit(solution)/shard_map/ppermute | solution.py:371
  79.1 2.3 %collective-permute-start.10 = (bf16[128,640]{1,0:T(8,128)(2,1)S(1)}, bf16[128,640]{1,0:T(8,128)(2,1)S(1)}, u32[]{:S(2)}, u32[]{:S(2)}) collective-permute-start(bf16[128,640]{1,0:T(8,128)(2,1)S(1)} %gathered_half.1.refs_1_), channel_id=1, source_target_pairs={{0,4},{4,0},{1,5},{5,1},{2,6},{6,2},{3,7},{7,3},{8,12},{12,8},{9,1... | collective-permute-start | bytes 491528 | tf_op jit(solution)/shard_map/ppermute | solution.py:375
  81.5 1.7 inside.1.refs_8_
  83.2 7.2 %heads_out.1 = (bf16[64,2048]{1,0:T(8,128)(2,1)S(1)}, bf16[64,2048]{1,0:T(8,128)(2,1)S(1)}, bf16[64,2048]{1,0:T(8,128)(2,1)S(1)}, bf16[64,2048]{1,0:T(8,128)(2,1...) custom-call(s32[3]{0:T(128)S(1)} %pad_add_fusion.place.refs_0_, ...), custom_call_target="tpu_custom_call" | custom-call | flops 2147483648 | bytes 8000000 | tf_op jit(solution)/shard_map/heads_out/pallas_call | solution.py:56
  90.5 1.7 collective-permute-start.11
  92.2 1.7 collective-permute-start.12
  93.8 1.3 collective-permute-start.14
  95.3 5.0 %collective-permute-done.11.refs_1_ = bf16[64,2048]{1,0:T(8,128)(2,1)S(1)} collective-permute-done((bf16[64,2048]{1,0:T(8,128)(2,1)S(1)}, bf16[64,2048]{1,0:T(8,128)(2,1)S(1)}, u32[]{:S(2)}, u32[]{:S(2)}) %collective-permute-start.11) | collective-permute-done | bytes 262176 | tf_op jit(solution)/shard_map/ppermute | solution.py:371
  100.3 1.0 add_two.2
  101.3 1.0 collective-permute-start.13
  102.2 1.9 collective-permute-start.16
  104.1 1.3 collective-permute-done.14.refs_2_
  105.9 0.7 copy-done.20
  106.6 4.1 %collective-permute-done.13.refs_1_ = bf16[64,2048]{1,0:T(8,128)(2,1)S(1)} collective-permute-done((bf16[64,2048]{1,0:T(8,128)(2,1)}, bf16[64,2048]{1,0:T(8,128)(2,1)S(1)}, u32[]{:S(2)}, u32[]{:S(2)}) %collective-permute-start.13) | collective-permute-done | bytes 262176 | tf_op jit(solution)/shard_map/ppermute | solution.py:371
  110.7 0.7 copy-done.22
  111.5 1.0 copy-done.21
  112.4 0.9 copy-done.23
  113.4 1.6 rows_mid.1
  114.9 0.7 copy-done.16
  115.6 0.7 copy-done.18
  116.7 2.3 %collective-permute-start.20 = (bf16[64,2048]{1,0:T(8,128)(2,1)S(1)}, bf16[64,2048]{1,0:T(8,128)(2,1)S(1)}, u32[]{:S(2)}, u32[]{:S(2)}) collective-permute-start(bf16[64,2048]{1,0:T(8,128)(2,1)S(1)} %get-tuple-element.40.d), channel_id=1, source_target_pairs={{0,3},{1,0},{2,1},{3,2},{4,7},{5,4},{6,5},{7,6},{8,11},{9,8},{10,9... | collective-permute-start | bytes 786440 | tf_op jit(solution)/shard_map/ppermute | solution.py:371
  119.0 0.7 collective-permute-start.22
  119.7 4.3 %collective-permute-done.17.a = bf16[64,2048]{1,0:T(8,128)(2,1)S(1)} collective-permute-done((bf16[64,2048]{1,0:T(8,128)(2,1)S(1)}, bf16[64,2048]{1,0:T(8,128)(2,1)S(1)}, u32[]{:S(2)}, u32[]{:S(2)}) %collective-permute-start.17) | collective-permute-done | bytes 262176 | tf_op jit(solution)/shard_map/ppermute | solution.py:371
  124.0 2.7 %collective-permute-start.21 = (bf16[64,2048]{1,0:T(8,128)(2,1)S(1)}, bf16[64,2048]{1,0:T(8,128)(2,1)S(1)}, u32[]{:S(2)}, u32[]{:S(2)}) collective-permute-start(bf16[64,2048]{1,0:T(8,128)(2,1)S(1)} %collective-permute-done.20.d), channel_id=1, source_target_pairs={{0,3},{1,0},{2,1},{3,2},{4,7},{5,4},{6,5},{7,6},{8,11},{9,8},{10,9... | collective-permute-start | bytes 786440 | tf_op jit(solution)/shard_map/ppermute | solution.py:371
  126.7 1.8 collective-permute-done.22.c
  128.5 0.7 copy-done.9
  129.2 1.7 collective-permute-done.19.a
  130.9 0.7 copy-done.11
  131.6 2.5 %collective-permute-done.21.b = bf16[64,2048]{1,0:T(8,128)(2,1)S(1)} collective-permute-done((bf16[64,2048]{1,0:T(8,128)(2,1)S(1)}, bf16[64,2048]{1,0:T(8,128)(2,1)S(1)}, u32[]{:S(2)}, u32[]{:S(2)}) %collective-permute-start.21) | collective-permute-done | bytes 262176 | tf_op jit(solution)/shard_map/ppermute | solution.py:371
  134.1 0.7 copy-done.13
  134.8 5.1 %all-gather.2.cloned.1.call-done.up.down = bf16[2048,4096]{1,0:T(8,128)(2,1)} async-done(((bf16[64,4096]{1,0:T(8,128)(2,1)}), bf16[2048,4096]{1,0:T(8,128)(2,1)}) %all-gather.2.cloned.1.call-update) | async-done | bytes 16777232 | tf_op jit(solution)/shard_map/all_gather | solution.py:416
  139.9 0.9 copy-done.10
  140.9 0.9 copy-done.12
  141.8 0.9 copy-done.14
  142.8 15.1 %hidden_rows.3 = (bf16[64,2048]{1,0:T(8,128)(2,1)S(1)}, bf16[64,2048]{1,0:T(8,128)(2,1)S(1)}, bf16[64,2048]{1,0:T(8,128)(2,1)S(1)}, bf16[64,2048]{1,0:T(8,128)(2,1)S(1)}) custom-call(bf16[64,2048]{1,0:T(8,128)(2,1)S(1)} %copy-done.12, bf16[64,2048]{1,0:T(8,128)(2,1)S(1)} %copy-done.14, bf16[64,2048]{1,0:T(8,128)(2,1)S(1)} %copy-done.10, ...), custom_call_target="tpu_custom_call" | custom-call | flops 4294967296 | bytes 16777216 | tf_op jit(solution)/shard_map/hidden_rows/pallas_call | solution.py:336
  158.0 2.7 %collective-permute-start.24 = (bf16[64,2048]{1,0:T(8,128)(2,1)S(1)}, bf16[64,2048]{1,0:T(8,128)(2,1)S(1)}, u32[]{:S(2)}, u32[]{:S(2)}) collective-permute-start(bf16[64,2048]{1,0:T(8,128)(2,1)S(1)} %get-tuple-element.45), channel_id=1, source_target_pairs={{0,3},{1,0},{2,1},{3,2},{4,7},{5,4},{6,5},{7,6},{8,11},{9,8},{10,9... | collective-permute-start | bytes 786440 | tf_op jit(solution)/shard_map/ppermute | solution.py:371
  160.7 15.1 %hidden_rows.2 = (bf16[64,2048]{1,0:T(8,128)(2,1)S(1)}, bf16[64,2048]{1,0:T(8,128)(2,1)S(1)}, bf16[64,2048]{1,0:T(8,128)(2,1)S(1)}, bf16[64,2048]{1,0:T(8,128)(2,1)S(1)}) custom-call(bf16[64,2048]{1,0:T(8,128)(2,1)S(1)} %collective-permute-done.17.a, bf16[64,2048]{1,0:T(8,128)(2,1)S(1)} %collective-permute-done.18.b, ...), custom_call_target="tpu_custom_call" | custom-call | flops 4294967296 | bytes 16777216 | tf_op jit(solution)/shard_map/hidden_rows/pallas_call | solution.py:336
  175.8 2.7 %collective-permute-start.26 = (bf16[64,2048]{1,0:T(8,128)(2,1)S(1)}, bf16[64,2048]{1,0:T(8,128)(2,1)S(1)}, u32[]{:S(2)}, u32[]{:S(2)}) collective-permute-start(bf16[64,2048]{1,0:T(8,128)(2,1)S(1)} %get-tuple-element.47), channel_id=1, source_target_pairs={{0,3},{1,0},{2,1},{3,2},{4,7},{5,4},{6,5},{7,6},{8,11},{9,8},{10,9... | collective-permute-start | bytes 786440 | tf_op jit(solution)/shard_map/ppermute | solution.py:371
  178.9 2.6 %collective-permute-start.28 = (bf16[64,2048]{1,0:T(8,128)(2,1)S(1)}, bf16[64,2048]{1,0:T(8,128)(2,1)S(1)}, u32[]{:S(2)}, u32[]{:S(2)}) collective-permute-start(bf16[64,2048]{1,0:T(8,128)(2,1)S(1)} %get-tuple-element.51), channel_id=1, source_target_pairs={{0,3},{1,0},{2,1},{3,2},{4,7},{5,4},{6,5},{7,6},{8,11},{9,8},{10,9... | collective-permute-start | bytes 786440 | tf_op jit(solution)/shard_map/ppermute | solution.py:371
  181.5 1.5 collective-permute-done.26.refs_2_
  183.0 3.5 %collective-permute-done.25.refs_1_ = bf16[64,2048]{1,0:T(8,128)(2,1)S(1)} collective-permute-done((bf16[64,2048]{1,0:T(8,128)(2,1)S(1)}, bf16[64,2048]{1,0:T(8,128)(2,1)S(1)}, u32[]{:S(2)}, u32[]{:S(2)}) %collective-permute-start.25) | collective-permute-done | bytes 262176 | tf_op jit(solution)/shard_map/ppermute | solution.py:371
  186.5 2.1 %collective-permute-done.28.refs_6_ = bf16[64,2048]{1,0:T(8,128)(2,1)S(1)} collective-permute-done((bf16[64,2048]{1,0:T(8,128)(2,1)S(1)}, bf16[64,2048]{1,0:T(8,128)(2,1)S(1)}, u32[]{:S(2)}, u32[]{:S(2)}) %collective-permute-start.28) | collective-permute-done | bytes 262176 | tf_op jit(solution)/shard_map/ppermute | solution.py:371
  188.7 1.3 last_sum.1
  (81 shorter events, 4.7 us)
Async XLA Ops:
  6.5 97.5 %copy-start = (bf16[512,2048]{1,0:T(8,128)(2,1)S(1)}, bf16[512,2048]{1,0:T(8,128)(2,1)}, u32[]{:S(2)}) copy-start(bf16[512,2048]{1,0:T(8,128)(2,1)} %param.16) | copy-start | bytes 6291460
  6.6 133.4 %all-gather.2.cloned.1.call-start = ((), (), s32[]{:S(2)}) async-start(), calls=%async_computation | async-start | bytes 17301504 | tf_op jit(solution)/shard_map/all_gather | solution.py:416
  8.6 1.0 copy-start.1
  9.7 0.9 copy-start.3
  10.6 0.9 copy-start.5
  11.6 0.9 copy-start.7
  12.5 0.7 copy-start.26
  13.2 0.7 copy-start.28
  13.8 67.6 %copy-start.2 = (bf16[512,512]{1,0:T(8,128)(2,1)S(1)}, bf16[512,512]{1,0:T(8,128)(2,1)}, u32[]{:S(2)}) copy-start(bf16[512,512]{1,0:T(8,128)(2,1)} %refs_2_.3) | copy-start | bytes 1572868
  13.8 67.6 %copy-start.4 = (bf16[512,256]{1,0:T(8,128)(2,1)S(1)}, bf16[512,256]{1,0:T(8,128)(2,1)}, u32[]{:S(2)}) copy-start(bf16[512,256]{1,0:T(8,128)(2,1)} %refs_1_.3) | copy-start | bytes 786436
  13.8 67.6 %copy-start.6 = (bf16[512,256]{1,0:T(8,128)(2,1)S(1)}, bf16[512,256]{1,0:T(8,128)(2,1)}, u32[]{:S(2)}) copy-start(bf16[512,256]{1,0:T(8,128)(2,1)} %refs_6_.2) | copy-start | bytes 786436
  13.8 67.6 %copy-start.27 = (f32[1,512]{1,0:T(1,128)S(1)}, f32[1,512]{1,0:T(1,128)}, u32[]{:S(2)}) copy-start(f32[1,512]{1,0:T(1,128)} %refs_6_.3) | copy-start | bytes 6148
  13.8 67.6 %copy-start.29 = (f32[1,512]{1,0:T(1,128)S(1)}, f32[1,512]{1,0:T(1,128)}, u32[]{:S(2)}) copy-start(f32[1,512]{1,0:T(1,128)} %refs_7_.3) | copy-start | bytes 6148
  15.1 22.0 %collective-permute-start = (bf16[2,128,768]{2,1,0:T(8,128)(2,1)S(1)}, bf16[2,128,768]{2,1,0:T(8,128)(2,1)}, u32[]{:S(2)}, u32[]{:S(2)}) collective-permute-start(bf16[2,128,768]{2,1,0:T(8,128)(2,1)S(1)} %own_state.1.own), channel_id=1, source_target_pairs={{0,4},{4,0},{1,5},{5,1},{2,6},{6,2},{3,7},{7,3},{8,12},{12,8},{9,1... | collective-permute-start | bytes 1179656 | tf_op jit(solution)/shard_map/ppermute | solution.py:375
  35.7 45.8 %copy-start.8 = (bf16[512,128]{1,0:T(8,128)(2,1)S(1)}, bf16[512,128]{1,0:T(8,128)(2,1)}, u32[]{:S(2)}) copy-start(bf16[512,128]{1,0:T(8,128)(2,1)} %refs_5_.4) | copy-start | bytes 393220
  35.7 45.8 %copy-start.15 = (bf16[512,256]{1,0:T(8,128)(2,1)S(1)}, bf16[512,256]{1,0:T(8,128)(2,1)}, u32[]{:S(2)}) copy-start(bf16[512,256]{1,0:T(8,128)(2,1)} %refs_4_.5) | copy-start | bytes 786436
  35.7 45.8 %copy-start.24 = (bf16[512,128]{1,0:T(8,128)(2,1)S(1)}, bf16[512,128]{1,0:T(8,128)(2,1)}, u32[]{:S(2)}) copy-start(bf16[512,128]{1,0:T(8,128)(2,1)} %refs_5_.5) | copy-start | bytes 393220
  38.6 6.2 %collective-permute-start.1 = (bf16[32,768]{1,0:T(8,128)(2,1)S(1)}, bf16[32,768]{1,0:T(8,128)(2,1)S(1)}, u32[]{:S(2)}, u32[]{:S(2)}) collective-permute-start(bf16[32,768]{1,0:T(8,128)(2,1)S(1)} %get-tuple-element.55), channel_id=1, source_target_pairs={{0,8},{8,16},{16,24},{24,0},{1,9},{9,17},{17,25},{25,1},{2,10},{10... | collective-permute-start | bytes 147464 | tf_op jit(solution)/shard_map/ppermute | solution.py:371
  38.7 6.1 %collective-permute-start.2 = (bf16[32,768]{1,0:T(8,128)(2,1)S(1)}, bf16[32,768]{1,0:T(8,128)(2,1)S(1)}, u32[]{:S(2)}, u32[]{:S(2)}) collective-permute-start(bf16[32,768]{1,0:T(8,128)(2,1)S(1)} %get-tuple-element.54), channel_id=1, source_target_pairs={{0,16},{8,24},{16,0},{24,8},{1,17},{9,25},{17,1},{25,9},{2,18},{10... | collective-permute-start | bytes 147464 | tf_op jit(solution)/shard_map/ppermute | solution.py:371
  38.9 8.5 %collective-permute-start.3 = (bf16[32,768]{1,0:T(8,128)(2,1)S(1)}, bf16[32,768]{1,0:T(8,128)(2,1)S(1)}, u32[]{:S(2)}, u32[]{:S(2)}) collective-permute-start(bf16[32,768]{1,0:T(8,128)(2,1)S(1)} %get-tuple-element.53), channel_id=1, source_target_pairs={{0,24},{8,0},{16,8},{24,16},{1,25},{9,1},{17,9},{25,17},{2,26},{10... | collective-permute-start | bytes 147464 | tf_op jit(solution)/shard_map/ppermute | solution.py:371
  48.1 35.1 %copy-start.30 = (bf16[256,2048]{1,0:T(8,128)(2,1)S(1)}, bf16[256,2048]{1,0:T(8,128)(2,1)}, u32[]{:S(2)}) copy-start(bf16[256,2048]{1,0:T(8,128)(2,1)} %refs_12_.1) | copy-start | bytes 3145732
  48.1 35.1 %copy-start.31 = (f32[512]{0:T(512)S(1)}, f32[512]{0:T(512)}, u32[]{:S(2)}) copy-start(f32[512]{0:T(512)} %param.25) | copy-start | bytes 6148
  48.1 35.1 %copy-start.32 = (f32[256]{0:T(256)S(1)}, f32[256]{0:T(256)}, u32[]{:S(2)}) copy-start(f32[256]{0:T(256)} %param.26) | copy-start | bytes 3076
  48.1 13.8 %collective-permute-start.4 = (bf16[1,32,768]{2,1,0:T(8,128)(2,1)S(1)}, bf16[1,32,768]{2,1,0:T(8,128)(2,1)S(1)}, u32[]{:S(2)}, u32[]{:S(2)}) collective-permute-start(bf16[1,32,768]{2,1,0:T(8,128)(2,1)S(1)} %of_group.1), channel_id=1, source_target_pairs={{0,32},{32,64},{64,96},{1,33},{33,65},{65,97},{2,34},{34,66},{66,9... | collective-permute-start | bytes 147464 | tf_op jit(solution)/shard_map/ppermute | solution.py:371
  49.6 13.2 %collective-permute-start.5 = (bf16[1,32,768]{2,1,0:T(8,128)(2,1)S(1)}, bf16[1,32,768]{2,1,0:T(8,128)(2,1)S(1)}, u32[]{:S(2)}, u32[]{:S(2)}) collective-permute-start(bf16[1,32,768]{2,1,0:T(8,128)(2,1)S(1)} %of_group.1), channel_id=1, source_target_pairs={{0,64},{32,96},{1,65},{33,97},{2,66},{34,98},{3,67},{35,99},{4,68}... | collective-permute-start | bytes 147464 | tf_op jit(solution)/shard_map/ppermute | solution.py:371
  60.6 8.3 %collective-permute-start.6 = (bf16[1,32,768]{2,1,0:T(8,128)(2,1)S(1)}, bf16[1,32,768]{2,1,0:T(8,128)(2,1)S(1)}, u32[]{:S(2)}, u32[]{:S(2)}) collective-permute-start(bf16[1,32,768]{2,1,0:T(8,128)(2,1)S(1)} %of_group.1), channel_id=1, source_target_pairs={{0,96},{1,97},{2,98},{3,99},{4,100},{5,101},{6,102},{7,103},{8,104... | collective-permute-start | bytes 147464 | tf_op jit(solution)/shard_map/ppermute | solution.py:371
  69.7 5.8 %collective-permute-start.7 = (bf16[32,640]{1,0:T(8,128)(2,1)S(1)}, bf16[32,640]{1,0:T(8,128)(2,1)S(1)}, u32[]{:S(2)}, u32[]{:S(2)}) collective-permute-start(bf16[32,640]{1,0:T(8,128)(2,1)S(1)} %get-tuple-element.59), channel_id=1, source_target_pairs={{0,8},{8,16},{16,24},{24,0},{1,9},{9,17},{17,25},{25,1},{2,10},{10... | collective-permute-start | bytes 122888 | tf_op jit(solution)/shard_map/ppermute | solution.py:371
  72.7 5.8 %collective-permute-start.8 = (bf16[32,640]{1,0:T(8,128)(2,1)S(1)}, bf16[32,640]{1,0:T(8,128)(2,1)S(1)}, u32[]{:S(2)}, u32[]{:S(2)}) collective-permute-start(bf16[32,640]{1,0:T(8,128)(2,1)S(1)} %get-tuple-element.58), channel_id=1, source_target_pairs={{0,16},{8,24},{16,0},{24,8},{1,17},{9,25},{17,1},{25,9},{2,18},{10... | collective-permute-start | bytes 122888 | tf_op jit(solution)/shard_map/ppermute | solution.py:371
  72.7 5.8 %collective-permute-start.9 = (bf16[32,640]{1,0:T(8,128)(2,1)S(1)}, bf16[32,640]{1,0:T(8,128)(2,1)S(1)}, u32[]{:S(2)}, u32[]{:S(2)}) collective-permute-start(bf16[32,640]{1,0:T(8,128)(2,1)S(1)} %get-tuple-element.57), channel_id=1, source_target_pairs={{0,24},{8,0},{16,8},{24,16},{1,25},{9,1},{17,9},{25,17},{2,26},{10... | collective-permute-start | bytes 122888 | tf_op jit(solution)/shard_map/ppermute | solution.py:371
  79.1 4.1 %collective-permute-start.10 = (bf16[128,640]{1,0:T(8,128)(2,1)S(1)}, bf16[128,640]{1,0:T(8,128)(2,1)S(1)}, u32[]{:S(2)}, u32[]{:S(2)}) collective-permute-start(bf16[128,640]{1,0:T(8,128)(2,1)S(1)} %gathered_half.1.refs_1_), channel_id=1, source_target_pairs={{0,4},{4,0},{1,5},{5,1},{2,6},{6,2},{3,7},{7,3},{8,12},{12,8},{9,1... | collective-permute-start | bytes 491528 | tf_op jit(solution)/shard_map/ppermute | solution.py:375
  90.4 21.0 %copy-start.25 = (f32[2048]{0:T(1024)S(1)}, f32[2048]{0:T(1024)}, u32[]{:S(2)}) copy-start(f32[2048]{0:T(1024)} %param.29) | copy-start | bytes 24580
  90.5 9.8 %collective-permute-start.11 = (bf16[64,2048]{1,0:T(8,128)(2,1)S(1)}, bf16[64,2048]{1,0:T(8,128)(2,1)S(1)}, u32[]{:S(2)}, u32[]{:S(2)}) collective-permute-start(bf16[64,2048]{1,0:T(8,128)(2,1)S(1)} %get-tuple-element.31), channel_id=1, source_target_pairs={{0,1},{1,2},{2,3},{3,0},{4,5},{5,6},{6,7},{7,4},{8,9},{9,10},{10,1... | collective-permute-start | bytes 786440 | tf_op jit(solution)/shard_map/ppermute | solution.py:371
  92.2 8.1 %collective-permute-start.12 = (bf16[64,2048]{1,0:T(8,128)(2,1)S(1)}, bf16[64,2048]{1,0:T(8,128)(2,1)S(1)}, u32[]{:S(2)}, u32[]{:S(2)}) collective-permute-start(bf16[64,2048]{1,0:T(8,128)(2,1)S(1)} %get-tuple-element.33), channel_id=1, source_target_pairs={{0,3},{1,0},{2,1},{3,2},{4,7},{5,4},{6,5},{7,6},{8,11},{9,8},{10,9... | collective-permute-start | bytes 786440 | tf_op jit(solution)/shard_map/ppermute | solution.py:371
  93.8 11.6 %collective-permute-start.14 = (bf16[64,2048]{1,0:T(8,128)(2,1)}, bf16[64,2048]{1,0:T(8,128)(2,1)S(1)}, u32[]{:S(2)}, u32[]{:S(2)}) collective-permute-start(bf16[64,2048]{1,0:T(8,128)(2,1)} %get-tuple-element.35), channel_id=1, source_target_pairs={{0,3},{1,0},{2,1},{3,2},{4,7},{5,4},{6,5},{7,6},{8,11},{9,8},{10,9... | collective-permute-start | bytes 786440 | tf_op jit(solution)/shard_map/ppermute | solution.py:371
  95.2 10.7 %collective-permute-start.15 = (bf16[64,2048]{1,0:T(8,128)(2,1)}, bf16[64,2048]{1,0:T(8,128)(2,1)S(1)}, u32[]{:S(2)}, u32[]{:S(2)}) collective-permute-start(bf16[64,2048]{1,0:T(8,128)(2,1)} %get-tuple-element.37), channel_id=1, source_target_pairs={{0,1},{1,2},{2,3},{3,0},{4,5},{5,6},{6,7},{7,4},{8,9},{9,10},{10,1... | collective-permute-start | bytes 786440 | tf_op jit(solution)/shard_map/ppermute | solution.py:371
  101.3 9.5 %collective-permute-start.13 = (bf16[64,2048]{1,0:T(8,128)(2,1)}, bf16[64,2048]{1,0:T(8,128)(2,1)S(1)}, u32[]{:S(2)}, u32[]{:S(2)}) collective-permute-start(bf16[64,2048]{1,0:T(8,128)(2,1)} %get-tuple-element.34), channel_id=1, source_target_pairs={{0,1},{1,2},{2,3},{3,0},{4,5},{5,6},{6,7},{7,4},{8,9},{9,10},{10,1... | collective-permute-start | bytes 786440 | tf_op jit(solution)/shard_map/ppermute | solution.py:371
  102.2 9.2 %collective-permute-start.16 = (bf16[64,2048]{1,0:T(8,128)(2,1)}, bf16[64,2048]{1,0:T(8,128)(2,1)}, u32[]{:S(2)}, u32[]{:S(2)}) collective-permute-start(bf16[64,2048]{1,0:T(8,128)(2,1)} %get-tuple-element.38), channel_id=1, source_target_pairs={{0,3},{1,0},{2,1},{3,2},{4,7},{5,4},{6,5},{7,6},{8,11},{9,8},{10,9... | collective-permute-start | bytes 786440 | tf_op jit(solution)/shard_map/ppermute | solution.py:371
  105.9 0.7 copy-start.20
  110.7 0.7 copy-start.22
  111.4 1.0 copy-start.21
  112.4 0.9 copy-start.23
  114.9 0.7 copy-start.16
  115.6 0.7 copy-start.18
  116.3 7.7 %collective-permute-start.17 = (bf16[64,2048]{1,0:T(8,128)(2,1)S(1)}, bf16[64,2048]{1,0:T(8,128)(2,1)S(1)}, u32[]{:S(2)}, u32[]{:S(2)}) collective-permute-start(bf16[64,2048]{1,0:T(8,128)(2,1)S(1)} %get-tuple-element.39.c), channel_id=1, source_target_pairs={{0,1},{1,2},{2,3},{3,0},{4,5},{5,6},{6,7},{7,4},{8,9},{9,10},{10,1... | collective-permute-start | bytes 786440 | tf_op jit(solution)/shard_map/ppermute | solution.py:371
  116.7 7.3 %collective-permute-start.20 = (bf16[64,2048]{1,0:T(8,128)(2,1)S(1)}, bf16[64,2048]{1,0:T(8,128)(2,1)S(1)}, u32[]{:S(2)}, u32[]{:S(2)}) collective-permute-start(bf16[64,2048]{1,0:T(8,128)(2,1)S(1)} %get-tuple-element.40.d), channel_id=1, source_target_pairs={{0,3},{1,0},{2,1},{3,2},{4,7},{5,4},{6,5},{7,6},{8,11},{9,8},{10,9... | collective-permute-start | bytes 786440 | tf_op jit(solution)/shard_map/ppermute | solution.py:371
  119.0 9.5 %collective-permute-start.22 = (bf16[64,2048]{1,0:T(8,128)(2,1)S(1)}, bf16[64,2048]{1,0:T(8,128)(2,1)S(1)}, u32[]{:S(2)}, u32[]{:S(2)}) collective-permute-start(bf16[64,2048]{1,0:T(8,128)(2,1)S(1)} %get-tuple-element.39.c), channel_id=1, source_target_pairs={{0,3},{1,0},{2,1},{3,2},{4,7},{5,4},{6,5},{7,6},{8,11},{9,8},{10,9... | collective-permute-start | bytes 786440 | tf_op jit(solution)/shard_map/ppermute | solution.py:371
  124.0 6.9 %collective-permute-start.19 = (bf16[64,2048]{1,0:T(8,128)(2,1)S(1)}, bf16[64,2048]{1,0:T(8,128)(2,1)S(1)}, u32[]{:S(2)}, u32[]{:S(2)}) collective-permute-start(bf16[64,2048]{1,0:T(8,128)(2,1)S(1)} %collective-permute-done.17.a), channel_id=1, source_target_pairs={{0,1},{1,2},{2,3},{3,0},{4,5},{5,6},{6,7},{7,4},{8,9},{9,10},{10,1... | collective-permute-start | bytes 786440 | tf_op jit(solution)/shard_map/ppermute | solution.py:371
  124.0 10.1 %collective-permute-start.21 = (bf16[64,2048]{1,0:T(8,128)(2,1)S(1)}, bf16[64,2048]{1,0:T(8,128)(2,1)S(1)}, u32[]{:S(2)}, u32[]{:S(2)}) collective-permute-start(bf16[64,2048]{1,0:T(8,128)(2,1)S(1)} %collective-permute-done.20.d), channel_id=1, source_target_pairs={{0,3},{1,0},{2,1},{3,2},{4,7},{5,4},{6,5},{7,6},{8,11},{9,8},{10,9... | collective-permute-start | bytes 786440 | tf_op jit(solution)/shard_map/ppermute | solution.py:371
  126.7 34.0 %collective-permute-start.18 = (bf16[64,2048]{1,0:T(8,128)(2,1)S(1)}, bf16[64,2048]{1,0:T(8,128)(2,1)S(1)}, u32[]{:S(2)}, u32[]{:S(2)}) collective-permute-start(bf16[64,2048]{1,0:T(8,128)(2,1)S(1)} %get-tuple-element.40.d), channel_id=1, source_target_pairs={{0,1},{1,2},{2,3},{3,0},{4,5},{5,6},{6,7},{7,4},{8,9},{9,10},{10,1... | collective-permute-start | bytes 786440 | tf_op jit(solution)/shard_map/ppermute | solution.py:371
  128.5 0.7 copy-start.9
  130.9 0.7 copy-start.11
  134.1 0.7 copy-start.13
  139.9 0.9 copy-start.10
  140.9 0.9 copy-start.12
  141.8 0.9 copy-start.14
  157.8 20.7 %collective-permute-start.23 = (bf16[64,2048]{1,0:T(8,128)(2,1)S(1)}, bf16[64,2048]{1,0:T(8,128)(2,1)S(1)}, u32[]{:S(2)}, u32[]{:S(2)}) collective-permute-start(bf16[64,2048]{1,0:T(8,128)(2,1)S(1)} %get-tuple-element.43), channel_id=1, source_target_pairs={{0,1},{1,2},{2,3},{3,0},{4,5},{5,6},{6,7},{7,4},{8,9},{9,10},{10,1... | collective-permute-start | bytes 786440 | tf_op jit(solution)/shard_map/ppermute | solution.py:371
  158.0 20.5 %collective-permute-start.24 = (bf16[64,2048]{1,0:T(8,128)(2,1)S(1)}, bf16[64,2048]{1,0:T(8,128)(2,1)S(1)}, u32[]{:S(2)}, u32[]{:S(2)}) collective-permute-start(bf16[64,2048]{1,0:T(8,128)(2,1)S(1)} %get-tuple-element.45), channel_id=1, source_target_pairs={{0,3},{1,0},{2,1},{3,2},{4,7},{5,4},{6,5},{7,6},{8,11},{9,8},{10,9... | collective-permute-start | bytes 786440 | tf_op jit(solution)/shard_map/ppermute | solution.py:371
  160.6 28.0 %copy-start.17 = (bf16[64,2048]{1,0:T(8,128)(2,1)S(1)}, bf16[64,2048]{1,0:T(8,128)(2,1)}, u32[]{:S(2)}) copy-start(bf16[64,2048]{1,0:T(8,128)(2,1)} %copy-done.16) | copy-start | bytes 786436
  160.6 28.0 %copy-start.19 = (bf16[64,2048]{1,0:T(8,128)(2,1)S(1)}, bf16[64,2048]{1,0:T(8,128)(2,1)}, u32[]{:S(2)}) copy-start(bf16[64,2048]{1,0:T(8,128)(2,1)} %copy-done.18) | copy-start | bytes 786436
  160.6 20.9 %collective-permute-start.27 = (bf16[64,2048]{1,0:T(8,128)(2,1)S(1)}, bf16[64,2048]{1,0:T(8,128)(2,1)S(1)}, u32[]{:S(2)}, u32[]{:S(2)}) collective-permute-start(bf16[64,2048]{1,0:T(8,128)(2,1)S(1)} %get-tuple-element.50), channel_id=1, source_target_pairs={{0,1},{1,2},{2,3},{3,0},{4,5},{5,6},{6,7},{7,4},{8,9},{9,10},{10,1... | collective-permute-start | bytes 786440 | tf_op jit(solution)/shard_map/ppermute | solution.py:371
  175.8 7.2 %collective-permute-start.26 = (bf16[64,2048]{1,0:T(8,128)(2,1)S(1)}, bf16[64,2048]{1,0:T(8,128)(2,1)S(1)}, u32[]{:S(2)}, u32[]{:S(2)}) collective-permute-start(bf16[64,2048]{1,0:T(8,128)(2,1)S(1)} %get-tuple-element.47), channel_id=1, source_target_pairs={{0,3},{1,0},{2,1},{3,2},{4,7},{5,4},{6,5},{7,6},{8,11},{9,8},{10,9... | collective-permute-start | bytes 786440 | tf_op jit(solution)/shard_map/ppermute | solution.py:371
  178.8 7.8 %collective-permute-start.25 = (bf16[64,2048]{1,0:T(8,128)(2,1)S(1)}, bf16[64,2048]{1,0:T(8,128)(2,1)S(1)}, u32[]{:S(2)}, u32[]{:S(2)}) collective-permute-start(bf16[64,2048]{1,0:T(8,128)(2,1)S(1)} %get-tuple-element.46), channel_id=1, source_target_pairs={{0,1},{1,2},{2,3},{3,0},{4,5},{5,6},{6,7},{7,4},{8,9},{9,10},{10,1... | collective-permute-start | bytes 786440 | tf_op jit(solution)/shard_map/ppermute | solution.py:371
  178.9 9.8 %collective-permute-start.28 = (bf16[64,2048]{1,0:T(8,128)(2,1)S(1)}, bf16[64,2048]{1,0:T(8,128)(2,1)S(1)}, u32[]{:S(2)}, u32[]{:S(2)}) collective-permute-start(bf16[64,2048]{1,0:T(8,128)(2,1)S(1)} %get-tuple-element.51), channel_id=1, source_target_pairs={{0,3},{1,0},{2,1},{3,2},{4,7},{5,4},{6,5},{7,6},{8,11},{9,8},{10,9... | collective-permute-start | bytes 786440 | tf_op jit(solution)/shard_map/ppermute | solution.py:371
Sparse Core Ops, SparseCore 0:
  9.2 130.6 all-gather.1

commit v3 on v2

--- a/solution.py
+++ b/solution.py
@@ -23,44 +23,59 @@
     return pl.BlockSpec(memory_space=pltpu.SMEM)
 
 
-def whole(a):
-    return pl.BlockSpec(a.shape, lambda *_: (0,) * len(a.shape))
-
-
-def call(body, outs, *args, scratch=(), flops=0, moved=0, pull=False):
+class Far:
+    def __init__(self, x):
+        self.x = x
+
+
+def call(body, outs, *args, scratch=(), flops=0, moved=0, far_out=False, limit=48):
     many = isinstance(outs, (list, tuple))
     outs = list(outs) if many else [outs]
-    inner, pulled = body, []
-    if pull:
-        pulled = [n for n, a in enumerate(args) if a.dtype != jnp.int32]
-
-        def inner(*refs):
-            given = list(refs[: len(args)])
-            kept = refs[len(args) : len(refs) - len(pulled) - 1]
-            held, sems = refs[len(refs) - len(pulled) - 1 : -1], refs[-1]
-            copies = []
-            for k, n in enumerate(pulled):
-                copies.append(pltpu.make_async_copy(given[n], held[k], sems.at[k]))
-                copies[-1].start()
-                given[n] = held[k]
-            for copy in copies:
-                copy.wait()
-            body(*given, *kept)
-
-        far = pl.BlockSpec(memory_space=pltpu.HBM)
-        specs = [smem() if a.dtype == jnp.int32 else far for a in args]
-        scratch = list(scratch) + [pltpu.VMEM(args[n].shape, args[n].dtype) for n in pulled]
-        scratch.append(pltpu.SemaphoreType.DMA((len(pulled),)))
-    else:
-        specs = [smem() if a.dtype == jnp.int32 else vmem() for a in args]
+    pulled = [n for n, a in enumerate(args) if isinstance(a, Far)]
+    args = [
+        pltpu.with_memory_space_constraint(a.x, pltpu.HBM) if isinstance(a, Far) else a
+        for a in args
+    ]
+    pushed = list(range(len(outs))) if far_out else []
+    own = len(scratch)
+
+    def inner(*refs):
+        given, rest = list(refs[: len(args)]), list(refs[len(args) :])
+        results, rest = rest[: len(outs)], rest[len(outs) :]
+        kept, rest = rest[:own], rest[own:]
+        held, sent = rest[: len(pulled)], rest[len(pulled) : len(pulled) + len(pushed)]
+        sems = rest[-1]
+        copies = []
+        for k, n in enumerate(pulled):
+            copies.append(pltpu.make_async_copy(given[n], held[k], sems.at[k]))
+            copies[-1].start()
+            given[n] = held[k]
+        for copy in copies:
+            copy.wait()
+        body(*given, *(sent if pushed else results), *kept)
+        copies = []
+        for k in range(len(pushed)):
+            copies.append(pltpu.make_async_copy(sent[k], results[k], sems.at[len(pulled) + k]))
+            copies[-1].start()
+        for copy in copies:
+            copy.wait()
+
+    far = pl.BlockSpec(memory_space=pltpu.HBM)
+    specs = [
+        smem() if a.dtype == jnp.int32 else far if n in pulled else vmem()
+        for n, a in enumerate(args)
+    ]
+    buffers = [pltpu.VMEM(args[n].shape, args[n].dtype) for n in pulled]
+    buffers += [pltpu.VMEM(outs[n].shape, outs[n].dtype) for n in pushed]
     result = pl.pallas_call(
         inner,
-        grid=(1,) if pull else (),
-        out_shape=outs,
+        out_shape=[pltpu.HBM(o.shape, o.dtype) for o in outs] if far_out else outs,
         in_specs=specs,
-        out_specs=[whole(o) if pull else vmem() for o in outs],
-        scratch_shapes=list(scratch),
-        compiler_params=pltpu.CompilerParams(vmem_limit_bytes=48 * 2**20),
+        out_specs=[far if far_out else vmem() for _ in outs],
+        scratch_shapes=[
+            *scratch, *buffers, pltpu.SemaphoreType.DMA((max(len(pulled) + len(pushed), 1),))
+        ],
+        compiler_params=pltpu.CompilerParams(vmem_limit_bytes=limit * 2**20),
         cost_estimate=pl.CostEstimate(flops=flops, bytes_accessed=moved, transcendentals=0),
         name=body.__name__,
     )(*args)
@@ -298,62 +313,96 @@
         normed[...] = (values * lax.rsqrt(power + EPS) * gain[...]).astype(BF16)
 
 
-def hidden_rows(a, b, c, d, up, down, out_a, out_b, out_c, out_d, rows, hidden, sems):
-    step = pl.program_id(0)
-    size, block = a.shape[0], up.shape[1]
-    ups = hidden.shape[1] // block
-
-    @pl.when(step == 0)
-    def _():
-        copies = [
-            pltpu.make_async_copy(part, rows.at[pl.ds(n * size, size), :], sems.at[n])
-            for n, part in enumerate((a, b, c, d))
-        ]
-        for copy in copies:
-            copy.start()
-        for copy in copies:
-            copy.wait()
-
-    @pl.when(step < ups)
-    def _():
-        raised = jnp.maximum(mm(rows[...], up[...]), 0.0)
-        start = pl.multiple_of(step * block, block)
-        hidden[:, pl.ds(start, block)] = (raised * raised).astype(BF16)
-
-    @pl.when(step >= ups)
-    def _():
-        done = mm(hidden[...], down[...], ((1,), (1,))).astype(BF16)
-        for n, out in enumerate((out_a, out_b, out_c, out_d)):
-            out[...] = done[n * size : (n + 1) * size]
+def hidden_rows(
+    a, b, c, d, weights, out_a, out_b, out_c, out_d, rows, up, down, total, hidden,
+    done_rows, row_sems, up_sems, down_sems, out_sems,
+):
+    size, block, count = a.shape[0], up.shape[1], up.shape[0]
+    units = up.shape[2]
+    chunk = rows.shape[2]
+
+    def fetch_rows(n, part, k):
+        to = rows.at[k, pl.ds(n * size, size), :]
+        return pltpu.make_async_copy(part.at[:, pl.ds(k * chunk, chunk)], to, row_sems.at[n, k])
+
+    def fetch(k, column, to, sems):
+        start = pl.multiple_of(k * block, block)
+        source = weights.at[pl.ds(start, block), pl.ds(column * units, units)]
+        return pltpu.make_async_copy(source, to.at[k], sems.at[k])
+
+    parts = (a, b, c, d)
+    for n, part in enumerate(parts):
+        for k in range(rows.shape[0]):
+            fetch_rows(n, part, k).start()
+
+    @pl.loop(0, count)
+    def _(k):
+        fetch(k, 0, up, up_sems).start()
+
+    @pl.loop(0, count)
+    def _(k):
+        fetch(k, 1, down, down_sems).start()
+
+    for n, part in enumerate(parts):
+        for k in range(rows.shape[0]):
+            fetch_rows(n, part, k).wait()
+
+    total[...] = jnp.zeros_like(total)
+
+    @pl.loop(0, count)
+    def _(k):
+        fetch(k, 0, up, up_sems).wait()
+        total[...] += mm(rows[k], up[k])
+
+    raised = jnp.maximum(total[...], 0.0)
+    hidden[...] = (raised * raised).astype(BF16)
+
+    @pl.loop(0, count)
+    def _(k):
+        fetch(k, 1, down, down_sems).wait()
+        done = mm(hidden[...], down[k], ((1,), (1,))).astype(BF16)
+        start = pl.multiple_of(k * block, block)
+        for n in range(4):
+            done_rows[n, :, pl.ds(start, block)] = done[n * size : (n + 1) * size]
+
+    copies = []
+    for n, out in enumerate((out_a, out_b, out_c, out_d)):
+        copies.append(pltpu.make_async_copy(done_rows.at[n], out, out_sems.at[n]))
+        copies[-1].start()
+    for copy in copies:
+        copy.wait()
 
 
 def feed_forward(parts, weights):
     size, width = parts[0].shape
     units = weights.shape[1] // 2
     block = 256
-    ups, downs = units // block, width // block
-    put_out = pl.BlockSpec((size, block), lambda s: (0, jnp.maximum(s - ups, 0)))
+    count = width // block
+    far = pl.BlockSpec(memory_space=pltpu.HBM)
+    held = [pltpu.with_memory_space_constraint(p, pltpu.HBM) for p in (*parts, weights)]
     return pl.pallas_call(
         hidden_rows,
-        grid=(ups + downs,),
-        out_shape=[shaped((size, width), BF16)] * 4,
-        in_specs=[pl.BlockSpec(memory_space=pltpu.HBM) for _ in parts]
-        + [
-            pl.BlockSpec((width, block), lambda s: (0, jnp.minimum(s, ups - 1))),
-            pl.BlockSpec((block, units), lambda s: (jnp.maximum(s - ups, 0), 1)),
-        ],
-        out_specs=[put_out] * 4,
+        out_shape=[pltpu.HBM((size, width), BF16)] * 4,
+        in_specs=[far] * 5,
+        out_specs=[far] * 4,
         scratch_shapes=[
-            pltpu.VMEM((4 * size, width), BF16),
+            pltpu.VMEM((count, 4 * size, block), BF16),
+            pltpu.VMEM((count, block, units), BF16),
+            pltpu.VMEM((count, block, units), BF16),
+            pltpu.VMEM((4 * size, units), F32),
             pltpu.VMEM((4 * size, units), BF16),
+            pltpu.VMEM((4, size, width), BF16),
+            pltpu.SemaphoreType.DMA((4, count)),
+            pltpu.SemaphoreType.DMA((count,)),
+            pltpu.SemaphoreType.DMA((count,)),
             pltpu.SemaphoreType.DMA((4,)),
         ],
-        compiler_params=pltpu.CompilerParams(vmem_limit_bytes=48 * 2**20),
+        compiler_params=pltpu.CompilerParams(vmem_limit_bytes=40 * 2**20),
         cost_estimate=pl.CostEstimate(
             flops=16 * size * width * units, bytes_accessed=4 * units * width, transcendentals=0
         ),
         name="hidden_rows",
-    )(*parts, weights, weights)
+    )(*held)
 
 
 def last_sum(own_a, left_a, right_a, mid_a, own_b, left_b, right_b, mid_b, out):
@@ -386,7 +435,9 @@
 def reduced(far, right_a, right_b, left_a, left_b):
     came_right_b, came_left_a = turn(right_b, 1), turn(left_a, -1)
     like = [shaped(right_a.shape, BF16)] * 2
-    right_sum, left_sum = call(add_two, like, right_a, far[0], left_b, far[1], pull=True)
+    right_sum, left_sum = call(
+        add_two, like, Far(right_a), far[0], Far(left_b), far[1], far_out=True, limit=16
+    )
     return turn(right_sum, 1), came_right_b, came_left_a, turn(left_sum, -1)
 
 
@@ -421,15 +472,15 @@
     lanes = wide_value + 2 * LANES
     own = call(
         own_state, shaped((2, half, lanes), BF16),
-        key_wide, value_wide, decay_wide, key_narrow, value_narrow, decay_narrow,
-        flops=2 * length * wide_key * wide_value, moved=10**6, pull=True,
+        *map(Far, (key_wide, value_wide, decay_wide, key_narrow, value_narrow, decay_narrow)),
+        flops=2 * length * wide_key * wide_value, moved=10**6,
     )
     sibling = swap(own)
     within = call(
         inside, shaped((length, wide_value + thin_value), F32),
-        query_wide, key_wide, value_wide, decay_wide,
-        query_narrow, key_narrow, value_narrow, decay_narrow,
-        flops=6 * length * length * wide_value, moved=4 * 10**6, pull=True,
+        *map(Far, (query_wide, key_wide, value_wide, decay_wide)),
+        *map(Far, (query_narrow, key_narrow, value_narrow, decay_narrow)),
+        flops=6 * length * length * wide_value, moved=4 * 10**6,
     )
     rows = half // 4
     pieces = call(of_chip, shaped((4, rows, lanes), BF16), place, own, sibling)
@@ -450,16 +501,16 @@
     quarter = portion // 2
     far_a, far_b, right_a, right_b, left_a, left_b, own_a, own_b = call(
         heads_out, [shaped((quarter, width), BF16)] * 8,
-        place, own_half, other_half, sibling, query_wide, query_narrow,
-        decay_wide, decay_narrow, within, gain_wide[None], gain_narrow[None],
-        out_wide, out_narrow,
+        place, own_half, other_half, sibling,
+        *map(Far, (query_wide, query_narrow, decay_wide, decay_narrow)), within,
+        *map(Far, (gain_wide[None], gain_narrow[None], out_wide, out_narrow)),
         scratch=[
             pltpu.VMEM((wide_key, wide_value), BF16),
             pltpu.VMEM((key_narrow.shape[1], thin_value), BF16),
             pltpu.VMEM((length, wide_value), BF16),
             pltpu.VMEM((length, thin_value), BF16),
         ],
-        flops=4 * length * wide_value * width, moved=8 * 10**6, pull=True,
+        flops=4 * length * wide_value * width, moved=8 * 10**6, far_out=True,
     )
     from_left_a, from_left_b, from_right_a, from_right_b = reduced(
         sent_far(far_a, far_b), right_a, right_b, left_a, left_b
@@ -467,8 +518,8 @@
     own_stream = lax.dynamic_slice_in_dim(stream_in, member * portion, portion, 0)
     mid_a, mid_b, normed_a, normed_b = call(
         rows_mid, [shaped((quarter, width), BF16)] * 4,
-        own_a, from_left_a, from_right_a, own_b, from_left_b, from_right_b,
-        own_stream, mlp_gain[None], pull=True,
+        Far(own_a), from_left_a, from_right_a, Far(own_b), from_left_b, from_right_b,
+        Far(own_stream), Far(mlp_gain[None]), far_out=True, limit=16,
     )
     far_a, far_b, right_a, right_b, left_a, left_b = spread(normed_a, normed_b)
     far_a, far_b, right_a, right_b = feed_forward((far_a, far_b, right_a, right_b), weights)
@@ -479,7 +530,8 @@
     )
     return call(
         last_sum, shaped((portion, width), BF16),
-        own_a, from_left_a, from_right_a, mid_a, own_b, from_left_b, from_right_b, mid_b, pull=True,
+        Far(own_a), from_left_a, from_right_a, Far(mid_a),
+        Far(own_b), from_left_b, from_right_b, Far(mid_b), far_out=True, limit=16,
     )
 
 

time: 199 us -> 186 us (0.935)
  local copies, waits for them, and re-layouts: 15 us -> 1.59 us
  waiting for transfers between devices: 50.9 us -> 54.2 us
  Pallas kernels: 47.9 us -> 45.3 us
    unnamed x66 -> x12, local copies, waits for them, and re-layouts: 14.9 us -> 0.73 us
    all_gather x1, waiting for transfers between devices: 5.1 us -> 11.8 us  [on_device(): weights = lax.all_gather(both, SP, axis=0, tiled=True)]
    ppermute x27, waiting for transfers between devices: 44.3 us -> 41 us  [shift(): return lax.ppermute(x, axis, pairs)]
    pallas_call x13, Pallas kernels: 47.9 us -> 45.3 us  [the longest x11 24.1 us: call(): pl.pallas_call(inner, out_shape=[pltpu.HBM(o.shape, o.dtype) for o in out...]
  transfers between devices with their start and end apart: 30 -> 30, of which waited for: 19 -> 17; matrix products, arithmetic and copies ran while one was open for 0% -> 1% of each run, Pallas kernels for 24% -> 23%
where the time goes in v3:
time: 186 us; the launch traced here: 185 us
  starting transfers between devices  67.7 us (36%)
  waiting for transfers between devices  54.2 us (29%)
  Pallas kernels  45.3 us (24%)
  between operations  13.7 us (7%)
  other arithmetic  2.08 us (1%)
    ppermute x27, starting transfers between devices, shift(): return lax.ppermute(x, axis, pairs)  45.3 us
    ppermute x27, waiting for transfers between devices, shift(): return lax.ppermute(x, axis, pairs)  41 us
    pallas_call x11, Pallas kernels, call(): pl.pallas_call(inner, out_shape=[pltpu.HBM(o.shape, o.dtype) for o in out...  24.1 us
    ppermute x2, starting transfers between devices, swap(): return lax.ppermute(x, 'core', [(0, 1), (1, 0)])  22.4 us
    pallas_call x2, Pallas kernels, feed_forward(): pl.pallas_call(hidden_rows, out_shape=[pltpu.HBM((size, width), BF16)] *...  21.2 us
    all_gather x1, waiting for transfers between devices, on_device(): weights = lax.all_gather(both, SP, axis=0, tiled=True)  11.8 us
  transfers between devices with their start and end apart: 30, of which 17 were waited for; matrix products, arithmetic and copies ran while one was open for 1% of the time, Pallas kernels for 23%

profile of v3, /device:TPU:33, one launch (start us, length us, event | category | flops | bytes accessed | tf_op | source)
XLA Modules:
  0.0 184.6 jit_solution(5946346852239935810)
XLA Ops:
  6.6 2.0 %pad_maximum_fusion = bf16[64,4096]{1,0:T(8,128)(2,1)} fusion(bf16[64,2048]{1,0:T(8,128)(2,1)} %bitcast.23, bf16[64,2048]{1,0:T(8,128)(2,1)} %param.30), kind=kLoop, calls=%fused_computation | loop fusion | flops 1048576 | bytes 1048576 | tf_op jit(solution)/shard_map/concatenate | solution.py:466
  8.6 0.1 all-gather.2.cloned.1.call-update
  8.6 2.3 %own_state.1.refs_1_ = bf16[2,128,768]{2,1,0:T(8,128)(2,1)S(1)} custom-call(bf16[512,256]{1,0:T(8,128)(2,1)} %refs_1_.3, bf16[512,512]{1,0:T(8,128)(2,1)} %refs_2_.3, f32[1,512]{1,0:T(1,128)} %refs_6_.3, bf16[512,128]{1,0:T(8,128)(2,1)} %refs_5_.4, bf16[512,256]{1,0:T(8,128)(2,1)} %refs_6_.2, f32[1,512]{1,0:T(1,128)} %refs_7_.3), custom_call_target="tpu_custom_call" | custom-call | flops 134217728 | bytes 1000000 | tf_op jit(solution)/shard_map/own_state/pallas_call | solution.py:70
  10.9 20.5 %collective-permute-start = (bf16[2,128,768]{2,1,0:T(8,128)(2,1)S(1)}, bf16[2,128,768]{2,1,0:T(8,128)(2,1)S(1)}, u32[]{:S(2)}, u32[]{:S(2)}) collective-permute-start(bf16[2,128,768]{2,1,0:T(8,128)(2,1)S(1)} %own_state.1.refs_1_), channel_id=1, source_target_pairs={{0,4},{4,0},{1,5},{5,1},{2,6},{6,2},{3,7},{7,3},{8,12},{12,8},{9,1... | collective-permute-start | bytes 1179656 | tf_op jit(solution)/shard_map/ppermute | solution.py:424
  31.4 0.1 pad_add_fusion.refs_0_
  31.5 1.3 collective-permute-done.refs_2_.refs_3_
  32.8 0.9 of_chip.1
  33.7 0.1 collective-permute-start.1
  33.9 0.1 collective-permute-start.2
  34.0 3.1 %collective-permute-start.3 = (bf16[32,768]{1,0:T(8,128)(2,1)S(1)}, bf16[32,768]{1,0:T(8,128)(2,1)S(1)}, u32[]{:S(2)}, u32[]{:S(2)}) collective-permute-start(bf16[32,768]{1,0:T(8,128)(2,1)S(1)} %get-tuple-element.53), channel_id=1, source_target_pairs={{0,24},{8,0},{16,8},{24,16},{1,25},{9,1},{17,9},{25,17},{2,26},{10... | collective-permute-start | bytes 147464 | tf_op jit(solution)/shard_map/ppermute | solution.py:420
  37.1 1.5 collective-permute-done.1.refs_2_
  38.7 0.0 collective-permute-done.2.refs_3_
  38.7 1.1 collective-permute-done.3.refs_4_
  39.7 0.8 of_group.1
  40.5 1.3 collective-permute-start.4
  41.8 12.2 %collective-permute-start.5 = (bf16[1,32,768]{2,1,0:T(8,128)(2,1)S(1)}, bf16[1,32,768]{2,1,0:T(8,128)(2,1)S(1)}, u32[]{:S(2)}, u32[]{:S(2)}) collective-permute-start(bf16[1,32,768]{2,1,0:T(8,128)(2,1)S(1)} %of_group.1), channel_id=1, source_target_pairs={{0,64},{32,96},{1,65},{33,97},{2,66},{34,98},{3,67},{35,99},{4,68}... | collective-permute-start | bytes 147464 | tf_op jit(solution)/shard_map/ppermute | solution.py:420
  54.1 1.3 collective-permute-start.6
  55.4 0.0 collective-permute-done.4.refs_5_
  55.4 0.9 collective-permute-done.5.refs_6_
  56.2 6.5 %collective-permute-done.6.refs_7_ = bf16[1,32,768]{2,1,0:T(8,128)(2,1)S(1)} collective-permute-done((bf16[1,32,768]{2,1,0:T(8,128)(2,1)S(1)}, bf16[1,32,768]{2,1,0:T(8,128)(2,1)S(1)}, u32[]{:S(2)}, u32[]{:S(2)}) %collective-permute-start.6) | collective-permute-done | bytes 49184 | tf_op jit(solution)/shard_map/ppermute | solution.py:420
  62.7 0.8 before_each.1
  63.5 2.0 %collective-permute-start.7 = (bf16[32,640]{1,0:T(8,128)(2,1)S(1)}, bf16[32,640]{1,0:T(8,128)(2,1)S(1)}, u32[]{:S(2)}, u32[]{:S(2)}) collective-permute-start(bf16[32,640]{1,0:T(8,128)(2,1)S(1)} %get-tuple-element.59), channel_id=1, source_target_pairs={{0,8},{8,16},{16,24},{24,0},{1,9},{9,17},{17,25},{25,1},{2,10},{10... | collective-permute-start | bytes 122888 | tf_op jit(solution)/shard_map/ppermute | solution.py:420
  65.6 0.0 collective-permute-start.8
  65.6 2.2 %collective-permute-start.9 = (bf16[32,640]{1,0:T(8,128)(2,1)S(1)}, bf16[32,640]{1,0:T(8,128)(2,1)S(1)}, u32[]{:S(2)}, u32[]{:S(2)}) collective-permute-start(bf16[32,640]{1,0:T(8,128)(2,1)S(1)} %get-tuple-element.57), channel_id=1, source_target_pairs={{0,24},{8,0},{16,8},{24,16},{1,25},{9,1},{17,9},{25,17},{2,26},{10... | collective-permute-start | bytes 122888 | tf_op jit(solution)/shard_map/ppermute | solution.py:420
  67.8 1.5 collective-permute-done.7.refs_2_
  69.3 2.5 %collective-permute-done.8.refs_3_ = bf16[32,640]{1,0:T(8,128)(2,1)S(1)} collective-permute-done((bf16[32,640]{1,0:T(8,128)(2,1)S(1)}, bf16[32,640]{1,0:T(8,128)(2,1)S(1)}, u32[]{:S(2)}, u32[]{:S(2)}) %collective-permute-start.8) | collective-permute-done | bytes 40992 | tf_op jit(solution)/shard_map/ppermute | solution.py:420
  71.8 0.6 gathered_half.1.refs_1_
  72.4 1.9 %collective-permute-start.10 = (bf16[128,640]{1,0:T(8,128)(2,1)S(1)}, bf16[128,640]{1,0:T(8,128)(2,1)S(1)}, u32[]{:S(2)}, u32[]{:S(2)}) collective-permute-start(bf16[128,640]{1,0:T(8,128)(2,1)S(1)} %gathered_half.1.refs_1_), channel_id=1, source_target_pairs={{0,4},{4,0},{1,5},{5,1},{2,6},{6,2},{3,7},{7,3},{8,12},{12,8},{9,1... | collective-permute-start | bytes 491528 | tf_op jit(solution)/shard_map/ppermute | solution.py:424
  74.3 2.6 %inside.1.refs_8_ = f32[512,768]{1,0:T(8,128)S(1)} custom-call(bf16[512,256]{1,0:T(8,128)(2,1)} %refs_4_.5, bf16[512,256]{1,0:T(8,128)(2,1)} %refs_1_.3, bf16[512,512]{1,0:T(8,128)(2,1)} %refs_2_.3, f32[1,512]{1,0:T(1,128)} %refs_6_.3, bf16[512,128]{1,0:T(8,128)(2,1)} %refs_5_.5, bf16[512,128]{1,0:T(8,128)(2,1)} %refs_5_.4, bf16[512,256]{1,0:T(8,128)(2,1)} %refs_6_.2, ...), custom_call_target="tpu_custom_call" | custom-call | flops 805306368 | bytes 4000000 | tf_op jit(solution)/shard_map/inside/pallas_call | solution.py:70
  77.0 7.5 %heads_out.1 = (bf16[64,2048]{1,0:T(8,128)(2,1)}, bf16[64,2048]{1,0:T(8,128)(2,1)}, bf16[64,2048]{1,0:T(8,128)(2,1)}, bf16[64,2048]{1,0:T(8,128)(2,1)}, bf16[64,...) custom-call(s32[3]{0:T(128)S(1)} %pad_add_fusion.refs_0_, ...), custom_call_target="tpu_custom_call" | custom-call | flops 2147483648 | bytes 8000000 | tf_op jit(solution)/shard_map/heads_out/pallas_call | solution.py:70
  84.4 1.8 collective-permute-start.11
  86.2 1.7 collective-permute-start.12
  87.9 1.3 collective-permute-start.14
  89.3 0.1 collective-permute-start.15
  89.4 5.4 %collective-permute-done.11.refs_1_ = bf16[64,2048]{1,0:T(8,128)(2,1)S(1)} collective-permute-done((bf16[64,2048]{1,0:T(8,128)(2,1)}, bf16[64,2048]{1,0:T(8,128)(2,1)S(1)}, u32[]{:S(2)}, u32[]{:S(2)}) %collective-permute-start.11) | collective-permute-done | bytes 262176 | tf_op jit(solution)/shard_map/ppermute | solution.py:420
  94.8 1.9 %add_two.2 = (bf16[64,2048]{1,0:T(8,128)(2,1)}, bf16[64,2048]{1,0:T(8,128)(2,1)}) custom-call(bf16[64,2048]{1,0:T(8,128)(2,1)} %get-tuple-element.30.refs_0_, bf16[64,2048]{1,0:T(8,128)(2,1)S(1)} %collective-permute-done.11.refs_1_, bf16[64,2048]{1,0:T(8,128)(2,1)} %get-tuple-element.32.refs_2_, bf16[64,2048]{1,0:T(8,128)(2,1)S(1)} %collective-permute-done.12.refs_3_), custom_call_target="tpu_custom_call" | custom-call | tf_op jit(solution)/shard_map/add_two/pallas_call | solution.py:70
  96.7 0.8 collective-permute-start.13
  97.5 2.0 %collective-permute-start.16 = (bf16[64,2048]{1,0:T(8,128)(2,1)}, bf16[64,2048]{1,0:T(8,128)(2,1)S(1)}, u32[]{:S(2)}, u32[]{:S(2)}) collective-permute-start(bf16[64,2048]{1,0:T(8,128)(2,1)} %get-tuple-element.38), channel_id=1, source_target_pairs={{0,3},{1,0},{2,1},{3,2},{4,7},{5,4},{6,5},{7,6},{8,11},{9,8},{10,9... | collective-permute-start | bytes 786440 | tf_op jit(solution)/shard_map/ppermute | solution.py:420
  99.5 0.8 constant_dynamic-slice_fusion.refs_6_
  100.3 0.0 collective-permute-done.15.refs_4_
  100.4 4.6 %collective-permute-done.13.refs_1_ = bf16[64,2048]{1,0:T(8,128)(2,1)S(1)} collective-permute-done((bf16[64,2048]{1,0:T(8,128)(2,1)}, bf16[64,2048]{1,0:T(8,128)(2,1)S(1)}, u32[]{:S(2)}, u32[]{:S(2)}) %collective-permute-start.13) | collective-permute-done | bytes 262176 | tf_op jit(solution)/shard_map/ppermute | solution.py:420
  105.0 2.6 %rows_mid.1 = (bf16[64,2048]{1,0:T(8,128)(2,1)}, bf16[64,2048]{1,0:T(8,128)(2,1)}, bf16[64,2048]{1,0:T(8,128)(2,1)}, bf16[64,2048]{1,0:T(8,128)(2,1)}) custom-call(bf16[64,2048]{1,0:T(8,128)(2,1)} %get-tuple-element.29.refs_0_, bf16[64,2048]{1,0:T(8,128)(2,1)S(1)} %collective-permute-done.13.refs_1_, bf16[64,2048]{1,0:T(8,128)(2,1)S(1)} %collective-permute-done.14.refs_2_, ...), custom_call_target="tpu_custom_call" | custom-call | tf_op jit(solution)/shard_map/rows_mid/pallas_call | solution.py:70
  107.6 0.3 collective-permute-start.17
  107.9 2.5 %collective-permute-start.20 = (bf16[64,2048]{1,0:T(8,128)(2,1)}, bf16[64,2048]{1,0:T(8,128)(2,1)S(1)}, u32[]{:S(2)}, u32[]{:S(2)}) collective-permute-start(bf16[64,2048]{1,0:T(8,128)(2,1)} %get-tuple-element.40.d), channel_id=1, source_target_pairs={{0,3},{1,0},{2,1},{3,2},{4,7},{5,4},{6,5},{7,6},{8,11},{9,8},{10,9... | collective-permute-start | bytes 786440 | tf_op jit(solution)/shard_map/ppermute | solution.py:420
  110.4 1.3 collective-permute-start.22
  111.6 3.4 %collective-permute-done.17.a = bf16[64,2048]{1,0:T(8,128)(2,1)S(1)} collective-permute-done((bf16[64,2048]{1,0:T(8,128)(2,1)}, bf16[64,2048]{1,0:T(8,128)(2,1)S(1)}, u32[]{:S(2)}, u32[]{:S(2)}) %collective-permute-start.17) | collective-permute-done | bytes 262176 | tf_op jit(solution)/shard_map/ppermute | solution.py:420
  115.1 2.7 %collective-permute-start.21 = (bf16[64,2048]{1,0:T(8,128)(2,1)S(1)}, bf16[64,2048]{1,0:T(8,128)(2,1)}, u32[]{:S(2)}, u32[]{:S(2)}) collective-permute-start(bf16[64,2048]{1,0:T(8,128)(2,1)S(1)} %collective-permute-done.20.d), channel_id=1, source_target_pairs={{0,3},{1,0},{2,1},{3,2},{4,7},{5,4},{6,5},{7,6},{8,11},{9,8},{10,9... | collective-permute-start | bytes 786440 | tf_op jit(solution)/shard_map/ppermute | solution.py:420
  117.8 1.9 %collective-permute-done.22.c = bf16[64,2048]{1,0:T(8,128)(2,1)S(1)} collective-permute-done((bf16[64,2048]{1,0:T(8,128)(2,1)}, bf16[64,2048]{1,0:T(8,128)(2,1)S(1)}, u32[]{:S(2)}, u32[]{:S(2)}) %collective-permute-start.22) | collective-permute-done | bytes 262176 | tf_op jit(solution)/shard_map/ppermute | solution.py:420
  119.7 1.9 %collective-permute-done.19.a = bf16[64,2048]{1,0:T(8,128)(2,1)S(1)} collective-permute-done((bf16[64,2048]{1,0:T(8,128)(2,1)S(1)}, bf16[64,2048]{1,0:T(8,128)(2,1)S(1)}, u32[]{:S(2)}, u32[]{:S(2)}) %collective-permute-start.19) | collective-permute-done | bytes 262176 | tf_op jit(solution)/shard_map/ppermute | solution.py:420
  121.5 3.7 %collective-permute-done.21.b = bf16[64,2048]{1,0:T(8,128)(2,1)} collective-permute-done((bf16[64,2048]{1,0:T(8,128)(2,1)S(1)}, bf16[64,2048]{1,0:T(8,128)(2,1)}, u32[]{:S(2)}, u32[]{:S(2)}) %collective-permute-start.21) | collective-permute-done | bytes 262176 | tf_op jit(solution)/shard_map/ppermute | solution.py:420
  125.2 11.8 %all-gather.2.cloned.1.call-done.weights = bf16[2048,4096]{1,0:T(8,128)(2,1)} async-done(((bf16[64,4096]{1,0:T(8,128)(2,1)}), bf16[2048,4096]{1,0:T(8,128)(2,1)}) %all-gather.2.cloned.1.call-update) | async-done | bytes 16777232 | tf_op jit(solution)/shard_map/all_gather | solution.py:467
  137.1 10.6 %hidden_rows.3 = (bf16[64,2048]{1,0:T(8,128)(2,1)}, bf16[64,2048]{1,0:T(8,128)(2,1)}, bf16[64,2048]{1,0:T(8,128)(2,1)}, bf16[64,2048]{1,0:T(8,128)(2,1)}) custom-call(bf16[64,2048]{1,0:T(8,128)(2,1)} %copy-done.5, bf16[64,2048]{1,0:T(8,128)(2,1)} %collective-permute-done.21.b, bf16[64,2048]{1,0:T(8,128)(2,1)} %copy-done.4, bf16[64,2048]{1,0:T(8,128)(2,1)} %copy-done.3, ...), custom_call_target="tpu_custom_call" | custom-call | flops 4294967296 | bytes 16777216 | tf_op jit(solution)/shard_map/hidden_rows/pallas_call | solution.py:383
  147.7 1.0 collective-permute-start.23
  148.7 1.8 collective-permute-start.24
  150.5 0.7 copy-done.2
  151.2 10.6 %hidden_rows.2 = (bf16[64,2048]{1,0:T(8,128)(2,1)}, bf16[64,2048]{1,0:T(8,128)(2,1)}, bf16[64,2048]{1,0:T(8,128)(2,1)}, bf16[64,2048]{1,0:T(8,128)(2,1)}) custom-call(bf16[64,2048]{1,0:T(8,128)(2,1)} %copy-done.1, bf16[64,2048]{1,0:T(8,128)(2,1)} %copy-done.2, bf16[64,2048]{1,0:T(8,128)(2,1)} %get-tuple-element.39.c, bf16[64,2048]{1,0:T(8,128)(2,1)} %get-tuple-element.40.d, ...), custom_call_target="tpu_custom_call" | custom-call | flops 4294967296 | bytes 16777216 | tf_op jit(solution)/shard_map/hidden_rows/pallas_call | solution.py:383
  161.8 2.8 %collective-permute-start.26 = (bf16[64,2048]{1,0:T(8,128)(2,1)}, bf16[64,2048]{1,0:T(8,128)(2,1)S(1)}, u32[]{:S(2)}, u32[]{:S(2)}) collective-permute-start(bf16[64,2048]{1,0:T(8,128)(2,1)} %get-tuple-element.47), channel_id=1, source_target_pairs={{0,3},{1,0},{2,1},{3,2},{4,7},{5,4},{6,5},{7,6},{8,11},{9,8},{10,9... | collective-permute-start | bytes 786440 | tf_op jit(solution)/shard_map/ppermute | solution.py:420
  164.6 1.9 %add_two.3 = (bf16[64,2048]{1,0:T(8,128)(2,1)}, bf16[64,2048]{1,0:T(8,128)(2,1)}) custom-call(bf16[64,2048]{1,0:T(8,128)(2,1)} %get-tuple-element.42.refs_0_, bf16[64,2048]{1,0:T(8,128)(2,1)S(1)} %collective-permute-done.23.refs_1_, bf16[64,2048]{1,0:T(8,128)(2,1)} %get-tuple-element.44.refs_2_, bf16[64,2048]{1,0:T(8,128)(2,1)S(1)} %collective-permute-done.24.refs_3_), custom_call_target="tpu_custom_call" | custom-call | tf_op jit(solution)/shard_map/add_two/pallas_call | solution.py:70
  166.5 0.1 collective-permute-start.25
  166.7 2.7 %collective-permute-start.28 = (bf16[64,2048]{1,0:T(8,128)(2,1)}, bf16[64,2048]{1,0:T(8,128)(2,1)S(1)}, u32[]{:S(2)}, u32[]{:S(2)}) collective-permute-start(bf16[64,2048]{1,0:T(8,128)(2,1)} %get-tuple-element.51), channel_id=1, source_target_pairs={{0,3},{1,0},{2,1},{3,2},{4,7},{5,4},{6,5},{7,6},{8,11},{9,8},{10,9... | collective-permute-start | bytes 786440 | tf_op jit(solution)/shard_map/ppermute | solution.py:420
  169.3 0.1 collective-permute-done.26.refs_2_
  169.5 5.1 %collective-permute-done.25.refs_1_ = bf16[64,2048]{1,0:T(8,128)(2,1)S(1)} collective-permute-done((bf16[64,2048]{1,0:T(8,128)(2,1)}, bf16[64,2048]{1,0:T(8,128)(2,1)S(1)}, u32[]{:S(2)}, u32[]{:S(2)}) %collective-permute-start.25) | collective-permute-done | bytes 262176 | tf_op jit(solution)/shard_map/ppermute | solution.py:420
  174.5 0.9 collective-permute-done.28.refs_6_
  175.4 2.3 %last_sum.1 = bf16[128,2048]{1,0:T(8,128)(2,1)} custom-call(bf16[64,2048]{1,0:T(8,128)(2,1)} %get-tuple-element.41.refs_0_, bf16[64,2048]{1,0:T(8,128)(2,1)S(1)} %collective-permute-done.25.refs_1_, bf16[64,2048]{1,0:T(8,128)(2,1)S(1)} %collective-permute-done.26.refs_2_, bf16[64,2048]{1,0:T(8,128)(2,1)} %get-tuple-element.48.refs_3_, ...), custom_call_target="tpu_custom_call" | custom-call | tf_op jit(solution)/shard_map/last_sum/pallas_call | solution.py:70
  (27 shorter events, 0.1 us)
Async XLA Ops:
  6.5 93.0 %copy-start = (bf16[512,2048]{1,0:T(8,128)(2,1)S(1)}, bf16[512,2048]{1,0:T(8,128)(2,1)}, u32[]{:S(2)}) copy-start(bf16[512,2048]{1,0:T(8,128)(2,1)} %param.16) | copy-start | bytes 6291460
  6.6 130.5 %all-gather.2.cloned.1.call-start = ((), (), s32[]{:S(2)}) async-start(), calls=%async_computation | async-start | bytes 17301504 | tf_op jit(solution)/shard_map/all_gather | solution.py:467
  10.9 21.9 %collective-permute-start = (bf16[2,128,768]{2,1,0:T(8,128)(2,1)S(1)}, bf16[2,128,768]{2,1,0:T(8,128)(2,1)S(1)}, u32[]{:S(2)}, u32[]{:S(2)}) collective-permute-start(bf16[2,128,768]{2,1,0:T(8,128)(2,1)S(1)} %own_state.1.refs_1_), channel_id=1, source_target_pairs={{0,4},{4,0},{1,5},{5,1},{2,6},{6,2},{3,7},{7,3},{8,12},{12,8},{9,1... | collective-permute-start | bytes 1179656 | tf_op jit(solution)/shard_map/ppermute | solution.py:424
  33.7 4.9 %collective-permute-start.1 = (bf16[32,768]{1,0:T(8,128)(2,1)S(1)}, bf16[32,768]{1,0:T(8,128)(2,1)S(1)}, u32[]{:S(2)}, u32[]{:S(2)}) collective-permute-start(bf16[32,768]{1,0:T(8,128)(2,1)S(1)} %get-tuple-element.55), channel_id=1, source_target_pairs={{0,8},{8,16},{16,24},{24,0},{1,9},{9,17},{17,25},{25,1},{2,10},{10... | collective-permute-start | bytes 147464 | tf_op jit(solution)/shard_map/ppermute | solution.py:420
  33.9 4.8 %collective-permute-start.2 = (bf16[32,768]{1,0:T(8,128)(2,1)S(1)}, bf16[32,768]{1,0:T(8,128)(2,1)S(1)}, u32[]{:S(2)}, u32[]{:S(2)}) collective-permute-start(bf16[32,768]{1,0:T(8,128)(2,1)S(1)} %get-tuple-element.54), channel_id=1, source_target_pairs={{0,16},{8,24},{16,0},{24,8},{1,17},{9,25},{17,1},{25,9},{2,18},{10... | collective-permute-start | bytes 147464 | tf_op jit(solution)/shard_map/ppermute | solution.py:420
  34.0 5.7 %collective-permute-start.3 = (bf16[32,768]{1,0:T(8,128)(2,1)S(1)}, bf16[32,768]{1,0:T(8,128)(2,1)S(1)}, u32[]{:S(2)}, u32[]{:S(2)}) collective-permute-start(bf16[32,768]{1,0:T(8,128)(2,1)S(1)} %get-tuple-element.53), channel_id=1, source_target_pairs={{0,24},{8,0},{16,8},{24,16},{1,25},{9,1},{17,9},{25,17},{2,26},{10... | collective-permute-start | bytes 147464 | tf_op jit(solution)/shard_map/ppermute | solution.py:420
  40.5 14.9 %collective-permute-start.4 = (bf16[1,32,768]{2,1,0:T(8,128)(2,1)S(1)}, bf16[1,32,768]{2,1,0:T(8,128)(2,1)S(1)}, u32[]{:S(2)}, u32[]{:S(2)}) collective-permute-start(bf16[1,32,768]{2,1,0:T(8,128)(2,1)S(1)} %of_group.1), channel_id=1, source_target_pairs={{0,32},{32,64},{64,96},{1,33},{33,65},{65,97},{2,34},{34,66},{66,9... | collective-permute-start | bytes 147464 | tf_op jit(solution)/shard_map/ppermute | solution.py:420
  41.8 14.4 %collective-permute-start.5 = (bf16[1,32,768]{2,1,0:T(8,128)(2,1)S(1)}, bf16[1,32,768]{2,1,0:T(8,128)(2,1)S(1)}, u32[]{:S(2)}, u32[]{:S(2)}) collective-permute-start(bf16[1,32,768]{2,1,0:T(8,128)(2,1)S(1)} %of_group.1), channel_id=1, source_target_pairs={{0,64},{32,96},{1,65},{33,97},{2,66},{34,98},{3,67},{35,99},{4,68}... | collective-permute-start | bytes 147464 | tf_op jit(solution)/shard_map/ppermute | solution.py:420
  54.1 8.7 %collective-permute-start.6 = (bf16[1,32,768]{2,1,0:T(8,128)(2,1)S(1)}, bf16[1,32,768]{2,1,0:T(8,128)(2,1)S(1)}, u32[]{:S(2)}, u32[]{:S(2)}) collective-permute-start(bf16[1,32,768]{2,1,0:T(8,128)(2,1)S(1)} %of_group.1), channel_id=1, source_target_pairs={{0,96},{1,97},{2,98},{3,99},{4,100},{5,101},{6,102},{7,103},{8,104... | collective-permute-start | bytes 147464 | tf_op jit(solution)/shard_map/ppermute | solution.py:420
  63.5 5.8 %collective-permute-start.7 = (bf16[32,640]{1,0:T(8,128)(2,1)S(1)}, bf16[32,640]{1,0:T(8,128)(2,1)S(1)}, u32[]{:S(2)}, u32[]{:S(2)}) collective-permute-start(bf16[32,640]{1,0:T(8,128)(2,1)S(1)} %get-tuple-element.59), channel_id=1, source_target_pairs={{0,8},{8,16},{16,24},{24,0},{1,9},{9,17},{17,25},{25,1},{2,10},{10... | collective-permute-start | bytes 122888 | tf_op jit(solution)/shard_map/ppermute | solution.py:420
  65.6 6.3 %collective-permute-start.8 = (bf16[32,640]{1,0:T(8,128)(2,1)S(1)}, bf16[32,640]{1,0:T(8,128)(2,1)S(1)}, u32[]{:S(2)}, u32[]{:S(2)}) collective-permute-start(bf16[32,640]{1,0:T(8,128)(2,1)S(1)} %get-tuple-element.58), channel_id=1, source_target_pairs={{0,16},{8,24},{16,0},{24,8},{1,17},{9,25},{17,1},{25,9},{2,18},{10... | collective-permute-start | bytes 122888 | tf_op jit(solution)/shard_map/ppermute | solution.py:420
  65.6 6.3 %collective-permute-start.9 = (bf16[32,640]{1,0:T(8,128)(2,1)S(1)}, bf16[32,640]{1,0:T(8,128)(2,1)S(1)}, u32[]{:S(2)}, u32[]{:S(2)}) collective-permute-start(bf16[32,640]{1,0:T(8,128)(2,1)S(1)} %get-tuple-element.57), channel_id=1, source_target_pairs={{0,24},{8,0},{16,8},{24,16},{1,25},{9,1},{17,9},{25,17},{2,26},{10... | collective-permute-start | bytes 122888 | tf_op jit(solution)/shard_map/ppermute | solution.py:420
  72.4 4.5 %collective-permute-start.10 = (bf16[128,640]{1,0:T(8,128)(2,1)S(1)}, bf16[128,640]{1,0:T(8,128)(2,1)S(1)}, u32[]{:S(2)}, u32[]{:S(2)}) collective-permute-start(bf16[128,640]{1,0:T(8,128)(2,1)S(1)} %gathered_half.1.refs_1_), channel_id=1, source_target_pairs={{0,4},{4,0},{1,5},{5,1},{2,6},{6,2},{3,7},{7,3},{8,12},{12,8},{9,1... | collective-permute-start | bytes 491528 | tf_op jit(solution)/shard_map/ppermute | solution.py:424
  84.4 10.3 %collective-permute-start.11 = (bf16[64,2048]{1,0:T(8,128)(2,1)}, bf16[64,2048]{1,0:T(8,128)(2,1)S(1)}, u32[]{:S(2)}, u32[]{:S(2)}) collective-permute-start(bf16[64,2048]{1,0:T(8,128)(2,1)} %get-tuple-element.31), channel_id=1, source_target_pairs={{0,1},{1,2},{2,3},{3,0},{4,5},{5,6},{6,7},{7,4},{8,9},{9,10},{10,1... | collective-permute-start | bytes 786440 | tf_op jit(solution)/shard_map/ppermute | solution.py:420
  86.2 8.5 %collective-permute-start.12 = (bf16[64,2048]{1,0:T(8,128)(2,1)}, bf16[64,2048]{1,0:T(8,128)(2,1)S(1)}, u32[]{:S(2)}, u32[]{:S(2)}) collective-permute-start(bf16[64,2048]{1,0:T(8,128)(2,1)} %get-tuple-element.33), channel_id=1, source_target_pairs={{0,3},{1,0},{2,1},{3,2},{4,7},{5,4},{6,5},{7,6},{8,11},{9,8},{10,9... | collective-permute-start | bytes 786440 | tf_op jit(solution)/shard_map/ppermute | solution.py:420
  87.9 12.4 %collective-permute-start.14 = (bf16[64,2048]{1,0:T(8,128)(2,1)}, bf16[64,2048]{1,0:T(8,128)(2,1)S(1)}, u32[]{:S(2)}, u32[]{:S(2)}) collective-permute-start(bf16[64,2048]{1,0:T(8,128)(2,1)} %get-tuple-element.35), channel_id=1, source_target_pairs={{0,3},{1,0},{2,1},{3,2},{4,7},{5,4},{6,5},{7,6},{8,11},{9,8},{10,9... | collective-permute-start | bytes 786440 | tf_op jit(solution)/shard_map/ppermute | solution.py:420
  89.3 11.1 %collective-permute-start.15 = (bf16[64,2048]{1,0:T(8,128)(2,1)}, bf16[64,2048]{1,0:T(8,128)(2,1)S(1)}, u32[]{:S(2)}, u32[]{:S(2)}) collective-permute-start(bf16[64,2048]{1,0:T(8,128)(2,1)} %get-tuple-element.37), channel_id=1, source_target_pairs={{0,1},{1,2},{2,3},{3,0},{4,5},{5,6},{6,7},{7,4},{8,9},{9,10},{10,1... | collective-permute-start | bytes 786440 | tf_op jit(solution)/shard_map/ppermute | solution.py:420
  96.7 8.3 %collective-permute-start.13 = (bf16[64,2048]{1,0:T(8,128)(2,1)}, bf16[64,2048]{1,0:T(8,128)(2,1)S(1)}, u32[]{:S(2)}, u32[]{:S(2)}) collective-permute-start(bf16[64,2048]{1,0:T(8,128)(2,1)} %get-tuple-element.34), channel_id=1, source_target_pairs={{0,1},{1,2},{2,3},{3,0},{4,5},{5,6},{6,7},{7,4},{8,9},{9,10},{10,1... | collective-permute-start | bytes 786440 | tf_op jit(solution)/shard_map/ppermute | solution.py:420
  97.5 7.5 %collective-permute-start.16 = (bf16[64,2048]{1,0:T(8,128)(2,1)}, bf16[64,2048]{1,0:T(8,128)(2,1)S(1)}, u32[]{:S(2)}, u32[]{:S(2)}) collective-permute-start(bf16[64,2048]{1,0:T(8,128)(2,1)} %get-tuple-element.38), channel_id=1, source_target_pairs={{0,3},{1,0},{2,1},{3,2},{4,7},{5,4},{6,5},{7,6},{8,11},{9,8},{10,9... | collective-permute-start | bytes 786440 | tf_op jit(solution)/shard_map/ppermute | solution.py:420
  107.6 7.5 %collective-permute-start.17 = (bf16[64,2048]{1,0:T(8,128)(2,1)}, bf16[64,2048]{1,0:T(8,128)(2,1)S(1)}, u32[]{:S(2)}, u32[]{:S(2)}) collective-permute-start(bf16[64,2048]{1,0:T(8,128)(2,1)} %get-tuple-element.39.c), channel_id=1, source_target_pairs={{0,1},{1,2},{2,3},{3,0},{4,5},{5,6},{6,7},{7,4},{8,9},{9,10},{10,1... | collective-permute-start | bytes 786440 | tf_op jit(solution)/shard_map/ppermute | solution.py:420
  107.9 7.2 %collective-permute-start.20 = (bf16[64,2048]{1,0:T(8,128)(2,1)}, bf16[64,2048]{1,0:T(8,128)(2,1)S(1)}, u32[]{:S(2)}, u32[]{:S(2)}) collective-permute-start(bf16[64,2048]{1,0:T(8,128)(2,1)} %get-tuple-element.40.d), channel_id=1, source_target_pairs={{0,3},{1,0},{2,1},{3,2},{4,7},{5,4},{6,5},{7,6},{8,11},{9,8},{10,9... | collective-permute-start | bytes 786440 | tf_op jit(solution)/shard_map/ppermute | solution.py:420
  110.4 9.3 %collective-permute-start.22 = (bf16[64,2048]{1,0:T(8,128)(2,1)}, bf16[64,2048]{1,0:T(8,128)(2,1)S(1)}, u32[]{:S(2)}, u32[]{:S(2)}) collective-permute-start(bf16[64,2048]{1,0:T(8,128)(2,1)} %get-tuple-element.39.c), channel_id=1, source_target_pairs={{0,3},{1,0},{2,1},{3,2},{4,7},{5,4},{6,5},{7,6},{8,11},{9,8},{10,9... | collective-permute-start | bytes 786440 | tf_op jit(solution)/shard_map/ppermute | solution.py:420
  115.1 32.6 %copy-start.1 = (bf16[64,2048]{1,0:T(8,128)(2,1)}, bf16[64,2048]{1,0:T(8,128)(2,1)S(1)}, u32[]{:S(2)}) copy-start(bf16[64,2048]{1,0:T(8,128)(2,1)S(1)} %collective-permute-done.17.a) | copy-start | bytes 786436
  115.1 6.5 %collective-permute-start.19 = (bf16[64,2048]{1,0:T(8,128)(2,1)S(1)}, bf16[64,2048]{1,0:T(8,128)(2,1)S(1)}, u32[]{:S(2)}, u32[]{:S(2)}) collective-permute-start(bf16[64,2048]{1,0:T(8,128)(2,1)S(1)} %collective-permute-done.17.a), channel_id=1, source_target_pairs={{0,1},{1,2},{2,3},{3,0},{4,5},{5,6},{6,7},{7,4},{8,9},{9,10},{10,1... | collective-permute-start | bytes 786440 | tf_op jit(solution)/shard_map/ppermute | solution.py:420
  115.1 22.0 %copy-start.3 = (bf16[64,2048]{1,0:T(8,128)(2,1)}, bf16[64,2048]{1,0:T(8,128)(2,1)S(1)}, u32[]{:S(2)}) copy-start(bf16[64,2048]{1,0:T(8,128)(2,1)S(1)} %collective-permute-done.20.d) | copy-start | bytes 786436
  115.1 10.1 %collective-permute-start.21 = (bf16[64,2048]{1,0:T(8,128)(2,1)S(1)}, bf16[64,2048]{1,0:T(8,128)(2,1)}, u32[]{:S(2)}, u32[]{:S(2)}) collective-permute-start(bf16[64,2048]{1,0:T(8,128)(2,1)S(1)} %collective-permute-done.20.d), channel_id=1, source_target_pairs={{0,3},{1,0},{2,1},{3,2},{4,7},{5,4},{6,5},{7,6},{8,11},{9,8},{10,9... | collective-permute-start | bytes 786440 | tf_op jit(solution)/shard_map/ppermute | solution.py:420
  117.8 32.7 %collective-permute-start.18 = (bf16[64,2048]{1,0:T(8,128)(2,1)}, bf16[64,2048]{1,0:T(8,128)(2,1)S(1)}, u32[]{:S(2)}, u32[]{:S(2)}) collective-permute-start(bf16[64,2048]{1,0:T(8,128)(2,1)} %get-tuple-element.40.d), channel_id=1, source_target_pairs={{0,1},{1,2},{2,3},{3,0},{4,5},{5,6},{6,7},{7,4},{8,9},{9,10},{10,1... | collective-permute-start | bytes 786440 | tf_op jit(solution)/shard_map/ppermute | solution.py:420
  119.7 17.4 %copy-start.4 = (bf16[64,2048]{1,0:T(8,128)(2,1)}, bf16[64,2048]{1,0:T(8,128)(2,1)S(1)}, u32[]{:S(2)}) copy-start(bf16[64,2048]{1,0:T(8,128)(2,1)S(1)} %collective-permute-done.22.c) | copy-start | bytes 786436
  121.5 15.5 %copy-start.5 = (bf16[64,2048]{1,0:T(8,128)(2,1)}, bf16[64,2048]{1,0:T(8,128)(2,1)S(1)}, u32[]{:S(2)}) copy-start(bf16[64,2048]{1,0:T(8,128)(2,1)S(1)} %collective-permute-done.19.a) | copy-start | bytes 786436
  147.7 16.9 %collective-permute-start.23 = (bf16[64,2048]{1,0:T(8,128)(2,1)}, bf16[64,2048]{1,0:T(8,128)(2,1)S(1)}, u32[]{:S(2)}, u32[]{:S(2)}) collective-permute-start(bf16[64,2048]{1,0:T(8,128)(2,1)} %get-tuple-element.43), channel_id=1, source_target_pairs={{0,1},{1,2},{2,3},{3,0},{4,5},{5,6},{6,7},{7,4},{8,9},{9,10},{10,1... | collective-permute-start | bytes 786440 | tf_op jit(solution)/shard_map/ppermute | solution.py:420
  148.7 15.9 %collective-permute-start.24 = (bf16[64,2048]{1,0:T(8,128)(2,1)}, bf16[64,2048]{1,0:T(8,128)(2,1)S(1)}, u32[]{:S(2)}, u32[]{:S(2)}) collective-permute-start(bf16[64,2048]{1,0:T(8,128)(2,1)} %get-tuple-element.45), channel_id=1, source_target_pairs={{0,3},{1,0},{2,1},{3,2},{4,7},{5,4},{6,5},{7,6},{8,11},{9,8},{10,9... | collective-permute-start | bytes 786440 | tf_op jit(solution)/shard_map/ppermute | solution.py:420
  150.5 18.9 %collective-permute-start.27 = (bf16[64,2048]{1,0:T(8,128)(2,1)}, bf16[64,2048]{1,0:T(8,128)(2,1)S(1)}, u32[]{:S(2)}, u32[]{:S(2)}) collective-permute-start(bf16[64,2048]{1,0:T(8,128)(2,1)} %get-tuple-element.50), channel_id=1, source_target_pairs={{0,1},{1,2},{2,3},{3,0},{4,5},{5,6},{6,7},{7,4},{8,9},{9,10},{10,1... | collective-permute-start | bytes 786440 | tf_op jit(solution)/shard_map/ppermute | solution.py:420
  150.5 0.7 copy-start.2
  161.8 7.6 %collective-permute-start.26 = (bf16[64,2048]{1,0:T(8,128)(2,1)}, bf16[64,2048]{1,0:T(8,128)(2,1)S(1)}, u32[]{:S(2)}, u32[]{:S(2)}) collective-permute-start(bf16[64,2048]{1,0:T(8,128)(2,1)} %get-tuple-element.47), channel_id=1, source_target_pairs={{0,3},{1,0},{2,1},{3,2},{4,7},{5,4},{6,5},{7,6},{8,11},{9,8},{10,9... | collective-permute-start | bytes 786440 | tf_op jit(solution)/shard_map/ppermute | solution.py:420
  166.5 8.0 %collective-permute-start.25 = (bf16[64,2048]{1,0:T(8,128)(2,1)}, bf16[64,2048]{1,0:T(8,128)(2,1)S(1)}, u32[]{:S(2)}, u32[]{:S(2)}) collective-permute-start(bf16[64,2048]{1,0:T(8,128)(2,1)} %get-tuple-element.46), channel_id=1, source_target_pairs={{0,1},{1,2},{2,3},{3,0},{4,5},{5,6},{6,7},{7,4},{8,9},{9,10},{10,1... | collective-permute-start | bytes 786440 | tf_op jit(solution)/shard_map/ppermute | solution.py:420
  166.7 8.7 %collective-permute-start.28 = (bf16[64,2048]{1,0:T(8,128)(2,1)}, bf16[64,2048]{1,0:T(8,128)(2,1)S(1)}, u32[]{:S(2)}, u32[]{:S(2)}) collective-permute-start(bf16[64,2048]{1,0:T(8,128)(2,1)} %get-tuple-element.51), channel_id=1, source_target_pairs={{0,3},{1,0},{2,1},{3,2},{4,7},{5,4},{6,5},{7,6},{8,11},{9,8},{10,9... | collective-permute-start | bytes 786440 | tf_op jit(solution)/shard_map/ppermute | solution.py:420
Sparse Core Ops, SparseCore 0:
  9.2 127.8 all-gather.1

commit v4 on v3

--- a/solution.py
+++ b/solution.py
@@ -313,27 +313,25 @@
         normed[...] = (values * lax.rsqrt(power + EPS) * gain[...]).astype(BF16)
 
 
-def hidden_rows(
-    a, b, c, d, weights, out_a, out_b, out_c, out_d, rows, up, down, total, hidden,
-    done_rows, row_sems, up_sems, down_sems, out_sems,
-):
-    size, block, count = a.shape[0], up.shape[1], up.shape[0]
-    units = up.shape[2]
-    chunk = rows.shape[2]
-
-    def fetch_rows(n, part, k):
+def hidden_rows(*refs):
+    *ends, rows, up, down, total, hidden, done_rows, row_sems, up_sems, down_sems, out_sems = refs
+    number = len(ends) // 2
+    parts, weights, outs = ends[:number], ends[number], ends[number + 1 :]
+    count, block, units = up.shape
+    size = parts[0].shape[0]
+
+    def fetch_rows(n, k):
         to = rows.at[k, pl.ds(n * size, size), :]
-        return pltpu.make_async_copy(part.at[:, pl.ds(k * chunk, chunk)], to, row_sems.at[n, k])
+        return pltpu.make_async_copy(parts[n].at[:, pl.ds(k * block, block)], to, row_sems.at[n, k])
 
     def fetch(k, column, to, sems):
         start = pl.multiple_of(k * block, block)
         source = weights.at[pl.ds(start, block), pl.ds(column * units, units)]
         return pltpu.make_async_copy(source, to.at[k], sems.at[k])
 
-    parts = (a, b, c, d)
-    for n, part in enumerate(parts):
-        for k in range(rows.shape[0]):
-            fetch_rows(n, part, k).start()
+    pairs = [(n, k) for k in range(count) for n in range(number)]
+    for pair in pairs:
+        fetch_rows(*pair).start()
 
     @pl.loop(0, count)
     def _(k):
@@ -343,9 +341,8 @@
     def _(k):
         fetch(k, 1, down, down_sems).start()
 
-    for n, part in enumerate(parts):
-        for k in range(rows.shape[0]):
-            fetch_rows(n, part, k).wait()
+    for pair in pairs:
+        fetch_rows(*pair).wait()
 
     total[...] = jnp.zeros_like(total)
 
@@ -360,14 +357,14 @@
     @pl.loop(0, count)
     def _(k):
         fetch(k, 1, down, down_sems).wait()
+        start = pl.multiple_of(k * block, block)
         done = mm(hidden[...], down[k], ((1,), (1,))).astype(BF16)
-        start = pl.multiple_of(k * block, block)
-        for n in range(4):
-            done_rows[n, :, pl.ds(start, block)] = done[n * size : (n + 1) * size]
+        done_rows[:, pl.ds(start, block)] = done
 
     copies = []
-    for n, out in enumerate((out_a, out_b, out_c, out_d)):
-        copies.append(pltpu.make_async_copy(done_rows.at[n], out, out_sems.at[n]))
+    for n, out in enumerate(outs):
+        source = done_rows.at[pl.ds(n * size, size), :]
+        copies.append(pltpu.make_async_copy(source, out, out_sems.at[n]))
         copies[-1].start()
     for copy in copies:
         copy.wait()
@@ -376,30 +373,30 @@
 def feed_forward(parts, weights):
     size, width = parts[0].shape
     units = weights.shape[1] // 2
-    block = 256
-    count = width // block
+    number, block = len(parts), 512
+    count, total = width // block, number * size
     far = pl.BlockSpec(memory_space=pltpu.HBM)
     held = [pltpu.with_memory_space_constraint(p, pltpu.HBM) for p in (*parts, weights)]
     return pl.pallas_call(
         hidden_rows,
-        out_shape=[pltpu.HBM((size, width), BF16)] * 4,
-        in_specs=[far] * 5,
-        out_specs=[far] * 4,
+        out_shape=[pltpu.HBM((size, width), BF16)] * number,
+        in_specs=[far] * (number + 1),
+        out_specs=[far] * number,
         scratch_shapes=[
-            pltpu.VMEM((count, 4 * size, block), BF16),
+            pltpu.VMEM((count, total, block), BF16),
             pltpu.VMEM((count, block, units), BF16),
             pltpu.VMEM((count, block, units), BF16),
-            pltpu.VMEM((4 * size, units), F32),
-            pltpu.VMEM((4 * size, units), BF16),
-            pltpu.VMEM((4, size, width), BF16),
-            pltpu.SemaphoreType.DMA((4, count)),
+            pltpu.VMEM((total, units), F32),
+            pltpu.VMEM((total, units), BF16),
+            pltpu.VMEM((total, width), BF16),
+            pltpu.SemaphoreType.DMA((number, count)),
             pltpu.SemaphoreType.DMA((count,)),
             pltpu.SemaphoreType.DMA((count,)),
-            pltpu.SemaphoreType.DMA((4,)),
+            pltpu.SemaphoreType.DMA((number,)),
         ],
-        compiler_params=pltpu.CompilerParams(vmem_limit_bytes=40 * 2**20),
+        compiler_params=pltpu.CompilerParams(vmem_limit_bytes=44 * 2**20),
         cost_estimate=pl.CostEstimate(
-            flops=16 * size * width * units, bytes_accessed=4 * units * width, transcendentals=0
+            flops=4 * total * width * units, bytes_accessed=4 * units * width, transcendentals=0
         ),
         name="hidden_rows",
     )(*held)
@@ -428,17 +425,15 @@
     return shift(x, "tp", by, lax.axis_size("tp"))
 
 
-def sent_far(far_a, far_b):
-    return turn(far_a, 1), turn(far_b, -1)
-
-
-def reduced(far, right_a, right_b, left_a, left_b):
+def reduced(far_a, far_b, right_a, right_b, left_a, left_b):
+    came_far = turn(far_a, 1), turn(far_b, -1)
     came_right_b, came_left_a = turn(right_b, 1), turn(left_a, -1)
     like = [shaped(right_a.shape, BF16)] * 2
     right_sum, left_sum = call(
-        add_two, like, Far(right_a), far[0], Far(left_b), far[1], far_out=True, limit=16
-    )
-    return turn(right_sum, 1), came_right_b, came_left_a, turn(left_sum, -1)
+        add_two, like, Far(right_a), came_far[0], Far(left_b), came_far[1], far_out=True, limit=16
+    )
+    came = turn(right_sum, 1), came_right_b, came_left_a, turn(left_sum, -1)
+    return came, right_sum
 
 
 def spread(a, b):
@@ -512,22 +507,19 @@
         ],
         flops=4 * length * wide_value * width, moved=8 * 10**6, far_out=True,
     )
-    from_left_a, from_left_b, from_right_a, from_right_b = reduced(
-        sent_far(far_a, far_b), right_a, right_b, left_a, left_b
-    )
+    came, _ = reduced(far_a, far_b, right_a, right_b, left_a, left_b)
+    from_left_a, from_left_b, from_right_a, from_right_b = came
     own_stream = lax.dynamic_slice_in_dim(stream_in, member * portion, portion, 0)
     mid_a, mid_b, normed_a, normed_b = call(
         rows_mid, [shaped((quarter, width), BF16)] * 4,
         Far(own_a), from_left_a, from_right_a, Far(own_b), from_left_b, from_right_b,
         Far(own_stream), Far(mlp_gain[None]), far_out=True, limit=16,
     )
-    far_a, far_b, right_a, right_b, left_a, left_b = spread(normed_a, normed_b)
-    far_a, far_b, right_a, right_b = feed_forward((far_a, far_b, right_a, right_b), weights)
-    far = sent_far(far_a, far_b)
-    left_a, left_b, own_a, own_b = feed_forward((left_a, left_b, normed_a, normed_b), weights)
-    from_left_a, from_left_b, from_right_a, from_right_b = reduced(
-        far, right_a, right_b, left_a, left_b
-    )
+    others = feed_forward(spread(normed_a, normed_b), weights)
+    came, sent = reduced(*others)
+    from_left_a, from_left_b, from_right_a, from_right_b = came
+    normed_a, normed_b, _ = lax.optimization_barrier((normed_a, normed_b, sent))
+    own_a, own_b = feed_forward((normed_a, normed_b), weights)
     return call(
         last_sum, shaped((portion, width), BF16),
         Far(own_a), from_left_a, from_right_a, Far(mid_a),

time: 186 us -> 182 us (0.978)
  transfers between devices with their start and end apart: 30 -> 30, of which waited for: 17 -> 15; matrix products, arithmetic and copies ran while one was open for 1% -> 1% of each run, Pallas kernels for 23% -> 17%
where the time goes in v4:
time: 182 us; the launch traced here: 181 us
  starting transfers between devices  66.8 us (37%)
  waiting for transfers between devices  52.8 us (29%)
  Pallas kernels  44.7 us (25%)
  between operations  13.7 us (8%)
  other arithmetic  2.08 us (1%)
    ppermute x27, starting transfers between devices, shift(): return lax.ppermute(x, axis, pairs)  44.4 us
    ppermute x27, waiting for transfers between devices, shift(): return lax.ppermute(x, axis, pairs)  41.4 us
    pallas_call x11, Pallas kernels, call(): pl.pallas_call(inner, out_shape=[pltpu.HBM(o.shape, o.dtype) for o in out...  24.1 us
    ppermute x2, starting transfers between devices, swap(): return lax.ppermute(x, 'core', [(0, 1), (1, 0)])  22.4 us
    pallas_call x2, Pallas kernels, feed_forward(): pl.pallas_call(hidden_rows, out_shape=[pltpu.HBM((size, width), BF16)] *...  20.5 us
    all_gather x1, waiting for transfers between devices, on_device(): weights = lax.all_gather(both, SP, axis=0, tiled=True)  10.1 us
  transfers between devices with their start and end apart: 30, of which 15 were waited for; matrix products, arithmetic and copies ran while one was open for 1% of the time, Pallas kernels for 17%

profile of v4, /device:TPU:33, one launch (start us, length us, event | category | flops | bytes accessed | tf_op | source)
XLA Modules:
  0.0 180.9 jit_solution(5296050084456661029)
XLA Ops:
  6.6 2.0 %pad_maximum_fusion = bf16[64,4096]{1,0:T(8,128)(2,1)} fusion(bf16[64,2048]{1,0:T(8,128)(2,1)} %bitcast.23, bf16[64,2048]{1,0:T(8,128)(2,1)} %param.30), kind=kLoop, calls=%fused_computation | loop fusion | flops 1048576 | bytes 1048576 | tf_op jit(solution)/shard_map/concatenate | solution.py:461
  8.6 0.1 all-gather.2.cloned.1.call-update
  8.6 2.3 %own_state.1.refs_1_ = bf16[2,128,768]{2,1,0:T(8,128)(2,1)S(1)} custom-call(bf16[512,256]{1,0:T(8,128)(2,1)} %refs_1_.3, bf16[512,512]{1,0:T(8,128)(2,1)} %refs_2_.3, f32[1,512]{1,0:T(1,128)} %refs_6_.3, bf16[512,128]{1,0:T(8,128)(2,1)} %refs_5_.4, bf16[512,256]{1,0:T(8,128)(2,1)} %refs_6_.2, f32[1,512]{1,0:T(1,128)} %refs_7_.3), custom_call_target="tpu_custom_call" | custom-call | flops 134217728 | bytes 1000000 | tf_op jit(solution)/shard_map/own_state/pallas_call | solution.py:70
  10.9 20.5 %collective-permute-start = (bf16[2,128,768]{2,1,0:T(8,128)(2,1)S(1)}, bf16[2,128,768]{2,1,0:T(8,128)(2,1)S(1)}, u32[]{:S(2)}, u32[]{:S(2)}) collective-permute-start(bf16[2,128,768]{2,1,0:T(8,128)(2,1)S(1)} %own_state.1.refs_1_), channel_id=1, source_target_pairs={{0,4},{4,0},{1,5},{5,1},{2,6},{6,2},{3,7},{7,3},{8,12},{12,8},{9,1... | collective-permute-start | bytes 1179656 | tf_op jit(solution)/shard_map/ppermute | solution.py:421
  31.4 0.1 pad_add_fusion.refs_0_
  31.5 1.3 collective-permute-done.refs_2_.refs_3_
  32.8 0.9 of_chip.1
  33.7 0.1 collective-permute-start.1
  33.9 0.1 collective-permute-start.2
  34.0 3.1 %collective-permute-start.3 = (bf16[32,768]{1,0:T(8,128)(2,1)S(1)}, bf16[32,768]{1,0:T(8,128)(2,1)S(1)}, u32[]{:S(2)}, u32[]{:S(2)}) collective-permute-start(bf16[32,768]{1,0:T(8,128)(2,1)S(1)} %get-tuple-element.57), channel_id=1, source_target_pairs={{0,24},{8,0},{16,8},{24,16},{1,25},{9,1},{17,9},{25,17},{2,26},{10... | collective-permute-start | bytes 147464 | tf_op jit(solution)/shard_map/ppermute | solution.py:417
  37.1 1.5 collective-permute-done.1.refs_2_
  38.7 0.0 collective-permute-done.2.refs_3_
  38.7 1.1 collective-permute-done.3.refs_4_
  39.7 0.8 of_group.1
  40.5 1.3 collective-permute-start.4
  41.8 12.2 %collective-permute-start.5 = (bf16[1,32,768]{2,1,0:T(8,128)(2,1)S(1)}, bf16[1,32,768]{2,1,0:T(8,128)(2,1)S(1)}, u32[]{:S(2)}, u32[]{:S(2)}) collective-permute-start(bf16[1,32,768]{2,1,0:T(8,128)(2,1)S(1)} %of_group.1), channel_id=1, source_target_pairs={{0,64},{32,96},{1,65},{33,97},{2,66},{34,98},{3,67},{35,99},{4,68}... | collective-permute-start | bytes 147464 | tf_op jit(solution)/shard_map/ppermute | solution.py:417
  54.1 1.3 collective-permute-start.6
  55.4 0.0 collective-permute-done.4.refs_5_
  55.4 0.9 collective-permute-done.5.refs_6_
  56.2 6.5 %collective-permute-done.6.refs_7_ = bf16[1,32,768]{2,1,0:T(8,128)(2,1)S(1)} collective-permute-done((bf16[1,32,768]{2,1,0:T(8,128)(2,1)S(1)}, bf16[1,32,768]{2,1,0:T(8,128)(2,1)S(1)}, u32[]{:S(2)}, u32[]{:S(2)}) %collective-permute-start.6) | collective-permute-done | bytes 49184 | tf_op jit(solution)/shard_map/ppermute | solution.py:417
  62.7 0.8 before_each.1
  63.5 2.0 %collective-permute-start.7 = (bf16[32,640]{1,0:T(8,128)(2,1)S(1)}, bf16[32,640]{1,0:T(8,128)(2,1)S(1)}, u32[]{:S(2)}, u32[]{:S(2)}) collective-permute-start(bf16[32,640]{1,0:T(8,128)(2,1)S(1)} %get-tuple-element.63), channel_id=1, source_target_pairs={{0,8},{8,16},{16,24},{24,0},{1,9},{9,17},{17,25},{25,1},{2,10},{10... | collective-permute-start | bytes 122888 | tf_op jit(solution)/shard_map/ppermute | solution.py:417
  65.6 0.0 collective-permute-start.8
  65.6 2.2 %collective-permute-start.9 = (bf16[32,640]{1,0:T(8,128)(2,1)S(1)}, bf16[32,640]{1,0:T(8,128)(2,1)S(1)}, u32[]{:S(2)}, u32[]{:S(2)}) collective-permute-start(bf16[32,640]{1,0:T(8,128)(2,1)S(1)} %get-tuple-element.61), channel_id=1, source_target_pairs={{0,24},{8,0},{16,8},{24,16},{1,25},{9,1},{17,9},{25,17},{2,26},{10... | collective-permute-start | bytes 122888 | tf_op jit(solution)/shard_map/ppermute | solution.py:417
  67.8 1.5 collective-permute-done.7.refs_2_
  69.3 2.5 %collective-permute-done.8.refs_3_ = bf16[32,640]{1,0:T(8,128)(2,1)S(1)} collective-permute-done((bf16[32,640]{1,0:T(8,128)(2,1)S(1)}, bf16[32,640]{1,0:T(8,128)(2,1)S(1)}, u32[]{:S(2)}, u32[]{:S(2)}) %collective-permute-start.8) | collective-permute-done | bytes 40992 | tf_op jit(solution)/shard_map/ppermute | solution.py:417
  71.8 0.6 gathered_half.1.refs_1_
  72.4 1.9 %collective-permute-start.10 = (bf16[128,640]{1,0:T(8,128)(2,1)S(1)}, bf16[128,640]{1,0:T(8,128)(2,1)S(1)}, u32[]{:S(2)}, u32[]{:S(2)}) collective-permute-start(bf16[128,640]{1,0:T(8,128)(2,1)S(1)} %gathered_half.1.refs_1_), channel_id=1, source_target_pairs={{0,4},{4,0},{1,5},{5,1},{2,6},{6,2},{3,7},{7,3},{8,12},{12,8},{9,1... | collective-permute-start | bytes 491528 | tf_op jit(solution)/shard_map/ppermute | solution.py:421
  74.3 2.6 %inside.1.refs_8_ = f32[512,768]{1,0:T(8,128)S(1)} custom-call(bf16[512,256]{1,0:T(8,128)(2,1)} %refs_4_.5, bf16[512,256]{1,0:T(8,128)(2,1)} %refs_1_.3, bf16[512,512]{1,0:T(8,128)(2,1)} %refs_2_.3, f32[1,512]{1,0:T(1,128)} %refs_6_.3, bf16[512,128]{1,0:T(8,128)(2,1)} %refs_5_.5, bf16[512,128]{1,0:T(8,128)(2,1)} %refs_5_.4, bf16[512,256]{1,0:T(8,128)(2,1)} %refs_6_.2, ...), custom_call_target="tpu_custom_call" | custom-call | flops 805306368 | bytes 4000000 | tf_op jit(solution)/shard_map/inside/pallas_call | solution.py:70
  76.9 0.0 collective-permute-done.10.refs_2_
  77.0 7.5 %heads_out.1 = (bf16[64,2048]{1,0:T(8,128)(2,1)}, bf16[64,2048]{1,0:T(8,128)(2,1)}, bf16[64,2048]{1,0:T(8,128)(2,1)}, bf16[64,2048]{1,0:T(8,128)(2,1)}, bf16[64,...) custom-call(s32[3]{0:T(128)S(1)} %pad_add_fusion.refs_0_, ...), custom_call_target="tpu_custom_call" | custom-call | flops 2147483648 | bytes 8000000 | tf_op jit(solution)/shard_map/heads_out/pallas_call | solution.py:70
  84.4 1.8 collective-permute-start.11
  86.2 1.7 collective-permute-start.12
  87.9 1.3 collective-permute-start.14
  89.3 0.1 collective-permute-start.15
  89.4 5.4 %collective-permute-done.11.refs_1_ = bf16[64,2048]{1,0:T(8,128)(2,1)S(1)} collective-permute-done((bf16[64,2048]{1,0:T(8,128)(2,1)}, bf16[64,2048]{1,0:T(8,128)(2,1)S(1)}, u32[]{:S(2)}, u32[]{:S(2)}) %collective-permute-start.11) | collective-permute-done | bytes 262176 | tf_op jit(solution)/shard_map/ppermute | solution.py:417
  94.8 1.9 %add_two.2 = (bf16[64,2048]{1,0:T(8,128)(2,1)}, bf16[64,2048]{1,0:T(8,128)(2,1)}) custom-call(bf16[64,2048]{1,0:T(8,128)(2,1)} %get-tuple-element.32.refs_0_, bf16[64,2048]{1,0:T(8,128)(2,1)S(1)} %collective-permute-done.11.refs_1_, bf16[64,2048]{1,0:T(8,128)(2,1)} %get-tuple-element.34.refs_2_, bf16[64,2048]{1,0:T(8,128)(2,1)S(1)} %collective-permute-done.12.refs_3_), custom_call_target="tpu_custom_call" | custom-call | tf_op jit(solution)/shard_map/add_two/pallas_call | solution.py:70
  96.7 0.8 collective-permute-start.13
  97.5 2.0 %collective-permute-start.16 = (bf16[64,2048]{1,0:T(8,128)(2,1)}, bf16[64,2048]{1,0:T(8,128)(2,1)S(1)}, u32[]{:S(2)}, u32[]{:S(2)}) collective-permute-start(bf16[64,2048]{1,0:T(8,128)(2,1)} %get-tuple-element.40), channel_id=1, source_target_pairs={{0,3},{1,0},{2,1},{3,2},{4,7},{5,4},{6,5},{7,6},{8,11},{9,8},{10,9... | collective-permute-start | bytes 786440 | tf_op jit(solution)/shard_map/ppermute | solution.py:417
  99.5 0.8 constant_dynamic-slice_fusion.refs_6_
  100.3 0.0 collective-permute-done.15.refs_4_
  100.4 4.6 %collective-permute-done.13.refs_1_ = bf16[64,2048]{1,0:T(8,128)(2,1)S(1)} collective-permute-done((bf16[64,2048]{1,0:T(8,128)(2,1)}, bf16[64,2048]{1,0:T(8,128)(2,1)S(1)}, u32[]{:S(2)}, u32[]{:S(2)}) %collective-permute-start.13) | collective-permute-done | bytes 262176 | tf_op jit(solution)/shard_map/ppermute | solution.py:417
  105.0 2.6 %rows_mid.1 = (bf16[64,2048]{1,0:T(8,128)(2,1)}, bf16[64,2048]{1,0:T(8,128)(2,1)}, bf16[64,2048]{1,0:T(8,128)(2,1)}, bf16[64,2048]{1,0:T(8,128)(2,1)}) custom-call(bf16[64,2048]{1,0:T(8,128)(2,1)} %get-tuple-element.31.refs_0_, bf16[64,2048]{1,0:T(8,128)(2,1)S(1)} %collective-permute-done.13.refs_1_, bf16[64,2048]{1,0:T(8,128)(2,1)S(1)} %collective-permute-done.14.refs_2_, ...), custom_call_target="tpu_custom_call" | custom-call | tf_op jit(solution)/shard_map/rows_mid/pallas_call | solution.py:70
  107.6 0.3 collective-permute-start.17
  107.9 2.5 %collective-permute-start.19 = (bf16[64,2048]{1,0:T(8,128)(2,1)}, bf16[64,2048]{1,0:T(8,128)(2,1)S(1)}, u32[]{:S(2)}, u32[]{:S(2)}) collective-permute-start(bf16[64,2048]{1,0:T(8,128)(2,1)} %get-tuple-element.49.refs_1_), channel_id=1, source_target_pairs={{0,3},{1,0},{2,1},{3,2},{4,7},{5,4},{6,5},{7,6},{8,11},{9,8},{10,9... | collective-permute-start | bytes 786440 | tf_op jit(solution)/shard_map/ppermute | solution.py:417
  110.4 1.3 collective-permute-start.21
  111.6 0.2 collective-permute-start.22
  111.8 3.3 %collective-permute-done.17.refs_4_ = bf16[64,2048]{1,0:T(8,128)(2,1)S(1)} collective-permute-done((bf16[64,2048]{1,0:T(8,128)(2,1)}, bf16[64,2048]{1,0:T(8,128)(2,1)S(1)}, u32[]{:S(2)}, u32[]{:S(2)}) %collective-permute-start.17) | collective-permute-done | bytes 262176 | tf_op jit(solution)/shard_map/ppermute | solution.py:417
  115.1 2.7 %collective-permute-start.20 = (bf16[64,2048]{1,0:T(8,128)(2,1)S(1)}, bf16[64,2048]{1,0:T(8,128)(2,1)}, u32[]{:S(2)}, u32[]{:S(2)}) collective-permute-start(bf16[64,2048]{1,0:T(8,128)(2,1)S(1)} %collective-permute-done.19.refs_3_), channel_id=1, source_target_pairs={{0,3},{1,0},{2,1},{3,2},{4,7},{5,4},{6,5},{7,6},{8,11},{9,8},{10,9... | collective-permute-start | bytes 786440 | tf_op jit(solution)/shard_map/ppermute | solution.py:417
  117.8 1.9 %collective-permute-done.21.refs_2_ = bf16[64,2048]{1,0:T(8,128)(2,1)S(1)} collective-permute-done((bf16[64,2048]{1,0:T(8,128)(2,1)}, bf16[64,2048]{1,0:T(8,128)(2,1)S(1)}, u32[]{:S(2)}, u32[]{:S(2)}) %collective-permute-start.21) | collective-permute-done | bytes 262176 | tf_op jit(solution)/shard_map/ppermute | solution.py:417
  119.7 1.7 collective-permute-done.22.refs_5_
  121.4 5.6 %collective-permute-done.18.refs_0_ = bf16[64,2048]{1,0:T(8,128)(2,1)S(1)} collective-permute-done((bf16[64,2048]{1,0:T(8,128)(2,1)S(1)}, bf16[64,2048]{1,0:T(8,128)(2,1)S(1)}, u32[]{:S(2)}, u32[]{:S(2)}) %collective-permute-start.18) | collective-permute-done | bytes 262176 | tf_op jit(solution)/shard_map/ppermute | solution.py:417
  127.0 10.1 %all-gather.2.cloned.1.call-done.refs_6_.refs_2_ = bf16[2048,4096]{1,0:T(8,128)(2,1)} async-done(((bf16[64,4096]{1,0:T(8,128)(2,1)}), bf16[2048,4096]{1,0:T(8,128)(2,1)}) %all-gather.2.cloned.1.call-update) | async-done | bytes 16777232 | tf_op jit(solution)/shard_map/all_gather | solution.py:462
  137.1 11.9 %hidden_rows.2 = (bf16[64,2048]{1,0:T(8,128)(2,1)}, bf16[64,2048]{1,0:T(8,128)(2,1)}, bf16[64,2048]{1,0:T(8,128)(2,1)}, bf16[64,2048]{1,0:T(8,128)(2,1)}, bf16[6...) custom-call(bf16[64,2048]{1,0:T(8,128)(2,1)} %copy-done.5, bf16[64,2048]{1,0:T(8,128)(2,1)} %collective-permute-done.20.refs_1_, ...), custom_call_target="tpu_custom_call" | custom-call | flops 6442450944 | bytes 16777216 | tf_op jit(solution)/shard_map/hidden_rows/pallas_call | solution.py:380
  149.0 1.2 collective-permute-start.23
  150.2 1.8 collective-permute-start.24
  152.0 0.9 collective-permute-start.26
  152.9 0.5 collective-permute-start.27
  153.5 4.9 %collective-permute-done.23.refs_1_ = bf16[64,2048]{1,0:T(8,128)(2,1)S(1)} collective-permute-done((bf16[64,2048]{1,0:T(8,128)(2,1)}, bf16[64,2048]{1,0:T(8,128)(2,1)S(1)}, u32[]{:S(2)}, u32[]{:S(2)}) %collective-permute-start.23) | collective-permute-done | bytes 262176 | tf_op jit(solution)/shard_map/ppermute | solution.py:417
  158.3 1.9 %add_two.3 = (bf16[64,2048]{1,0:T(8,128)(2,1)}, bf16[64,2048]{1,0:T(8,128)(2,1)}) custom-call(bf16[64,2048]{1,0:T(8,128)(2,1)} %get-tuple-element.43.refs_0_, bf16[64,2048]{1,0:T(8,128)(2,1)S(1)} %collective-permute-done.23.refs_1_, bf16[64,2048]{1,0:T(8,128)(2,1)} %get-tuple-element.45.refs_2_, bf16[64,2048]{1,0:T(8,128)(2,1)S(1)} %collective-permute-done.24.refs_3_), custom_call_target="tpu_custom_call" | custom-call | tf_op jit(solution)/shard_map/add_two/pallas_call | solution.py:70
  160.3 0.7 collective-permute-start.25
  161.0 2.1 %collective-permute-start.28 = (bf16[64,2048]{1,0:T(8,128)(2,1)}, bf16[64,2048]{1,0:T(8,128)(2,1)S(1)}, u32[]{:S(2)}, u32[]{:S(2)}) collective-permute-start(bf16[64,2048]{1,0:T(8,128)(2,1)} %get-tuple-element.55), channel_id=1, source_target_pairs={{0,3},{1,0},{2,1},{3,2},{4,7},{5,4},{6,5},{7,6},{8,11},{9,8},{10,9... | collective-permute-start | bytes 786440 | tf_op jit(solution)/shard_map/ppermute | solution.py:417
  163.1 8.6 %hidden_rows.3 = (bf16[64,2048]{1,0:T(8,128)(2,1)}, bf16[64,2048]{1,0:T(8,128)(2,1)}) custom-call(bf16[64,2048]{1,0:T(8,128)(2,1)} %get-tuple-element.48.refs_0_, bf16[64,2048]{1,0:T(8,128)(2,1)} %get-tuple-element.49.refs_1_, bf16[2048,4096]{1,0:T(8,128)(2,1)} %all-gather.2.cloned.1.call-done.refs_6_.refs_2_), custom_call_target="tpu_custom_call" | custom-call | flops 2147483648 | bytes 16777216 | tf_op jit(solution)/shard_map/hidden_rows/pallas_call | solution.py:380
  171.7 2.3 %last_sum.1 = bf16[128,2048]{1,0:T(8,128)(2,1)} custom-call(bf16[64,2048]{1,0:T(8,128)(2,1)} %get-tuple-element.50.refs_0_, bf16[64,2048]{1,0:T(8,128)(2,1)S(1)} %collective-permute-done.25.refs_1_, bf16[64,2048]{1,0:T(8,128)(2,1)S(1)} %collective-permute-done.26.refs_2_, bf16[64,2048]{1,0:T(8,128)(2,1)} %get-tuple-element.52.refs_3_, ...), custom_call_target="tpu_custom_call" | custom-call | tf_op jit(solution)/shard_map/last_sum/pallas_call | solution.py:70
  (27 shorter events, 0.1 us)
Async XLA Ops:
  6.5 93.0 %copy-start = (bf16[512,2048]{1,0:T(8,128)(2,1)S(1)}, bf16[512,2048]{1,0:T(8,128)(2,1)}, u32[]{:S(2)}) copy-start(bf16[512,2048]{1,0:T(8,128)(2,1)} %param.16) | copy-start | bytes 6291460
  6.6 130.5 %all-gather.2.cloned.1.call-start = ((), (), s32[]{:S(2)}) async-start(), calls=%async_computation | async-start | bytes 17301504 | tf_op jit(solution)/shard_map/all_gather | solution.py:462
  10.9 21.9 %collective-permute-start = (bf16[2,128,768]{2,1,0:T(8,128)(2,1)S(1)}, bf16[2,128,768]{2,1,0:T(8,128)(2,1)S(1)}, u32[]{:S(2)}, u32[]{:S(2)}) collective-permute-start(bf16[2,128,768]{2,1,0:T(8,128)(2,1)S(1)} %own_state.1.refs_1_), channel_id=1, source_target_pairs={{0,4},{4,0},{1,5},{5,1},{2,6},{6,2},{3,7},{7,3},{8,12},{12,8},{9,1... | collective-permute-start | bytes 1179656 | tf_op jit(solution)/shard_map/ppermute | solution.py:421
  33.7 4.9 %collective-permute-start.1 = (bf16[32,768]{1,0:T(8,128)(2,1)S(1)}, bf16[32,768]{1,0:T(8,128)(2,1)S(1)}, u32[]{:S(2)}, u32[]{:S(2)}) collective-permute-start(bf16[32,768]{1,0:T(8,128)(2,1)S(1)} %get-tuple-element.59), channel_id=1, source_target_pairs={{0,8},{8,16},{16,24},{24,0},{1,9},{9,17},{17,25},{25,1},{2,10},{10... | collective-permute-start | bytes 147464 | tf_op jit(solution)/shard_map/ppermute | solution.py:417
  33.9 4.8 %collective-permute-start.2 = (bf16[32,768]{1,0:T(8,128)(2,1)S(1)}, bf16[32,768]{1,0:T(8,128)(2,1)S(1)}, u32[]{:S(2)}, u32[]{:S(2)}) collective-permute-start(bf16[32,768]{1,0:T(8,128)(2,1)S(1)} %get-tuple-element.58), channel_id=1, source_target_pairs={{0,16},{8,24},{16,0},{24,8},{1,17},{9,25},{17,1},{25,9},{2,18},{10... | collective-permute-start | bytes 147464 | tf_op jit(solution)/shard_map/ppermute | solution.py:417
  34.0 5.7 %collective-permute-start.3 = (bf16[32,768]{1,0:T(8,128)(2,1)S(1)}, bf16[32,768]{1,0:T(8,128)(2,1)S(1)}, u32[]{:S(2)}, u32[]{:S(2)}) collective-permute-start(bf16[32,768]{1,0:T(8,128)(2,1)S(1)} %get-tuple-element.57), channel_id=1, source_target_pairs={{0,24},{8,0},{16,8},{24,16},{1,25},{9,1},{17,9},{25,17},{2,26},{10... | collective-permute-start | bytes 147464 | tf_op jit(solution)/shard_map/ppermute | solution.py:417
  40.5 14.9 %collective-permute-start.4 = (bf16[1,32,768]{2,1,0:T(8,128)(2,1)S(1)}, bf16[1,32,768]{2,1,0:T(8,128)(2,1)S(1)}, u32[]{:S(2)}, u32[]{:S(2)}) collective-permute-start(bf16[1,32,768]{2,1,0:T(8,128)(2,1)S(1)} %of_group.1), channel_id=1, source_target_pairs={{0,32},{32,64},{64,96},{1,33},{33,65},{65,97},{2,34},{34,66},{66,9... | collective-permute-start | bytes 147464 | tf_op jit(solution)/shard_map/ppermute | solution.py:417
  41.8 14.4 %collective-permute-start.5 = (bf16[1,32,768]{2,1,0:T(8,128)(2,1)S(1)}, bf16[1,32,768]{2,1,0:T(8,128)(2,1)S(1)}, u32[]{:S(2)}, u32[]{:S(2)}) collective-permute-start(bf16[1,32,768]{2,1,0:T(8,128)(2,1)S(1)} %of_group.1), channel_id=1, source_target_pairs={{0,64},{32,96},{1,65},{33,97},{2,66},{34,98},{3,67},{35,99},{4,68}... | collective-permute-start | bytes 147464 | tf_op jit(solution)/shard_map/ppermute | solution.py:417
  54.1 8.7 %collective-permute-start.6 = (bf16[1,32,768]{2,1,0:T(8,128)(2,1)S(1)}, bf16[1,32,768]{2,1,0:T(8,128)(2,1)S(1)}, u32[]{:S(2)}, u32[]{:S(2)}) collective-permute-start(bf16[1,32,768]{2,1,0:T(8,128)(2,1)S(1)} %of_group.1), channel_id=1, source_target_pairs={{0,96},{1,97},{2,98},{3,99},{4,100},{5,101},{6,102},{7,103},{8,104... | collective-permute-start | bytes 147464 | tf_op jit(solution)/shard_map/ppermute | solution.py:417
  63.5 5.8 %collective-permute-start.7 = (bf16[32,640]{1,0:T(8,128)(2,1)S(1)}, bf16[32,640]{1,0:T(8,128)(2,1)S(1)}, u32[]{:S(2)}, u32[]{:S(2)}) collective-permute-start(bf16[32,640]{1,0:T(8,128)(2,1)S(1)} %get-tuple-element.63), channel_id=1, source_target_pairs={{0,8},{8,16},{16,24},{24,0},{1,9},{9,17},{17,25},{25,1},{2,10},{10... | collective-permute-start | bytes 122888 | tf_op jit(solution)/shard_map/ppermute | solution.py:417
  65.6 6.3 %collective-permute-start.8 = (bf16[32,640]{1,0:T(8,128)(2,1)S(1)}, bf16[32,640]{1,0:T(8,128)(2,1)S(1)}, u32[]{:S(2)}, u32[]{:S(2)}) collective-permute-start(bf16[32,640]{1,0:T(8,128)(2,1)S(1)} %get-tuple-element.62), channel_id=1, source_target_pairs={{0,16},{8,24},{16,0},{24,8},{1,17},{9,25},{17,1},{25,9},{2,18},{10... | collective-permute-start | bytes 122888 | tf_op jit(solution)/shard_map/ppermute | solution.py:417
  65.6 6.3 %collective-permute-start.9 = (bf16[32,640]{1,0:T(8,128)(2,1)S(1)}, bf16[32,640]{1,0:T(8,128)(2,1)S(1)}, u32[]{:S(2)}, u32[]{:S(2)}) collective-permute-start(bf16[32,640]{1,0:T(8,128)(2,1)S(1)} %get-tuple-element.61), channel_id=1, source_target_pairs={{0,24},{8,0},{16,8},{24,16},{1,25},{9,1},{17,9},{25,17},{2,26},{10... | collective-permute-start | bytes 122888 | tf_op jit(solution)/shard_map/ppermute | solution.py:417
  72.4 4.5 %collective-permute-start.10 = (bf16[128,640]{1,0:T(8,128)(2,1)S(1)}, bf16[128,640]{1,0:T(8,128)(2,1)S(1)}, u32[]{:S(2)}, u32[]{:S(2)}) collective-permute-start(bf16[128,640]{1,0:T(8,128)(2,1)S(1)} %gathered_half.1.refs_1_), channel_id=1, source_target_pairs={{0,4},{4,0},{1,5},{5,1},{2,6},{6,2},{3,7},{7,3},{8,12},{12,8},{9,1... | collective-permute-start | bytes 491528 | tf_op jit(solution)/shard_map/ppermute | solution.py:421
  84.4 10.3 %collective-permute-start.11 = (bf16[64,2048]{1,0:T(8,128)(2,1)}, bf16[64,2048]{1,0:T(8,128)(2,1)S(1)}, u32[]{:S(2)}, u32[]{:S(2)}) collective-permute-start(bf16[64,2048]{1,0:T(8,128)(2,1)} %get-tuple-element.33), channel_id=1, source_target_pairs={{0,1},{1,2},{2,3},{3,0},{4,5},{5,6},{6,7},{7,4},{8,9},{9,10},{10,1... | collective-permute-start | bytes 786440 | tf_op jit(solution)/shard_map/ppermute | solution.py:417
  86.2 8.5 %collective-permute-start.12 = (bf16[64,2048]{1,0:T(8,128)(2,1)}, bf16[64,2048]{1,0:T(8,128)(2,1)S(1)}, u32[]{:S(2)}, u32[]{:S(2)}) collective-permute-start(bf16[64,2048]{1,0:T(8,128)(2,1)} %get-tuple-element.35), channel_id=1, source_target_pairs={{0,3},{1,0},{2,1},{3,2},{4,7},{5,4},{6,5},{7,6},{8,11},{9,8},{10,9... | collective-permute-start | bytes 786440 | tf_op jit(solution)/shard_map/ppermute | solution.py:417
  87.9 12.4 %collective-permute-start.14 = (bf16[64,2048]{1,0:T(8,128)(2,1)}, bf16[64,2048]{1,0:T(8,128)(2,1)S(1)}, u32[]{:S(2)}, u32[]{:S(2)}) collective-permute-start(bf16[64,2048]{1,0:T(8,128)(2,1)} %get-tuple-element.37), channel_id=1, source_target_pairs={{0,3},{1,0},{2,1},{3,2},{4,7},{5,4},{6,5},{7,6},{8,11},{9,8},{10,9... | collective-permute-start | bytes 786440 | tf_op jit(solution)/shard_map/ppermute | solution.py:417
  89.3 11.1 %collective-permute-start.15 = (bf16[64,2048]{1,0:T(8,128)(2,1)}, bf16[64,2048]{1,0:T(8,128)(2,1)S(1)}, u32[]{:S(2)}, u32[]{:S(2)}) collective-permute-start(bf16[64,2048]{1,0:T(8,128)(2,1)} %get-tuple-element.39), channel_id=1, source_target_pairs={{0,1},{1,2},{2,3},{3,0},{4,5},{5,6},{6,7},{7,4},{8,9},{9,10},{10,1... | collective-permute-start | bytes 786440 | tf_op jit(solution)/shard_map/ppermute | solution.py:417
  96.7 8.3 %collective-permute-start.13 = (bf16[64,2048]{1,0:T(8,128)(2,1)}, bf16[64,2048]{1,0:T(8,128)(2,1)S(1)}, u32[]{:S(2)}, u32[]{:S(2)}) collective-permute-start(bf16[64,2048]{1,0:T(8,128)(2,1)} %get-tuple-element.36), channel_id=1, source_target_pairs={{0,1},{1,2},{2,3},{3,0},{4,5},{5,6},{6,7},{7,4},{8,9},{9,10},{10,1... | collective-permute-start | bytes 786440 | tf_op jit(solution)/shard_map/ppermute | solution.py:417
  97.5 7.5 %collective-permute-start.16 = (bf16[64,2048]{1,0:T(8,128)(2,1)}, bf16[64,2048]{1,0:T(8,128)(2,1)S(1)}, u32[]{:S(2)}, u32[]{:S(2)}) collective-permute-start(bf16[64,2048]{1,0:T(8,128)(2,1)} %get-tuple-element.40), channel_id=1, source_target_pairs={{0,3},{1,0},{2,1},{3,2},{4,7},{5,4},{6,5},{7,6},{8,11},{9,8},{10,9... | collective-permute-start | bytes 786440 | tf_op jit(solution)/shard_map/ppermute | solution.py:417
  107.6 7.5 %collective-permute-start.17 = (bf16[64,2048]{1,0:T(8,128)(2,1)}, bf16[64,2048]{1,0:T(8,128)(2,1)S(1)}, u32[]{:S(2)}, u32[]{:S(2)}) collective-permute-start(bf16[64,2048]{1,0:T(8,128)(2,1)} %get-tuple-element.48.refs_0_), channel_id=1, source_target_pairs={{0,1},{1,2},{2,3},{3,0},{4,5},{5,6},{6,7},{7,4},{8,9},{9,10},{10,1... | collective-permute-start | bytes 786440 | tf_op jit(solution)/shard_map/ppermute | solution.py:417
  107.9 7.2 %collective-permute-start.19 = (bf16[64,2048]{1,0:T(8,128)(2,1)}, bf16[64,2048]{1,0:T(8,128)(2,1)S(1)}, u32[]{:S(2)}, u32[]{:S(2)}) collective-permute-start(bf16[64,2048]{1,0:T(8,128)(2,1)} %get-tuple-element.49.refs_1_), channel_id=1, source_target_pairs={{0,3},{1,0},{2,1},{3,2},{4,7},{5,4},{6,5},{7,6},{8,11},{9,8},{10,9... | collective-permute-start | bytes 786440 | tf_op jit(solution)/shard_map/ppermute | solution.py:417
  110.4 9.3 %collective-permute-start.21 = (bf16[64,2048]{1,0:T(8,128)(2,1)}, bf16[64,2048]{1,0:T(8,128)(2,1)S(1)}, u32[]{:S(2)}, u32[]{:S(2)}) collective-permute-start(bf16[64,2048]{1,0:T(8,128)(2,1)} %get-tuple-element.48.refs_0_), channel_id=1, source_target_pairs={{0,3},{1,0},{2,1},{3,2},{4,7},{5,4},{6,5},{7,6},{8,11},{9,8},{10,9... | collective-permute-start | bytes 786440 | tf_op jit(solution)/shard_map/ppermute | solution.py:417
  111.6 9.7 %collective-permute-start.22 = (bf16[64,2048]{1,0:T(8,128)(2,1)}, bf16[64,2048]{1,0:T(8,128)(2,1)S(1)}, u32[]{:S(2)}, u32[]{:S(2)}) collective-permute-start(bf16[64,2048]{1,0:T(8,128)(2,1)} %get-tuple-element.49.refs_1_), channel_id=1, source_target_pairs={{0,1},{1,2},{2,3},{3,0},{4,5},{5,6},{6,7},{7,4},{8,9},{9,10},{10,1... | collective-permute-start | bytes 786440 | tf_op jit(solution)/shard_map/ppermute | solution.py:417
  115.1 22.0 %copy-start.1 = (bf16[64,2048]{1,0:T(8,128)(2,1)}, bf16[64,2048]{1,0:T(8,128)(2,1)S(1)}, u32[]{:S(2)}) copy-start(bf16[64,2048]{1,0:T(8,128)(2,1)S(1)} %collective-permute-done.17.refs_4_) | copy-start | bytes 786436
  115.1 11.9 %collective-permute-start.18 = (bf16[64,2048]{1,0:T(8,128)(2,1)S(1)}, bf16[64,2048]{1,0:T(8,128)(2,1)S(1)}, u32[]{:S(2)}, u32[]{:S(2)}) collective-permute-start(bf16[64,2048]{1,0:T(8,128)(2,1)S(1)} %collective-permute-done.17.refs_4_), channel_id=1, source_target_pairs={{0,1},{1,2},{2,3},{3,0},{4,5},{5,6},{6,7},{7,4},{8,9},{9,10},{10,1... | collective-permute-start | bytes 786440 | tf_op jit(solution)/shard_map/ppermute | solution.py:417
  115.1 22.0 %copy-start.2 = (bf16[64,2048]{1,0:T(8,128)(2,1)}, bf16[64,2048]{1,0:T(8,128)(2,1)S(1)}, u32[]{:S(2)}) copy-start(bf16[64,2048]{1,0:T(8,128)(2,1)S(1)} %collective-permute-done.19.refs_3_) | copy-start | bytes 786436
  115.1 11.9 %collective-permute-start.20 = (bf16[64,2048]{1,0:T(8,128)(2,1)S(1)}, bf16[64,2048]{1,0:T(8,128)(2,1)}, u32[]{:S(2)}, u32[]{:S(2)}) collective-permute-start(bf16[64,2048]{1,0:T(8,128)(2,1)S(1)} %collective-permute-done.19.refs_3_), channel_id=1, source_target_pairs={{0,3},{1,0},{2,1},{3,2},{4,7},{5,4},{6,5},{7,6},{8,11},{9,8},{10,9... | collective-permute-start | bytes 786440 | tf_op jit(solution)/shard_map/ppermute | solution.py:417
  119.7 17.4 %copy-start.3 = (bf16[64,2048]{1,0:T(8,128)(2,1)}, bf16[64,2048]{1,0:T(8,128)(2,1)S(1)}, u32[]{:S(2)}) copy-start(bf16[64,2048]{1,0:T(8,128)(2,1)S(1)} %collective-permute-done.21.refs_2_) | copy-start | bytes 786436
  121.4 15.7 %copy-start.4 = (bf16[64,2048]{1,0:T(8,128)(2,1)}, bf16[64,2048]{1,0:T(8,128)(2,1)S(1)}, u32[]{:S(2)}) copy-start(bf16[64,2048]{1,0:T(8,128)(2,1)S(1)} %collective-permute-done.22.refs_5_) | copy-start | bytes 786436
  127.0 10.1 %copy-start.5 = (bf16[64,2048]{1,0:T(8,128)(2,1)}, bf16[64,2048]{1,0:T(8,128)(2,1)S(1)}, u32[]{:S(2)}) copy-start(bf16[64,2048]{1,0:T(8,128)(2,1)S(1)} %collective-permute-done.18.refs_0_) | copy-start | bytes 786436
  149.0 9.3 %collective-permute-start.23 = (bf16[64,2048]{1,0:T(8,128)(2,1)}, bf16[64,2048]{1,0:T(8,128)(2,1)S(1)}, u32[]{:S(2)}, u32[]{:S(2)}) collective-permute-start(bf16[64,2048]{1,0:T(8,128)(2,1)} %get-tuple-element.44), channel_id=1, source_target_pairs={{0,1},{1,2},{2,3},{3,0},{4,5},{5,6},{6,7},{7,4},{8,9},{9,10},{10,1... | collective-permute-start | bytes 786440 | tf_op jit(solution)/shard_map/ppermute | solution.py:417
  150.2 8.1 %collective-permute-start.24 = (bf16[64,2048]{1,0:T(8,128)(2,1)}, bf16[64,2048]{1,0:T(8,128)(2,1)S(1)}, u32[]{:S(2)}, u32[]{:S(2)}) collective-permute-start(bf16[64,2048]{1,0:T(8,128)(2,1)} %get-tuple-element.46), channel_id=1, source_target_pairs={{0,3},{1,0},{2,1},{3,2},{4,7},{5,4},{6,5},{7,6},{8,11},{9,8},{10,9... | collective-permute-start | bytes 786440 | tf_op jit(solution)/shard_map/ppermute | solution.py:417
  152.0 19.7 %collective-permute-start.26 = (bf16[64,2048]{1,0:T(8,128)(2,1)}, bf16[64,2048]{1,0:T(8,128)(2,1)S(1)}, u32[]{:S(2)}, u32[]{:S(2)}) collective-permute-start(bf16[64,2048]{1,0:T(8,128)(2,1)} %get-tuple-element.51), channel_id=1, source_target_pairs={{0,3},{1,0},{2,1},{3,2},{4,7},{5,4},{6,5},{7,6},{8,11},{9,8},{10,9... | collective-permute-start | bytes 786440 | tf_op jit(solution)/shard_map/ppermute | solution.py:417
  152.9 18.8 %collective-permute-start.27 = (bf16[64,2048]{1,0:T(8,128)(2,1)}, bf16[64,2048]{1,0:T(8,128)(2,1)S(1)}, u32[]{:S(2)}, u32[]{:S(2)}) collective-permute-start(bf16[64,2048]{1,0:T(8,128)(2,1)} %get-tuple-element.54), channel_id=1, source_target_pairs={{0,1},{1,2},{2,3},{3,0},{4,5},{5,6},{6,7},{7,4},{8,9},{9,10},{10,1... | collective-permute-start | bytes 786440 | tf_op jit(solution)/shard_map/ppermute | solution.py:417
  160.3 11.5 %collective-permute-start.25 = (bf16[64,2048]{1,0:T(8,128)(2,1)}, bf16[64,2048]{1,0:T(8,128)(2,1)S(1)}, u32[]{:S(2)}, u32[]{:S(2)}) collective-permute-start(bf16[64,2048]{1,0:T(8,128)(2,1)} %get-tuple-element.47), channel_id=1, source_target_pairs={{0,1},{1,2},{2,3},{3,0},{4,5},{5,6},{6,7},{7,4},{8,9},{9,10},{10,1... | collective-permute-start | bytes 786440 | tf_op jit(solution)/shard_map/ppermute | solution.py:417
  161.0 10.7 %collective-permute-start.28 = (bf16[64,2048]{1,0:T(8,128)(2,1)}, bf16[64,2048]{1,0:T(8,128)(2,1)S(1)}, u32[]{:S(2)}, u32[]{:S(2)}) collective-permute-start(bf16[64,2048]{1,0:T(8,128)(2,1)} %get-tuple-element.55), channel_id=1, source_target_pairs={{0,3},{1,0},{2,1},{3,2},{4,7},{5,4},{6,5},{7,6},{8,11},{9,8},{10,9... | collective-permute-start | bytes 786440 | tf_op jit(solution)/shard_map/ppermute | solution.py:417
Sparse Core Ops, SparseCore 0:
  9.2 127.8 all-gather.1

commit v5 on v4

--- a/solution.py
+++ b/solution.py
@@ -285,9 +285,11 @@
         start = pl.multiple_of(order * 2 * rows, 2 * rows)
         turned_wide[pl.ds(start, 2 * rows), :] = wide[m * 2 * rows : (m + 1) * 2 * rows]
         turned_thin[pl.ds(start, 2 * rows), :] = thin[m * 2 * rows : (m + 1) * 2 * rows]
-    step = 512
-    for n in range(ow.shape[1] // step):
-        cols = slice(n * step, (n + 1) * step)
+    step = 1024
+
+    @pl.loop(0, ow.shape[1] // step)
+    def _(n):
+        cols = pl.ds(pl.multiple_of(n * step, step), step)
         done = (mm(turned_wide[...], ow[:, cols]) + mm(turned_thin[...], on[:, cols])).astype(BF16)
         for m, out in enumerate(outs):
             out[:, cols] = done[m * rows : (m + 1) * rows]
@@ -313,25 +315,35 @@
         normed[...] = (values * lax.rsqrt(power + EPS) * gain[...]).astype(BF16)
 
 
-def hidden_rows(*refs):
-    *ends, rows, up, down, total, hidden, done_rows, row_sems, up_sems, down_sems, out_sems = refs
-    number = len(ends) // 2
-    parts, weights, outs = ends[:number], ends[number], ends[number + 1 :]
-    count, block, units = up.shape
+def fetched(pairs, sems):
+    copies = [pltpu.make_async_copy(a, b, sems.at[n]) for n, (a, b) in enumerate(pairs)]
+    for copy in copies:
+        copy.start()
+    return copies
+
+
+def stacked(parts, rows):
     size = parts[0].shape[0]
-
-    def fetch_rows(n, k):
-        to = rows.at[k, pl.ds(n * size, size), :]
-        return pltpu.make_async_copy(parts[n].at[:, pl.ds(k * block, block)], to, row_sems.at[n, k])
+    return [rows.at[pl.ds(n * size, size), :] for n in range(len(parts))]
+
+
+def squared(x):
+    raised = jnp.maximum(x, 0.0)
+    return (raised * raised).astype(BF16)
+
+
+def first_rows(
+    a, b, weights, out_a, out_b, up, down, rows, total, hidden, row_sems, up_sems, down_sems
+):
+    units, block = up.shape[1], 512
+    count = up.shape[0] // block
 
     def fetch(k, column, to, sems):
-        start = pl.multiple_of(k * block, block)
-        source = weights.at[pl.ds(start, block), pl.ds(column * units, units)]
-        return pltpu.make_async_copy(source, to.at[k], sems.at[k])
-
-    pairs = [(n, k) for k in range(count) for n in range(number)]
-    for pair in pairs:
-        fetch_rows(*pair).start()
+        span = pl.ds(pl.multiple_of(k * block, block), block)
+        source = weights.at[span, pl.ds(column * units, units)]
+        return pltpu.make_async_copy(source, to.at[span, :], sems.at[k])
+
+    copies = fetched(list(zip((a, b), stacked((a, b), rows))), row_sems)
 
     @pl.loop(0, count)
     def _(k):
@@ -341,64 +353,100 @@
     def _(k):
         fetch(k, 1, down, down_sems).start()
 
-    for pair in pairs:
-        fetch_rows(*pair).wait()
-
+    for copy in copies:
+        copy.wait()
     total[...] = jnp.zeros_like(total)
 
     @pl.loop(0, count)
     def _(k):
         fetch(k, 0, up, up_sems).wait()
-        total[...] += mm(rows[k], up[k])
-
-    raised = jnp.maximum(total[...], 0.0)
-    hidden[...] = (raised * raised).astype(BF16)
+        span = pl.ds(pl.multiple_of(k * block, block), block)
+        total[...] += mm(rows[:, span], up[span, :])
+
+    hidden[...] = squared(total[...])
 
     @pl.loop(0, count)
     def _(k):
         fetch(k, 1, down, down_sems).wait()
-        start = pl.multiple_of(k * block, block)
-        done = mm(hidden[...], down[k], ((1,), (1,))).astype(BF16)
-        done_rows[:, pl.ds(start, block)] = done
-
-    copies = []
-    for n, out in enumerate(outs):
-        source = done_rows.at[pl.ds(n * size, size), :]
-        copies.append(pltpu.make_async_copy(source, out, out_sems.at[n]))
-        copies[-1].start()
-    for copy in copies:
+        span = pl.ds(pl.multiple_of(k * block, block), block)
+        rows[:, span] = mm(hidden[...], down[span, :], ((1,), (1,))).astype(BF16)
+
+    for copy in fetched(list(zip(stacked((a, b), rows), (out_a, out_b))), row_sems):
         copy.wait()
 
 
-def feed_forward(parts, weights):
+def more_rows(*refs):
+    *ends, rows, hidden, row_sems = refs
+    number = (len(ends) - 2) // 2
+    parts, (up, down), outs = ends[:number], ends[number : number + 2], ends[number + 2 :]
+    size, block = parts[0].shape[0], 1024
+    for copy in fetched(list(zip(parts, stacked(parts, rows))), row_sems):
+        copy.wait()
+
+    @pl.loop(0, up.shape[1] // block)
+    def _(n):
+        cols = pl.ds(pl.multiple_of(n * block, block), block)
+        hidden[:, cols] = squared(mm(rows[...], up[:, cols]))
+
+    @pl.loop(0, down.shape[0] // block)
+    def _(n):
+        cols = pl.ds(pl.multiple_of(n * block, block), block)
+        done = mm(hidden[...], down[cols, :], ((1,), (1,))).astype(BF16)
+        for m, out in enumerate(outs):
+            out[:, cols] = done[m * size : (m + 1) * size]
+
+
+def first_forward(parts, weights):
     size, width = parts[0].shape
     units = weights.shape[1] // 2
-    number, block = len(parts), 512
-    count, total = width // block, number * size
+    count, total = width // 512, 2 * size
     far = pl.BlockSpec(memory_space=pltpu.HBM)
     held = [pltpu.with_memory_space_constraint(p, pltpu.HBM) for p in (*parts, weights)]
-    return pl.pallas_call(
-        hidden_rows,
-        out_shape=[pltpu.HBM((size, width), BF16)] * number,
-        in_specs=[far] * (number + 1),
-        out_specs=[far] * number,
+    out_a, out_b, up, down = pl.pallas_call(
+        first_rows,
+        out_shape=[pltpu.HBM((size, width), BF16)] * 2 + [pltpu.VMEM((width, units), BF16)] * 2,
+        in_specs=[far] * 3,
+        out_specs=[far] * 2 + [vmem()] * 2,
         scratch_shapes=[
-            pltpu.VMEM((count, total, block), BF16),
-            pltpu.VMEM((count, block, units), BF16),
-            pltpu.VMEM((count, block, units), BF16),
+            pltpu.VMEM((total, width), BF16),
             pltpu.VMEM((total, units), F32),
             pltpu.VMEM((total, units), BF16),
-            pltpu.VMEM((total, width), BF16),
-            pltpu.SemaphoreType.DMA((number, count)),
+            pltpu.SemaphoreType.DMA((2,)),
             pltpu.SemaphoreType.DMA((count,)),
             pltpu.SemaphoreType.DMA((count,)),
-            pltpu.SemaphoreType.DMA((number,)),
         ],
-        compiler_params=pltpu.CompilerParams(vmem_limit_bytes=44 * 2**20),
+        compiler_params=pltpu.CompilerParams(vmem_limit_bytes=16 * 2**20),
         cost_estimate=pl.CostEstimate(
             flops=4 * total * width * units, bytes_accessed=4 * units * width, transcendentals=0
         ),
-        name="hidden_rows",
+        name="first_rows",
+    )(*held)
+    return out_a, out_b, (up, down)
+
+
+def more_forward(parts, weights):
+    size, width = parts[0].shape
+    units = weights[0].shape[1]
+    number = len(parts)
+    total = number * size
+    far = pl.BlockSpec(memory_space=pltpu.HBM)
+    held = list(parts)
+    held += [pltpu.with_memory_space_constraint(w, pltpu.VMEM) for w in weights]
+    return pl.pallas_call(
+        more_rows,
+        out_shape=[shaped((size, width), BF16)] * number,
+        in_specs=[pl.BlockSpec(memory_space=pl.ANY)] * number + [vmem()] * 2,
+        out_specs=[vmem()] * number,
+        scratch_shapes=[
+            pltpu.VMEM((total, width), BF16),
+            pltpu.VMEM((total, units), BF16),
+            pltpu.SemaphoreType.DMA((number,)),
+        ],
+        compiler_params=pltpu.CompilerParams(vmem_limit_bytes=24 * 2**20),
+        cost_estimate=pl.CostEstimate(
+            flops=4 * total * width * units, bytes_accessed=4 * units * width, transcendentals=0
+        ),
+        name="more_rows",
     )(*held)
 
 
@@ -425,12 +473,16 @@
     return shift(x, "tp", by, lax.axis_size("tp"))
 
 
-def reduced(far_a, far_b, right_a, right_b, left_a, left_b):
-    came_far = turn(far_a, 1), turn(far_b, -1)
+def sent_far(far_a, far_b):
+    return turn(far_a, 1), turn(far_b, -1)
+
+
+def reduced(came_far, right_a, right_b, left_a, left_b, near=False):
     came_right_b, came_left_a = turn(right_b, 1), turn(left_a, -1)
     like = [shaped(right_a.shape, BF16)] * 2
+    held = (right_a, left_b) if near else (Far(right_a), Far(left_b))
     right_sum, left_sum = call(
-        add_two, like, Far(right_a), came_far[0], Far(left_b), came_far[1], far_out=True, limit=16
+        add_two, like, held[0], came_far[0], held[1], came_far[1], far_out=not near, limit=16
     )
     came = turn(right_sum, 1), came_right_b, came_left_a, turn(left_sum, -1)
     return came, right_sum
@@ -485,7 +537,8 @@
         scratch=[pltpu.VMEM((4, rows, lanes), BF16)],
     )
     size = lax.axis_size("za")
-    near, mid, far = [shift(total, "za", d, size, wrap=False) for d in range(1, 4)]
+    near, far = [shift(total, "za", d, size, wrap=False) for d in (1, 3)]
+    mid = shift(near, "za", 1, size, wrap=False)
     found = call(
         before_each, shaped((4, rows, lanes - LANES), BF16), place, *got, near, mid, far,
         scratch=[pltpu.VMEM((4, rows, lanes), BF16), pltpu.VMEM((4, rows, lanes - LANES), BF16)],
@@ -507,7 +560,7 @@
         ],
         flops=4 * length * wide_value * width, moved=8 * 10**6, far_out=True,
     )
-    came, _ = reduced(far_a, far_b, right_a, right_b, left_a, left_b)
+    came, _ = reduced(sent_far(far_a, far_b), right_a, right_b, left_a, left_b)
     from_left_a, from_left_b, from_right_a, from_right_b = came
     own_stream = lax.dynamic_slice_in_dim(stream_in, member * portion, portion, 0)
     mid_a, mid_b, normed_a, normed_b = call(
@@ -515,15 +568,17 @@
         Far(own_a), from_left_a, from_right_a, Far(own_b), from_left_b, from_right_b,
         Far(own_stream), Far(mlp_gain[None]), far_out=True, limit=16,
     )
-    others = feed_forward(spread(normed_a, normed_b), weights)
-    came, sent = reduced(*others)
+    far_a, far_b, *others = spread(normed_a, normed_b)
+    far_a, far_b, kept = first_forward((far_a, far_b), weights)
+    came_far = sent_far(far_a, far_b)
+    came, sent = reduced(came_far, *more_forward(others, kept), near=True)
     from_left_a, from_left_b, from_right_a, from_right_b = came
     normed_a, normed_b, _ = lax.optimization_barrier((normed_a, normed_b, sent))
-    own_a, own_b = feed_forward((normed_a, normed_b), weights)
+    own_a, own_b = more_forward((normed_a, normed_b), kept)
     return call(
         last_sum, shaped((portion, width), BF16),
-        Far(own_a), from_left_a, from_right_a, Far(mid_a),
-        Far(own_b), from_left_b, from_right_b, Far(mid_b), far_out=True, limit=16,
+        own_a, from_left_a, from_right_a, Far(mid_a),
+        own_b, from_left_b, from_right_b, Far(mid_b), far_out=True, limit=16,
     )
 
 

time: 182 us -> 177 us (0.973)
  Pallas kernels: 44.7 us -> 40.3 us
    all_gather x1, waiting for transfers between devices: 10.1 us -> 19.5 us  [on_device(): weights = lax.all_gather(both, SP, axis=0, tiled=True)]
    ppermute x27, waiting for transfers between devices: 41.4 us -> 32.3 us  [shift(): return lax.ppermute(x, axis, pairs)]
    pallas_call x2 -> x3, Pallas kernels: 20.5 us -> 18.2 us  [the longest x2 9.74 us: more_forward(): pl.pallas_call(more_rows, out_shape=[shaped((size, width), BF16)] * numbe...]
    pallas_call x11, Pallas kernels: 24.1 us -> 22.1 us  [call(): pl.pallas_call(inner, out_shape=[pltpu.HBM(o.shape, o.dtype) for o in out...]
  transfers between devices with their start and end apart: 30 -> 30, of which waited for: 15 -> 14; matrix products, arithmetic and copies ran while one was open for 1% -> 1% of each run, Pallas kernels for 17% -> 22%
where the time goes in v5:
time: 177 us; the launch traced here: 176 us
  starting transfers between devices  66.3 us (37%)
  waiting for transfers between devices  53.2 us (30%)
  Pallas kernels  40.3 us (23%)
  between operations  13.7 us (8%)
  other arithmetic  2.08 us (1%)
    ppermute x27, starting transfers between devices, shift(): return lax.ppermute(x, axis, pairs)  43.2 us
    ppermute x27, waiting for transfers between devices, shift(): return lax.ppermute(x, axis, pairs)  32.3 us
    ppermute x2, starting transfers between devices, swap(): return lax.ppermute(x, 'core', [(0, 1), (1, 0)])  23.1 us
    pallas_call x11, Pallas kernels, call(): pl.pallas_call(inner, out_shape=[pltpu.HBM(o.shape, o.dtype) for o in out...  22.1 us
    all_gather x1, waiting for transfers between devices, on_device(): weights = lax.all_gather(both, SP, axis=0, tiled=True)  19.5 us
    pallas_call x2, Pallas kernels, more_forward(): pl.pallas_call(more_rows, out_shape=[shaped((size, width), BF16)] * numbe...  9.74 us
    pallas_call x1, Pallas kernels, first_forward(): pl.pallas_call(first_rows, out_shape=[pltpu.HBM((size, width), BF16)] * 2...  8.44 us
  transfers between devices with their start and end apart: 30, of which 14 were waited for; matrix products, arithmetic and copies ran while one was open for 1% of the time, Pallas kernels for 22%

profile of v5, /device:TPU:33, one launch (start us, length us, event | category | flops | bytes accessed | tf_op | source)
XLA Modules:
  0.0 176.4 jit_solution(5812234940288934154)
XLA Ops:
  6.6 2.0 %pad_maximum_fusion = bf16[64,4096]{1,0:T(8,128)(2,1)} fusion(bf16[64,2048]{1,0:T(8,128)(2,1)} %bitcast.23, bf16[64,2048]{1,0:T(8,128)(2,1)} %param.30), kind=kLoop, calls=%fused_computation | loop fusion | flops 1048576 | bytes 1048576 | tf_op jit(solution)/shard_map/concatenate | solution.py:513
  8.6 0.1 all-gather.2.cloned.1.call-update
  8.6 2.3 %own_state.1.refs_1_ = bf16[2,128,768]{2,1,0:T(8,128)(2,1)S(1)} custom-call(bf16[512,256]{1,0:T(8,128)(2,1)} %refs_1_.3, bf16[512,512]{1,0:T(8,128)(2,1)} %refs_2_.3, f32[1,512]{1,0:T(1,128)} %refs_6_.3, bf16[512,128]{1,0:T(8,128)(2,1)} %refs_5_.4, bf16[512,256]{1,0:T(8,128)(2,1)} %refs_6_.2, f32[1,512]{1,0:T(1,128)} %refs_7_.3), custom_call_target="tpu_custom_call" | custom-call | flops 134217728 | bytes 1000000 | tf_op jit(solution)/shard_map/own_state/pallas_call | solution.py:70
  10.9 20.5 %collective-permute-start = (bf16[2,128,768]{2,1,0:T(8,128)(2,1)S(1)}, bf16[2,128,768]{2,1,0:T(8,128)(2,1)S(1)}, u32[]{:S(2)}, u32[]{:S(2)}) collective-permute-start(bf16[2,128,768]{2,1,0:T(8,128)(2,1)S(1)} %own_state.1.refs_1_), channel_id=1, source_target_pairs={{0,4},{4,0},{1,5},{5,1},{2,6},{6,2},{3,7},{7,3},{8,12},{12,8},{9,1... | collective-permute-start | bytes 1179656 | tf_op jit(solution)/shard_map/ppermute | solution.py:469
  31.4 0.1 pad_add_fusion.refs_0_
  31.5 1.3 collective-permute-done.refs_2_.refs_3_
  32.8 0.9 of_chip.1
  33.7 0.1 collective-permute-start.1
  33.9 0.1 collective-permute-start.2
  34.0 3.1 %collective-permute-start.3 = (bf16[32,768]{1,0:T(8,128)(2,1)S(1)}, bf16[32,768]{1,0:T(8,128)(2,1)S(1)}, u32[]{:S(2)}, u32[]{:S(2)}) collective-permute-start(bf16[32,768]{1,0:T(8,128)(2,1)S(1)} %get-tuple-element.61), channel_id=1, source_target_pairs={{0,24},{8,0},{16,8},{24,16},{1,25},{9,1},{17,9},{25,17},{2,26},{10... | collective-permute-start | bytes 147464 | tf_op jit(solution)/shard_map/ppermute | solution.py:465
  37.1 1.5 collective-permute-done.1.refs_2_
  38.7 1.1 collective-permute-done.3.refs_4_
  39.7 0.8 of_group.1
  40.5 1.3 collective-permute-start.4
  41.8 6.5 %collective-permute-start.6 = (bf16[1,32,768]{2,1,0:T(8,128)(2,1)S(1)}, bf16[1,32,768]{2,1,0:T(8,128)(2,1)S(1)}, u32[]{:S(2)}, u32[]{:S(2)}) collective-permute-start(bf16[1,32,768]{2,1,0:T(8,128)(2,1)S(1)} %of_group.1), channel_id=1, source_target_pairs={{0,96},{1,97},{2,98},{3,99},{4,100},{5,101},{6,102},{7,103},{8,104... | collective-permute-start | bytes 147464 | tf_op jit(solution)/shard_map/ppermute | solution.py:465
  48.3 0.0 collective-permute-done.4.refs_5_
  48.3 4.2 %collective-permute-start.5 = (bf16[1,32,768]{2,1,0:T(8,128)(2,1)S(1)}, bf16[1,32,768]{2,1,0:T(8,128)(2,1)S(1)}, u32[]{:S(2)}, u32[]{:S(2)}) collective-permute-start(bf16[1,32,768]{2,1,0:T(8,128)(2,1)S(1)} %collective-permute-done.4.refs_5_), channel_id=1, source_target_pairs={{0,32},{32,64},{64,96},{1,33},{33,65},{65,97},{2,34},{34,66},{66,9... | collective-permute-start | bytes 147464 | tf_op jit(solution)/shard_map/ppermute | solution.py:465
  52.6 0.0 collective-permute-done.6.refs_7_
  52.6 2.2 %collective-permute-done.5.refs_6_ = bf16[1,32,768]{2,1,0:T(8,128)(2,1)S(1)} collective-permute-done((bf16[1,32,768]{2,1,0:T(8,128)(2,1)S(1)}, bf16[1,32,768]{2,1,0:T(8,128)(2,1)S(1)}, u32[]{:S(2)}, u32[]{:S(2)}) %collective-permute-start.5) | collective-permute-done | bytes 49184 | tf_op jit(solution)/shard_map/ppermute | solution.py:465
  54.8 0.8 before_each.1
  55.6 2.4 %collective-permute-start.7 = (bf16[32,640]{1,0:T(8,128)(2,1)S(1)}, bf16[32,640]{1,0:T(8,128)(2,1)S(1)}, u32[]{:S(2)}, u32[]{:S(2)}) collective-permute-start(bf16[32,640]{1,0:T(8,128)(2,1)S(1)} %get-tuple-element.67), channel_id=1, source_target_pairs={{0,8},{8,16},{16,24},{24,0},{1,9},{9,17},{17,25},{25,1},{2,10},{10... | collective-permute-start | bytes 122888 | tf_op jit(solution)/shard_map/ppermute | solution.py:465
  58.0 4.2 %collective-permute-start.8 = (bf16[32,640]{1,0:T(8,128)(2,1)S(1)}, bf16[32,640]{1,0:T(8,128)(2,1)S(1)}, u32[]{:S(2)}, u32[]{:S(2)}) collective-permute-start(bf16[32,640]{1,0:T(8,128)(2,1)S(1)} %get-tuple-element.66), channel_id=1, source_target_pairs={{0,16},{8,24},{16,0},{24,8},{1,17},{9,25},{17,1},{25,9},{2,18},{10... | collective-permute-start | bytes 122888 | tf_op jit(solution)/shard_map/ppermute | solution.py:465
  62.2 0.0 collective-permute-start.9
  62.2 1.7 collective-permute-done.7.refs_2_
  63.9 2.0 %collective-permute-done.8.refs_3_ = bf16[32,640]{1,0:T(8,128)(2,1)S(1)} collective-permute-done((bf16[32,640]{1,0:T(8,128)(2,1)S(1)}, bf16[32,640]{1,0:T(8,128)(2,1)S(1)}, u32[]{:S(2)}, u32[]{:S(2)}) %collective-permute-start.8) | collective-permute-done | bytes 40992 | tf_op jit(solution)/shard_map/ppermute | solution.py:465
  65.9 1.5 collective-permute-done.9.refs_4_
  67.4 0.6 gathered_half.1.refs_1_
  68.0 2.6 %collective-permute-start.10 = (bf16[128,640]{1,0:T(8,128)(2,1)S(1)}, bf16[128,640]{1,0:T(8,128)(2,1)S(1)}, u32[]{:S(2)}, u32[]{:S(2)}) collective-permute-start(bf16[128,640]{1,0:T(8,128)(2,1)S(1)} %gathered_half.1.refs_1_), channel_id=1, source_target_pairs={{0,4},{4,0},{1,5},{5,1},{2,6},{6,2},{3,7},{7,3},{8,12},{12,8},{9,1... | collective-permute-start | bytes 491528 | tf_op jit(solution)/shard_map/ppermute | solution.py:469
  70.5 2.7 %inside.1.refs_8_ = f32[512,768]{1,0:T(8,128)S(1)} custom-call(bf16[512,256]{1,0:T(8,128)(2,1)} %refs_4_.5, bf16[512,256]{1,0:T(8,128)(2,1)} %refs_1_.3, bf16[512,512]{1,0:T(8,128)(2,1)} %refs_2_.3, f32[1,512]{1,0:T(1,128)} %refs_6_.3, bf16[512,128]{1,0:T(8,128)(2,1)} %refs_5_.5, bf16[512,128]{1,0:T(8,128)(2,1)} %refs_5_.4, bf16[512,256]{1,0:T(8,128)(2,1)} %refs_6_.2, ...), custom_call_target="tpu_custom_call" | custom-call | flops 805306368 | bytes 4000000 | tf_op jit(solution)/shard_map/inside/pallas_call | solution.py:70
  73.2 0.0 collective-permute-done.10.refs_2_
  73.2 7.4 %heads_out.1 = (bf16[64,2048]{1,0:T(8,128)(2,1)}, bf16[64,2048]{1,0:T(8,128)(2,1)}, bf16[64,2048]{1,0:T(8,128)(2,1)}, bf16[64,2048]{1,0:T(8,128)(2,1)}, bf16[64,...) custom-call(s32[3]{0:T(128)S(1)} %pad_add_fusion.refs_0_, ...), custom_call_target="tpu_custom_call" | custom-call | flops 2147483648 | bytes 8000000 | tf_op jit(solution)/shard_map/heads_out/pallas_call | solution.py:70
  80.6 0.1 collective-permute-start.11
  80.7 2.7 %collective-permute-start.12 = (bf16[64,2048]{1,0:T(8,128)(2,1)}, bf16[64,2048]{1,0:T(8,128)(2,1)S(1)}, u32[]{:S(2)}, u32[]{:S(2)}) collective-permute-start(bf16[64,2048]{1,0:T(8,128)(2,1)} %get-tuple-element.37), channel_id=1, source_target_pairs={{0,3},{1,0},{2,1},{3,2},{4,7},{5,4},{6,5},{7,6},{8,11},{9,8},{10,9... | collective-permute-start | bytes 786440 | tf_op jit(solution)/shard_map/ppermute | solution.py:465
  83.4 0.0 collective-permute-start.14
  83.4 1.4 collective-permute-start.15
  84.9 5.2 %collective-permute-done.11.refs_1_ = bf16[64,2048]{1,0:T(8,128)(2,1)S(1)} collective-permute-done((bf16[64,2048]{1,0:T(8,128)(2,1)}, bf16[64,2048]{1,0:T(8,128)(2,1)S(1)}, u32[]{:S(2)}, u32[]{:S(2)}) %collective-permute-start.11) | collective-permute-done | bytes 262176 | tf_op jit(solution)/shard_map/ppermute | solution.py:465
  90.1 0.0 collective-permute-done.12.refs_3_
  90.1 2.0 %add_two.2 = (bf16[64,2048]{1,0:T(8,128)(2,1)}, bf16[64,2048]{1,0:T(8,128)(2,1)}) custom-call(bf16[64,2048]{1,0:T(8,128)(2,1)} %get-tuple-element.34.refs_0_, bf16[64,2048]{1,0:T(8,128)(2,1)S(1)} %collective-permute-done.11.refs_1_, bf16[64,2048]{1,0:T(8,128)(2,1)} %get-tuple-element.36.refs_2_, bf16[64,2048]{1,0:T(8,128)(2,1)S(1)} %collective-permute-done.12.refs_3_), custom_call_target="tpu_custom_call" | custom-call | tf_op jit(solution)/shard_map/add_two/pallas_call | solution.py:70
  92.0 0.1 collective-permute-start.13
  92.2 2.7 %collective-permute-start.16 = (bf16[64,2048]{1,0:T(8,128)(2,1)}, bf16[64,2048]{1,0:T(8,128)(2,1)S(1)}, u32[]{:S(2)}, u32[]{:S(2)}) collective-permute-start(bf16[64,2048]{1,0:T(8,128)(2,1)} %get-tuple-element.42), channel_id=1, source_target_pairs={{0,3},{1,0},{2,1},{3,2},{4,7},{5,4},{6,5},{7,6},{8,11},{9,8},{10,9... | collective-permute-start | bytes 786440 | tf_op jit(solution)/shard_map/ppermute | solution.py:465
  94.8 0.8 constant_dynamic-slice_fusion.refs_6_
  95.6 4.5 %collective-permute-done.13.refs_1_ = bf16[64,2048]{1,0:T(8,128)(2,1)S(1)} collective-permute-done((bf16[64,2048]{1,0:T(8,128)(2,1)}, bf16[64,2048]{1,0:T(8,128)(2,1)S(1)}, u32[]{:S(2)}, u32[]{:S(2)}) %collective-permute-start.13) | collective-permute-done | bytes 262176 | tf_op jit(solution)/shard_map/ppermute | solution.py:465
  100.2 2.5 %rows_mid.1 = (bf16[64,2048]{1,0:T(8,128)(2,1)}, bf16[64,2048]{1,0:T(8,128)(2,1)}, bf16[64,2048]{1,0:T(8,128)(2,1)}, bf16[64,2048]{1,0:T(8,128)(2,1)}) custom-call(bf16[64,2048]{1,0:T(8,128)(2,1)} %get-tuple-element.33.refs_0_, bf16[64,2048]{1,0:T(8,128)(2,1)S(1)} %collective-permute-done.13.refs_1_, bf16[64,2048]{1,0:T(8,128)(2,1)S(1)} %collective-permute-done.14.refs_2_, ...), custom_call_target="tpu_custom_call" | custom-call | tf_op jit(solution)/shard_map/rows_mid/pallas_call | solution.py:70
  102.7 0.2 collective-permute-start.19
  102.9 2.6 %collective-permute-start.18 = (bf16[64,2048]{1,0:T(8,128)(2,1)}, bf16[64,2048]{1,0:T(8,128)(2,1)S(1)}, u32[]{:S(2)}, u32[]{:S(2)}) collective-permute-start(bf16[64,2048]{1,0:T(8,128)(2,1)} %get-tuple-element.53.refs_1_), channel_id=1, source_target_pairs={{0,3},{1,0},{2,1},{3,2},{4,7},{5,4},{6,5},{7,6},{8,11},{9,8},{10,9... | collective-permute-start | bytes 786440 | tf_op jit(solution)/shard_map/ppermute | solution.py:465
  105.5 4.6 %collective-permute-done.19.refs_2_ = bf16[64,2048]{1,0:T(8,128)(2,1)S(1)} collective-permute-done((bf16[64,2048]{1,0:T(8,128)(2,1)}, bf16[64,2048]{1,0:T(8,128)(2,1)S(1)}, u32[]{:S(2)}, u32[]{:S(2)}) %collective-permute-start.19) | collective-permute-done | bytes 262176 | tf_op jit(solution)/shard_map/ppermute | solution.py:465
  110.2 2.7 %collective-permute-start.22 = (bf16[64,2048]{1,0:T(8,128)(2,1)S(1)}, bf16[64,2048]{1,0:T(8,128)(2,1)}, u32[]{:S(2)}, u32[]{:S(2)}) collective-permute-start(bf16[64,2048]{1,0:T(8,128)(2,1)S(1)} %collective-permute-done.18.refs_1_), channel_id=1, source_target_pairs={{0,3},{1,0},{2,1},{3,2},{4,7},{5,4},{6,5},{7,6},{8,11},{9,8},{10,9... | collective-permute-start | bytes 786440 | tf_op jit(solution)/shard_map/ppermute | solution.py:465
  112.8 0.0 collective-permute-start.17
  112.9 1.4 collective-permute-start.20
  114.3 2.3 %collective-permute-done.21.a = bf16[64,2048]{1,0:T(8,128)(2,1)S(1)} collective-permute-done((bf16[64,2048]{1,0:T(8,128)(2,1)S(1)}, bf16[64,2048]{1,0:T(8,128)(2,1)S(1)}, u32[]{:S(2)}, u32[]{:S(2)}) %collective-permute-start.21) | collective-permute-done | bytes 262176 | tf_op jit(solution)/shard_map/ppermute | solution.py:465
  116.6 19.5 %all-gather.2.cloned.1.call-done.weights = bf16[2048,4096]{1,0:T(8,128)(2,1)} async-done(((bf16[64,4096]{1,0:T(8,128)(2,1)}), bf16[2048,4096]{1,0:T(8,128)(2,1)}) %all-gather.2.cloned.1.call-update) | async-done | bytes 16777232 | tf_op jit(solution)/shard_map/all_gather | solution.py:514
  136.1 8.4 %first_rows.1 = (bf16[64,2048]{1,0:T(8,128)(2,1)}, bf16[64,2048]{1,0:T(8,128)(2,1)}, bf16[2048,2048]{1,0:T(8,128)(2,1)S(1)}, bf16[2048,2048]{1,0:T(8,128)(2,1)S(1)}) custom-call(bf16[64,2048]{1,0:T(8,128)(2,1)} %copy-done.3, bf16[64,2048]{1,0:T(8,128)(2,1)} %collective-permute-done.22.b, bf16[2048,4096]{1,0:T(8,128)(2,1)} %all-gather.2.cloned.1.call-done.weights), custom_call_target="tpu_custom_call" | custom-call | flops 2147483648 | bytes 16777216 | tf_op jit(solution)/shard_map/first_rows/pallas_call | solution.py:405
  144.5 0.9 collective-permute-start.23
  145.5 1.9 %collective-permute-start.24 = (bf16[64,2048]{1,0:T(8,128)(2,1)}, bf16[64,2048]{1,0:T(8,128)(2,1)S(1)}, u32[]{:S(2)}, u32[]{:S(2)}) collective-permute-start(bf16[64,2048]{1,0:T(8,128)(2,1)} %get-tuple-element.50), channel_id=1, source_target_pairs={{0,3},{1,0},{2,1},{3,2},{4,7},{5,4},{6,5},{7,6},{8,11},{9,8},{10,9... | collective-permute-start | bytes 786440 | tf_op jit(solution)/shard_map/ppermute | solution.py:465
  147.4 5.2 %more_rows.2 = (bf16[64,2048]{1,0:T(8,128)(2,1)S(1)}, bf16[64,2048]{1,0:T(8,128)(2,1)S(1)}, bf16[64,2048]{1,0:T(8,128)(2,1)S(1)}, bf16[64,2048]{1,0:T(8,128)(2,1)S(1)}) custom-call(bf16[64,2048]{1,0:T(8,128)(2,1)S(1)} %collective-permute-done.17.refs_0_, bf16[64,2048]{1,0:T(8,128)(2,1)S(1)} %collective-permute-done.18.refs_1_, ...), custom_call_target="tpu_custom_call" | custom-call | flops 4294967296 | bytes 16777216 | tf_op jit(solution)/shard_map/more_rows/pallas_call | solution.py:435
  152.6 1.2 collective-permute-start.26
  153.8 0.4 collective-permute-start.27
  154.2 0.1 add_two.3
  154.3 0.3 collective-permute-start.25
  154.6 2.5 %collective-permute-start.28 = (bf16[64,2048]{1,0:T(8,128)(2,1)S(1)}, bf16[64,2048]{1,0:T(8,128)(2,1)S(1)}, u32[]{:S(2)}, u32[]{:S(2)}) collective-permute-start(bf16[64,2048]{1,0:T(8,128)(2,1)S(1)} %get-tuple-element.59), channel_id=1, source_target_pairs={{0,3},{1,0},{2,1},{3,2},{4,7},{5,4},{6,5},{7,6},{8,11},{9,8},{10,9... | collective-permute-start | bytes 786440 | tf_op jit(solution)/shard_map/ppermute | solution.py:465
  157.1 4.5 %more_rows.3 = (bf16[64,2048]{1,0:T(8,128)(2,1)S(1)}, bf16[64,2048]{1,0:T(8,128)(2,1)S(1)}) custom-call(bf16[64,2048]{1,0:T(8,128)(2,1)S(1)} %copy-done.1, bf16[64,2048]{1,0:T(8,128)(2,1)S(1)} %copy-done.2, bf16[2048,2048]{1,0:T(8,128)(2,1)S(1)} %get-tuple-element.45.refs_4_.refs_2_, bf16[2048,2048]{1,0:T(8,128)(2,1)S(1)} %get-tuple-element.46.refs_5_.refs_3_), custom_call_target="tpu_custom_call" | custom-call | flops 2147483648 | bytes 16777216 | tf_op jit(solution)/shard_map/more_rows/pallas_call | solution.py:435
  161.6 0.1 collective-permute-done.27.refs_5_
  161.7 5.6 %collective-permute-done.25.refs_1_ = bf16[64,2048]{1,0:T(8,128)(2,1)S(1)} collective-permute-done((bf16[64,2048]{1,0:T(8,128)(2,1)S(1)}, bf16[64,2048]{1,0:T(8,128)(2,1)S(1)}, u32[]{:S(2)}, u32[]{:S(2)}) %collective-permute-start.25) | collective-permute-done | bytes 262176 | tf_op jit(solution)/shard_map/ppermute | solution.py:465
  167.4 2.1 %last_sum.1 = bf16[128,2048]{1,0:T(8,128)(2,1)} custom-call(bf16[64,2048]{1,0:T(8,128)(2,1)S(1)} %get-tuple-element.54.refs_0_, bf16[64,2048]{1,0:T(8,128)(2,1)S(1)} %collective-permute-done.25.refs_1_, bf16[64,2048]{1,0:T(8,128)(2,1)S(1)} %collective-permute-done.26.refs_2_, bf16[64,2048]{1,0:T(8,128)(2,1)} %get-tuple-element.56.refs_3_, ...), custom_call_target="tpu_custom_call" | custom-call | tf_op jit(solution)/shard_map/last_sum/pallas_call | solution.py:70
  (24 shorter events, 0.1 us)
Async XLA Ops:
  6.5 88.3 %copy-start = (bf16[512,2048]{1,0:T(8,128)(2,1)S(1)}, bf16[512,2048]{1,0:T(8,128)(2,1)}, u32[]{:S(2)}) copy-start(bf16[512,2048]{1,0:T(8,128)(2,1)} %param.16) | copy-start | bytes 6291460
  6.6 129.5 %all-gather.2.cloned.1.call-start = ((), (), s32[]{:S(2)}) async-start(), calls=%async_computation | async-start | bytes 17301504 | tf_op jit(solution)/shard_map/all_gather | solution.py:514
  10.9 21.9 %collective-permute-start = (bf16[2,128,768]{2,1,0:T(8,128)(2,1)S(1)}, bf16[2,128,768]{2,1,0:T(8,128)(2,1)S(1)}, u32[]{:S(2)}, u32[]{:S(2)}) collective-permute-start(bf16[2,128,768]{2,1,0:T(8,128)(2,1)S(1)} %own_state.1.refs_1_), channel_id=1, source_target_pairs={{0,4},{4,0},{1,5},{5,1},{2,6},{6,2},{3,7},{7,3},{8,12},{12,8},{9,1... | collective-permute-start | bytes 1179656 | tf_op jit(solution)/shard_map/ppermute | solution.py:469
  33.7 4.9 %collective-permute-start.1 = (bf16[32,768]{1,0:T(8,128)(2,1)S(1)}, bf16[32,768]{1,0:T(8,128)(2,1)S(1)}, u32[]{:S(2)}, u32[]{:S(2)}) collective-permute-start(bf16[32,768]{1,0:T(8,128)(2,1)S(1)} %get-tuple-element.63), channel_id=1, source_target_pairs={{0,8},{8,16},{16,24},{24,0},{1,9},{9,17},{17,25},{25,1},{2,10},{10... | collective-permute-start | bytes 147464 | tf_op jit(solution)/shard_map/ppermute | solution.py:465
  33.9 4.8 %collective-permute-start.2 = (bf16[32,768]{1,0:T(8,128)(2,1)S(1)}, bf16[32,768]{1,0:T(8,128)(2,1)S(1)}, u32[]{:S(2)}, u32[]{:S(2)}) collective-permute-start(bf16[32,768]{1,0:T(8,128)(2,1)S(1)} %get-tuple-element.62), channel_id=1, source_target_pairs={{0,16},{8,24},{16,0},{24,8},{1,17},{9,25},{17,1},{25,9},{2,18},{10... | collective-permute-start | bytes 147464 | tf_op jit(solution)/shard_map/ppermute | solution.py:465
  34.0 5.7 %collective-permute-start.3 = (bf16[32,768]{1,0:T(8,128)(2,1)S(1)}, bf16[32,768]{1,0:T(8,128)(2,1)S(1)}, u32[]{:S(2)}, u32[]{:S(2)}) collective-permute-start(bf16[32,768]{1,0:T(8,128)(2,1)S(1)} %get-tuple-element.61), channel_id=1, source_target_pairs={{0,24},{8,0},{16,8},{24,16},{1,25},{9,1},{17,9},{25,17},{2,26},{10... | collective-permute-start | bytes 147464 | tf_op jit(solution)/shard_map/ppermute | solution.py:465
  40.5 7.8 %collective-permute-start.4 = (bf16[1,32,768]{2,1,0:T(8,128)(2,1)S(1)}, bf16[1,32,768]{2,1,0:T(8,128)(2,1)S(1)}, u32[]{:S(2)}, u32[]{:S(2)}) collective-permute-start(bf16[1,32,768]{2,1,0:T(8,128)(2,1)S(1)} %of_group.1), channel_id=1, source_target_pairs={{0,32},{32,64},{64,96},{1,33},{33,65},{65,97},{2,34},{34,66},{66,9... | collective-permute-start | bytes 147464 | tf_op jit(solution)/shard_map/ppermute | solution.py:465
  41.8 10.8 %collective-permute-start.6 = (bf16[1,32,768]{2,1,0:T(8,128)(2,1)S(1)}, bf16[1,32,768]{2,1,0:T(8,128)(2,1)S(1)}, u32[]{:S(2)}, u32[]{:S(2)}) collective-permute-start(bf16[1,32,768]{2,1,0:T(8,128)(2,1)S(1)} %of_group.1), channel_id=1, source_target_pairs={{0,96},{1,97},{2,98},{3,99},{4,100},{5,101},{6,102},{7,103},{8,104... | collective-permute-start | bytes 147464 | tf_op jit(solution)/shard_map/ppermute | solution.py:465
  48.3 6.4 %collective-permute-start.5 = (bf16[1,32,768]{2,1,0:T(8,128)(2,1)S(1)}, bf16[1,32,768]{2,1,0:T(8,128)(2,1)S(1)}, u32[]{:S(2)}, u32[]{:S(2)}) collective-permute-start(bf16[1,32,768]{2,1,0:T(8,128)(2,1)S(1)} %collective-permute-done.4.refs_5_), channel_id=1, source_target_pairs={{0,32},{32,64},{64,96},{1,33},{33,65},{65,97},{2,34},{34,66},{66,9... | collective-permute-start | bytes 147464 | tf_op jit(solution)/shard_map/ppermute | solution.py:465
  55.6 8.3 %collective-permute-start.7 = (bf16[32,640]{1,0:T(8,128)(2,1)S(1)}, bf16[32,640]{1,0:T(8,128)(2,1)S(1)}, u32[]{:S(2)}, u32[]{:S(2)}) collective-permute-start(bf16[32,640]{1,0:T(8,128)(2,1)S(1)} %get-tuple-element.67), channel_id=1, source_target_pairs={{0,8},{8,16},{16,24},{24,0},{1,9},{9,17},{17,25},{25,1},{2,10},{10... | collective-permute-start | bytes 122888 | tf_op jit(solution)/shard_map/ppermute | solution.py:465
  58.0 7.9 %collective-permute-start.8 = (bf16[32,640]{1,0:T(8,128)(2,1)S(1)}, bf16[32,640]{1,0:T(8,128)(2,1)S(1)}, u32[]{:S(2)}, u32[]{:S(2)}) collective-permute-start(bf16[32,640]{1,0:T(8,128)(2,1)S(1)} %get-tuple-element.66), channel_id=1, source_target_pairs={{0,16},{8,24},{16,0},{24,8},{1,17},{9,25},{17,1},{25,9},{2,18},{10... | collective-permute-start | bytes 122888 | tf_op jit(solution)/shard_map/ppermute | solution.py:465
  62.2 5.1 %collective-permute-start.9 = (bf16[32,640]{1,0:T(8,128)(2,1)S(1)}, bf16[32,640]{1,0:T(8,128)(2,1)S(1)}, u32[]{:S(2)}, u32[]{:S(2)}) collective-permute-start(bf16[32,640]{1,0:T(8,128)(2,1)S(1)} %get-tuple-element.65), channel_id=1, source_target_pairs={{0,24},{8,0},{16,8},{24,16},{1,25},{9,1},{17,9},{25,17},{2,26},{10... | collective-permute-start | bytes 122888 | tf_op jit(solution)/shard_map/ppermute | solution.py:465
  68.0 5.3 %collective-permute-start.10 = (bf16[128,640]{1,0:T(8,128)(2,1)S(1)}, bf16[128,640]{1,0:T(8,128)(2,1)S(1)}, u32[]{:S(2)}, u32[]{:S(2)}) collective-permute-start(bf16[128,640]{1,0:T(8,128)(2,1)S(1)} %gathered_half.1.refs_1_), channel_id=1, source_target_pairs={{0,4},{4,0},{1,5},{5,1},{2,6},{6,2},{3,7},{7,3},{8,12},{12,8},{9,1... | collective-permute-start | bytes 491528 | tf_op jit(solution)/shard_map/ppermute | solution.py:469
  80.6 9.4 %collective-permute-start.11 = (bf16[64,2048]{1,0:T(8,128)(2,1)}, bf16[64,2048]{1,0:T(8,128)(2,1)S(1)}, u32[]{:S(2)}, u32[]{:S(2)}) collective-permute-start(bf16[64,2048]{1,0:T(8,128)(2,1)} %get-tuple-element.35), channel_id=1, source_target_pairs={{0,1},{1,2},{2,3},{3,0},{4,5},{5,6},{6,7},{7,4},{8,9},{9,10},{10,1... | collective-permute-start | bytes 786440 | tf_op jit(solution)/shard_map/ppermute | solution.py:465
  80.7 9.3 %collective-permute-start.12 = (bf16[64,2048]{1,0:T(8,128)(2,1)}, bf16[64,2048]{1,0:T(8,128)(2,1)S(1)}, u32[]{:S(2)}, u32[]{:S(2)}) collective-permute-start(bf16[64,2048]{1,0:T(8,128)(2,1)} %get-tuple-element.37), channel_id=1, source_target_pairs={{0,3},{1,0},{2,1},{3,2},{4,7},{5,4},{6,5},{7,6},{8,11},{9,8},{10,9... | collective-permute-start | bytes 786440 | tf_op jit(solution)/shard_map/ppermute | solution.py:465
  83.4 12.2 %collective-permute-start.14 = (bf16[64,2048]{1,0:T(8,128)(2,1)}, bf16[64,2048]{1,0:T(8,128)(2,1)S(1)}, u32[]{:S(2)}, u32[]{:S(2)}) collective-permute-start(bf16[64,2048]{1,0:T(8,128)(2,1)} %get-tuple-element.39), channel_id=1, source_target_pairs={{0,3},{1,0},{2,1},{3,2},{4,7},{5,4},{6,5},{7,6},{8,11},{9,8},{10,9... | collective-permute-start | bytes 786440 | tf_op jit(solution)/shard_map/ppermute | solution.py:465
  83.4 12.2 %collective-permute-start.15 = (bf16[64,2048]{1,0:T(8,128)(2,1)}, bf16[64,2048]{1,0:T(8,128)(2,1)S(1)}, u32[]{:S(2)}, u32[]{:S(2)}) collective-permute-start(bf16[64,2048]{1,0:T(8,128)(2,1)} %get-tuple-element.41), channel_id=1, source_target_pairs={{0,1},{1,2},{2,3},{3,0},{4,5},{5,6},{6,7},{7,4},{8,9},{9,10},{10,1... | collective-permute-start | bytes 786440 | tf_op jit(solution)/shard_map/ppermute | solution.py:465
  92.0 8.2 %collective-permute-start.13 = (bf16[64,2048]{1,0:T(8,128)(2,1)}, bf16[64,2048]{1,0:T(8,128)(2,1)S(1)}, u32[]{:S(2)}, u32[]{:S(2)}) collective-permute-start(bf16[64,2048]{1,0:T(8,128)(2,1)} %get-tuple-element.38), channel_id=1, source_target_pairs={{0,1},{1,2},{2,3},{3,0},{4,5},{5,6},{6,7},{7,4},{8,9},{9,10},{10,1... | collective-permute-start | bytes 786440 | tf_op jit(solution)/shard_map/ppermute | solution.py:465
  92.2 8.0 %collective-permute-start.16 = (bf16[64,2048]{1,0:T(8,128)(2,1)}, bf16[64,2048]{1,0:T(8,128)(2,1)S(1)}, u32[]{:S(2)}, u32[]{:S(2)}) collective-permute-start(bf16[64,2048]{1,0:T(8,128)(2,1)} %get-tuple-element.42), channel_id=1, source_target_pairs={{0,3},{1,0},{2,1},{3,2},{4,7},{5,4},{6,5},{7,6},{8,11},{9,8},{10,9... | collective-permute-start | bytes 786440 | tf_op jit(solution)/shard_map/ppermute | solution.py:465
  102.7 7.4 %collective-permute-start.19 = (bf16[64,2048]{1,0:T(8,128)(2,1)}, bf16[64,2048]{1,0:T(8,128)(2,1)S(1)}, u32[]{:S(2)}, u32[]{:S(2)}) collective-permute-start(bf16[64,2048]{1,0:T(8,128)(2,1)} %get-tuple-element.52.refs_0_), channel_id=1, source_target_pairs={{0,1},{1,2},{2,3},{3,0},{4,5},{5,6},{6,7},{7,4},{8,9},{9,10},{10,1... | collective-permute-start | bytes 786440 | tf_op jit(solution)/shard_map/ppermute | solution.py:465
  102.9 7.2 %collective-permute-start.18 = (bf16[64,2048]{1,0:T(8,128)(2,1)}, bf16[64,2048]{1,0:T(8,128)(2,1)S(1)}, u32[]{:S(2)}, u32[]{:S(2)}) collective-permute-start(bf16[64,2048]{1,0:T(8,128)(2,1)} %get-tuple-element.53.refs_1_), channel_id=1, source_target_pairs={{0,3},{1,0},{2,1},{3,2},{4,7},{5,4},{6,5},{7,6},{8,11},{9,8},{10,9... | collective-permute-start | bytes 786440 | tf_op jit(solution)/shard_map/ppermute | solution.py:465
  110.2 6.4 %collective-permute-start.21 = (bf16[64,2048]{1,0:T(8,128)(2,1)S(1)}, bf16[64,2048]{1,0:T(8,128)(2,1)S(1)}, u32[]{:S(2)}, u32[]{:S(2)}) collective-permute-start(bf16[64,2048]{1,0:T(8,128)(2,1)S(1)} %collective-permute-done.19.refs_2_), channel_id=1, source_target_pairs={{0,1},{1,2},{2,3},{3,0},{4,5},{5,6},{6,7},{7,4},{8,9},{9,10},{10,1... | collective-permute-start | bytes 786440 | tf_op jit(solution)/shard_map/ppermute | solution.py:465
  110.2 6.4 %collective-permute-start.22 = (bf16[64,2048]{1,0:T(8,128)(2,1)S(1)}, bf16[64,2048]{1,0:T(8,128)(2,1)}, u32[]{:S(2)}, u32[]{:S(2)}) collective-permute-start(bf16[64,2048]{1,0:T(8,128)(2,1)S(1)} %collective-permute-done.18.refs_1_), channel_id=1, source_target_pairs={{0,3},{1,0},{2,1},{3,2},{4,7},{5,4},{6,5},{7,6},{8,11},{9,8},{10,9... | collective-permute-start | bytes 786440 | tf_op jit(solution)/shard_map/ppermute | solution.py:465
  112.8 34.5 %collective-permute-start.17 = (bf16[64,2048]{1,0:T(8,128)(2,1)}, bf16[64,2048]{1,0:T(8,128)(2,1)S(1)}, u32[]{:S(2)}, u32[]{:S(2)}) collective-permute-start(bf16[64,2048]{1,0:T(8,128)(2,1)} %get-tuple-element.52.refs_0_), channel_id=1, source_target_pairs={{0,3},{1,0},{2,1},{3,2},{4,7},{5,4},{6,5},{7,6},{8,11},{9,8},{10,9... | collective-permute-start | bytes 786440 | tf_op jit(solution)/shard_map/ppermute | solution.py:465
  112.9 34.5 %collective-permute-start.20 = (bf16[64,2048]{1,0:T(8,128)(2,1)}, bf16[64,2048]{1,0:T(8,128)(2,1)S(1)}, u32[]{:S(2)}, u32[]{:S(2)}) collective-permute-start(bf16[64,2048]{1,0:T(8,128)(2,1)} %get-tuple-element.53.refs_1_), channel_id=1, source_target_pairs={{0,1},{1,2},{2,3},{3,0},{4,5},{5,6},{6,7},{7,4},{8,9},{9,10},{10,1... | collective-permute-start | bytes 786440 | tf_op jit(solution)/shard_map/ppermute | solution.py:465
  116.6 19.5 %copy-start.3 = (bf16[64,2048]{1,0:T(8,128)(2,1)}, bf16[64,2048]{1,0:T(8,128)(2,1)S(1)}, u32[]{:S(2)}) copy-start(bf16[64,2048]{1,0:T(8,128)(2,1)S(1)} %collective-permute-done.21.a) | copy-start | bytes 786436
  144.5 9.6 %collective-permute-start.23 = (bf16[64,2048]{1,0:T(8,128)(2,1)}, bf16[64,2048]{1,0:T(8,128)(2,1)S(1)}, u32[]{:S(2)}, u32[]{:S(2)}) collective-permute-start(bf16[64,2048]{1,0:T(8,128)(2,1)} %get-tuple-element.48), channel_id=1, source_target_pairs={{0,1},{1,2},{2,3},{3,0},{4,5},{5,6},{6,7},{7,4},{8,9},{9,10},{10,1... | collective-permute-start | bytes 786440 | tf_op jit(solution)/shard_map/ppermute | solution.py:465
  145.5 8.7 %collective-permute-start.24 = (bf16[64,2048]{1,0:T(8,128)(2,1)}, bf16[64,2048]{1,0:T(8,128)(2,1)S(1)}, u32[]{:S(2)}, u32[]{:S(2)}) collective-permute-start(bf16[64,2048]{1,0:T(8,128)(2,1)} %get-tuple-element.50), channel_id=1, source_target_pairs={{0,3},{1,0},{2,1},{3,2},{4,7},{5,4},{6,5},{7,6},{8,11},{9,8},{10,9... | collective-permute-start | bytes 786440 | tf_op jit(solution)/shard_map/ppermute | solution.py:465
  147.3 9.8 %copy-start.1 = (bf16[64,2048]{1,0:T(8,128)(2,1)S(1)}, bf16[64,2048]{1,0:T(8,128)(2,1)}, u32[]{:S(2)}) copy-start(bf16[64,2048]{1,0:T(8,128)(2,1)} %get-tuple-element.52.refs_0_) | copy-start | bytes 786436
  147.3 9.8 %copy-start.2 = (bf16[64,2048]{1,0:T(8,128)(2,1)S(1)}, bf16[64,2048]{1,0:T(8,128)(2,1)}, u32[]{:S(2)}) copy-start(bf16[64,2048]{1,0:T(8,128)(2,1)} %get-tuple-element.53.refs_1_) | copy-start | bytes 786436
  152.6 9.1 %collective-permute-start.26 = (bf16[64,2048]{1,0:T(8,128)(2,1)S(1)}, bf16[64,2048]{1,0:T(8,128)(2,1)S(1)}, u32[]{:S(2)}, u32[]{:S(2)}) collective-permute-start(bf16[64,2048]{1,0:T(8,128)(2,1)S(1)} %get-tuple-element.55), channel_id=1, source_target_pairs={{0,3},{1,0},{2,1},{3,2},{4,7},{5,4},{6,5},{7,6},{8,11},{9,8},{10,9... | collective-permute-start | bytes 786440 | tf_op jit(solution)/shard_map/ppermute | solution.py:465
  153.8 8.0 %collective-permute-start.27 = (bf16[64,2048]{1,0:T(8,128)(2,1)S(1)}, bf16[64,2048]{1,0:T(8,128)(2,1)S(1)}, u32[]{:S(2)}, u32[]{:S(2)}) collective-permute-start(bf16[64,2048]{1,0:T(8,128)(2,1)S(1)} %get-tuple-element.58), channel_id=1, source_target_pairs={{0,1},{1,2},{2,3},{3,0},{4,5},{5,6},{6,7},{7,4},{8,9},{9,10},{10,1... | collective-permute-start | bytes 786440 | tf_op jit(solution)/shard_map/ppermute | solution.py:465
  154.3 13.1 %collective-permute-start.25 = (bf16[64,2048]{1,0:T(8,128)(2,1)S(1)}, bf16[64,2048]{1,0:T(8,128)(2,1)S(1)}, u32[]{:S(2)}, u32[]{:S(2)}) collective-permute-start(bf16[64,2048]{1,0:T(8,128)(2,1)S(1)} %get-tuple-element.51), channel_id=1, source_target_pairs={{0,1},{1,2},{2,3},{3,0},{4,5},{5,6},{6,7},{7,4},{8,9},{9,10},{10,1... | collective-permute-start | bytes 786440 | tf_op jit(solution)/shard_map/ppermute | solution.py:465
  154.6 12.8 %collective-permute-start.28 = (bf16[64,2048]{1,0:T(8,128)(2,1)S(1)}, bf16[64,2048]{1,0:T(8,128)(2,1)S(1)}, u32[]{:S(2)}, u32[]{:S(2)}) collective-permute-start(bf16[64,2048]{1,0:T(8,128)(2,1)S(1)} %get-tuple-element.59), channel_id=1, source_target_pairs={{0,3},{1,0},{2,1},{3,2},{4,7},{5,4},{6,5},{7,6},{8,11},{9,8},{10,9... | collective-permute-start | bytes 786440 | tf_op jit(solution)/shard_map/ppermute | solution.py:465
Sparse Core Ops, SparseCore 0:
  9.2 126.8 all-gather.1

commit v6 on v5

--- a/solution.py
+++ b/solution.py
@@ -332,9 +332,11 @@
     return (raised * raised).astype(BF16)
 
 
-def first_rows(
-    a, b, weights, out_a, out_b, up, down, rows, total, hidden, row_sems, up_sems, down_sems
-):
+def first_rows(*refs):
+    *ends, up, down, rows, total, hidden, row_sems, up_sems, down_sems = refs
+    number = len(ends) // 2
+    parts, weights, outs = ends[:number], ends[number], ends[number + 1 :]
+    size = parts[0].shape[0]
     units, block = up.shape[1], 512
     count = up.shape[0] // block
 
@@ -343,7 +345,7 @@
         source = weights.at[span, pl.ds(column * units, units)]
         return pltpu.make_async_copy(source, to.at[span, :], sems.at[k])
 
-    copies = fetched(list(zip((a, b), stacked((a, b), rows))), row_sems)
+    copies = fetched(list(zip(parts, stacked(parts, rows))), row_sems)
 
     @pl.loop(0, count)
     def _(k):
@@ -369,10 +371,9 @@
     def _(k):
         fetch(k, 1, down, down_sems).wait()
         span = pl.ds(pl.multiple_of(k * block, block), block)
-        rows[:, span] = mm(hidden[...], down[span, :], ((1,), (1,))).astype(BF16)
-
-    for copy in fetched(list(zip(stacked((a, b), rows), (out_a, out_b))), row_sems):
-        copy.wait()
+        done = mm(hidden[...], down[span, :], ((1,), (1,))).astype(BF16)
+        for m, out in enumerate(outs):
+            out[:, span] = done[m * size : (m + 1) * size]
 
 
 def more_rows(*refs):
@@ -399,29 +400,31 @@
 def first_forward(parts, weights):
     size, width = parts[0].shape
     units = weights.shape[1] // 2
-    count, total = width // 512, 2 * size
+    number = len(parts)
+    count, total = width // 512, number * size
     far = pl.BlockSpec(memory_space=pltpu.HBM)
     held = [pltpu.with_memory_space_constraint(p, pltpu.HBM) for p in (*parts, weights)]
-    out_a, out_b, up, down = pl.pallas_call(
+    *done, up, down = pl.pallas_call(
         first_rows,
-        out_shape=[pltpu.HBM((size, width), BF16)] * 2 + [pltpu.VMEM((width, units), BF16)] * 2,
-        in_specs=[far] * 3,
-        out_specs=[far] * 2 + [vmem()] * 2,
+        out_shape=[pltpu.VMEM((size, width), BF16)] * number
+        + [pltpu.VMEM((width, units), BF16)] * 2,
+        in_specs=[far] * (number + 1),
+        out_specs=[vmem()] * (number + 2),
         scratch_shapes=[
             pltpu.VMEM((total, width), BF16),
             pltpu.VMEM((total, units), F32),
             pltpu.VMEM((total, units), BF16),
-            pltpu.SemaphoreType.DMA((2,)),
+            pltpu.SemaphoreType.DMA((number,)),
             pltpu.SemaphoreType.DMA((count,)),
             pltpu.SemaphoreType.DMA((count,)),
         ],
-        compiler_params=pltpu.CompilerParams(vmem_limit_bytes=16 * 2**20),
+        compiler_params=pltpu.CompilerParams(vmem_limit_bytes=20 * 2**20),
         cost_estimate=pl.CostEstimate(
             flops=4 * total * width * units, bytes_accessed=4 * units * width, transcendentals=0
         ),
         name="first_rows",
     )(*held)
-    return out_a, out_b, (up, down)
+    return done, (up, down)
 
 
 def more_forward(parts, weights):
@@ -450,13 +453,15 @@
     )(*held)
 
 
-def last_sum(own_a, left_a, right_a, mid_a, own_b, left_b, right_b, mid_b, out):
-    rows = own_a.shape[0]
-    halves = ((own_a, left_a, right_a, mid_a), (own_b, left_b, right_b, mid_b))
-    for n, parts in enumerate(halves):
-        total = parts[3][...].astype(F32)
-        for part in parts[:3]:
-            total = total + part[...].astype(F32)
+def with_middle(own_a, mid_a, own_b, mid_b, sum_a, sum_b):
+    sum_a[...] = own_a[...].astype(F32) + mid_a[...].astype(F32)
+    sum_b[...] = own_b[...].astype(F32) + mid_b[...].astype(F32)
+
+
+def last_sum(sum_a, left_a, right_a, sum_b, left_b, right_b, out):
+    rows = sum_a.shape[0]
+    for n, parts in enumerate(((sum_a, left_a, right_a), (sum_b, left_b, right_b))):
+        total = parts[0][...] + parts[1][...].astype(F32) + parts[2][...].astype(F32)
         out[n * rows : (n + 1) * rows] = total.astype(BF16)
 
 
@@ -477,14 +482,17 @@
     return turn(far_a, 1), turn(far_b, -1)
 
 
-def reduced(came_far, right_a, right_b, left_a, left_b, near=False):
-    came_right_b, came_left_a = turn(right_b, 1), turn(left_a, -1)
+def sent_plain(right_b, left_a):
+    return turn(right_b, 1), turn(left_a, -1)
+
+
+def reduced(came_far, came_plain, right_a, left_b, near=False):
     like = [shaped(right_a.shape, BF16)] * 2
     held = (right_a, left_b) if near else (Far(right_a), Far(left_b))
     right_sum, left_sum = call(
         add_two, like, held[0], came_far[0], held[1], came_far[1], far_out=not near, limit=16
     )
-    came = turn(right_sum, 1), came_right_b, came_left_a, turn(left_sum, -1)
+    came = turn(right_sum, 1), *came_plain, turn(left_sum, -1)
     return came, right_sum
 
 
@@ -560,7 +568,8 @@
         ],
         flops=4 * length * wide_value * width, moved=8 * 10**6, far_out=True,
     )
-    came, _ = reduced(sent_far(far_a, far_b), right_a, right_b, left_a, left_b)
+    came_far = sent_far(far_a, far_b)
+    came, _ = reduced(came_far, sent_plain(right_b, left_a), right_a, left_b)
     from_left_a, from_left_b, from_right_a, from_right_b = came
     own_stream = lax.dynamic_slice_in_dim(stream_in, member * portion, portion, 0)
     mid_a, mid_b, normed_a, normed_b = call(
@@ -568,17 +577,22 @@
         Far(own_a), from_left_a, from_right_a, Far(own_b), from_left_b, from_right_b,
         Far(own_stream), Far(mlp_gain[None]), far_out=True, limit=16,
     )
-    far_a, far_b, *others = spread(normed_a, normed_b)
-    far_a, far_b, kept = first_forward((far_a, far_b), weights)
+    far_a, far_b, right_a, right_b, left_a, left_b = spread(normed_a, normed_b)
+    done, kept = first_forward((far_a, far_b, right_b, left_a), weights)
+    far_a, far_b, right_b, left_a = done
     came_far = sent_far(far_a, far_b)
-    came, sent = reduced(came_far, *more_forward(others, kept), near=True)
+    came_plain = sent_plain(right_b, left_a)
+    right_a, left_b = more_forward((right_a, left_b), kept)
+    came, sent = reduced(came_far, came_plain, right_a, left_b, near=True)
     from_left_a, from_left_b, from_right_a, from_right_b = came
     normed_a, normed_b, _ = lax.optimization_barrier((normed_a, normed_b, sent))
     own_a, own_b = more_forward((normed_a, normed_b), kept)
+    sum_a, sum_b = call(
+        with_middle, [shaped(mid_a.shape, F32)] * 2, own_a, Far(mid_a), own_b, Far(mid_b), limit=16
+    )
     return call(
         last_sum, shaped((portion, width), BF16),
-        own_a, from_left_a, from_right_a, Far(mid_a),
-        own_b, from_left_b, from_right_b, Far(mid_b), far_out=True, limit=16,
+        sum_a, from_left_a, from_right_a, sum_b, from_left_b, from_right_b, far_out=True, limit=16,
     )
 
 

time: 177 us -> 172 us (0.972)
  waiting for transfers between devices: 53.2 us -> 49.9 us
    ppermute x27, waiting for transfers between devices: 32.3 us -> 29.8 us  [shift(): return lax.ppermute(x, axis, pairs)]
    pallas_call x11 -> x12, Pallas kernels: 22.1 us -> 22.1 us  [call(): pl.pallas_call(inner, out_shape=[pltpu.HBM(o.shape, o.dtype) for o in out...]
where the time goes in v6:
time: 172 us
  starting transfers between devices  66.2 us (38%)
  waiting for transfers between devices  49.9 us (29%)
  Pallas kernels  39.2 us (23%)
  between operations  13.7 us (8%)
  other arithmetic  2.09 us (1%)
    ppermute x27, starting transfers between devices, shift(): return lax.ppermute(x, axis, pairs)  43 us
    ppermute x27, waiting for transfers between devices, shift(): return lax.ppermute(x, axis, pairs)  29.8 us
    ppermute x2, starting transfers between devices, swap(): return lax.ppermute(x, 'core', [(0, 1), (1, 0)])  23.1 us
    pallas_call x12, Pallas kernels, call(): pl.pallas_call(inner, out_shape=[pltpu.HBM(o.shape, o.dtype) for o in out...  22.1 us
    all_gather x1, waiting for transfers between devices, on_device(): weights = lax.all_gather(both, SP, axis=0, tiled=True)  18.8 us
    pallas_call x2, Pallas kernels, more_forward(): pl.pallas_call(more_rows, out_shape=[shaped((size, width), BF16)] * numbe...  9.05 us
    pallas_call x1, Pallas kernels, first_forward(): pl.pallas_call(first_rows, out_shape=[pltpu.VMEM((size, width), BF16)] *...  8.04 us
  transfers between devices with their start and end apart: 30, of which 14 were waited for; matrix products, arithmetic and copies ran while one was open for 1% of the time, Pallas kernels for 22%

profile of v6, /device:TPU:33, one launch (start us, length us, event | category | flops | bytes accessed | tf_op | source)
XLA Modules:
  0.0 171.9 jit_solution(15901325244964836497)
XLA Ops:
  6.6 2.0 %pad_maximum_fusion = bf16[64,4096]{1,0:T(8,128)(2,1)} fusion(bf16[64,2048]{1,0:T(8,128)(2,1)} %bitcast.23, bf16[64,2048]{1,0:T(8,128)(2,1)} %param.30), kind=kLoop, calls=%fused_computation | loop fusion | flops 1048576 | bytes 1048576 | tf_op jit(solution)/shard_map/concatenate | solution.py:521
  8.6 0.1 all-gather.2.cloned.1.call-update
  8.6 2.3 %own_state.1.refs_1_ = bf16[2,128,768]{2,1,0:T(8,128)(2,1)S(1)} custom-call(bf16[512,256]{1,0:T(8,128)(2,1)} %refs_1_.3, bf16[512,512]{1,0:T(8,128)(2,1)} %refs_2_.3, f32[1,512]{1,0:T(1,128)} %refs_6_.3, bf16[512,128]{1,0:T(8,128)(2,1)} %refs_5_.4, bf16[512,256]{1,0:T(8,128)(2,1)} %refs_6_.2, f32[1,512]{1,0:T(1,128)} %refs_7_.3), custom_call_target="tpu_custom_call" | custom-call | flops 134217728 | bytes 1000000 | tf_op jit(solution)/shard_map/own_state/pallas_call | solution.py:70
  10.9 20.5 %collective-permute-start = (bf16[2,128,768]{2,1,0:T(8,128)(2,1)S(1)}, bf16[2,128,768]{2,1,0:T(8,128)(2,1)S(1)}, u32[]{:S(2)}, u32[]{:S(2)}) collective-permute-start(bf16[2,128,768]{2,1,0:T(8,128)(2,1)S(1)} %own_state.1.refs_1_), channel_id=1, source_target_pairs={{0,4},{4,0},{1,5},{5,1},{2,6},{6,2},{3,7},{7,3},{8,12},{12,8},{9,1... | collective-permute-start | bytes 1179656 | tf_op jit(solution)/shard_map/ppermute | solution.py:474
  31.4 0.1 pad_add_fusion.refs_0_
  31.5 1.3 collective-permute-done.refs_2_.refs_3_
  32.8 0.9 of_chip.1
  33.7 0.1 collective-permute-start.1
  33.9 0.1 collective-permute-start.2
  34.0 3.1 %collective-permute-start.3 = (bf16[32,768]{1,0:T(8,128)(2,1)S(1)}, bf16[32,768]{1,0:T(8,128)(2,1)S(1)}, u32[]{:S(2)}, u32[]{:S(2)}) collective-permute-start(bf16[32,768]{1,0:T(8,128)(2,1)S(1)} %get-tuple-element.65), channel_id=1, source_target_pairs={{0,24},{8,0},{16,8},{24,16},{1,25},{9,1},{17,9},{25,17},{2,26},{10... | collective-permute-start | bytes 147464 | tf_op jit(solution)/shard_map/ppermute | solution.py:470
  37.1 1.5 collective-permute-done.1.refs_2_
  38.7 0.0 collective-permute-done.2.refs_3_
  38.7 1.1 collective-permute-done.3.refs_4_
  39.7 0.8 of_group.1
  40.5 1.3 collective-permute-start.4
  41.8 6.5 %collective-permute-start.6 = (bf16[1,32,768]{2,1,0:T(8,128)(2,1)S(1)}, bf16[1,32,768]{2,1,0:T(8,128)(2,1)S(1)}, u32[]{:S(2)}, u32[]{:S(2)}) collective-permute-start(bf16[1,32,768]{2,1,0:T(8,128)(2,1)S(1)} %of_group.1), channel_id=1, source_target_pairs={{0,96},{1,97},{2,98},{3,99},{4,100},{5,101},{6,102},{7,103},{8,104... | collective-permute-start | bytes 147464 | tf_op jit(solution)/shard_map/ppermute | solution.py:470
  48.3 4.2 %collective-permute-start.5 = (bf16[1,32,768]{2,1,0:T(8,128)(2,1)S(1)}, bf16[1,32,768]{2,1,0:T(8,128)(2,1)S(1)}, u32[]{:S(2)}, u32[]{:S(2)}) collective-permute-start(bf16[1,32,768]{2,1,0:T(8,128)(2,1)S(1)} %collective-permute-done.4.refs_5_), channel_id=1, source_target_pairs={{0,32},{32,64},{64,96},{1,33},{33,65},{65,97},{2,34},{34,66},{66,9... | collective-permute-start | bytes 147464 | tf_op jit(solution)/shard_map/ppermute | solution.py:470
  52.6 2.2 %collective-permute-done.5.refs_6_ = bf16[1,32,768]{2,1,0:T(8,128)(2,1)S(1)} collective-permute-done((bf16[1,32,768]{2,1,0:T(8,128)(2,1)S(1)}, bf16[1,32,768]{2,1,0:T(8,128)(2,1)S(1)}, u32[]{:S(2)}, u32[]{:S(2)}) %collective-permute-start.5) | collective-permute-done | bytes 49184 | tf_op jit(solution)/shard_map/ppermute | solution.py:470
  54.8 0.8 before_each.1
  55.6 2.4 %collective-permute-start.7 = (bf16[32,640]{1,0:T(8,128)(2,1)S(1)}, bf16[32,640]{1,0:T(8,128)(2,1)S(1)}, u32[]{:S(2)}, u32[]{:S(2)}) collective-permute-start(bf16[32,640]{1,0:T(8,128)(2,1)S(1)} %get-tuple-element.71), channel_id=1, source_target_pairs={{0,8},{8,16},{16,24},{24,0},{1,9},{9,17},{17,25},{25,1},{2,10},{10... | collective-permute-start | bytes 122888 | tf_op jit(solution)/shard_map/ppermute | solution.py:470
  58.0 4.2 %collective-permute-start.8 = (bf16[32,640]{1,0:T(8,128)(2,1)S(1)}, bf16[32,640]{1,0:T(8,128)(2,1)S(1)}, u32[]{:S(2)}, u32[]{:S(2)}) collective-permute-start(bf16[32,640]{1,0:T(8,128)(2,1)S(1)} %get-tuple-element.70), channel_id=1, source_target_pairs={{0,16},{8,24},{16,0},{24,8},{1,17},{9,25},{17,1},{25,9},{2,18},{10... | collective-permute-start | bytes 122888 | tf_op jit(solution)/shard_map/ppermute | solution.py:470
  62.2 0.0 collective-permute-start.9
  62.2 1.7 collective-permute-done.7.refs_2_
  63.9 2.0 %collective-permute-done.8.refs_3_ = bf16[32,640]{1,0:T(8,128)(2,1)S(1)} collective-permute-done((bf16[32,640]{1,0:T(8,128)(2,1)S(1)}, bf16[32,640]{1,0:T(8,128)(2,1)S(1)}, u32[]{:S(2)}, u32[]{:S(2)}) %collective-permute-start.8) | collective-permute-done | bytes 40992 | tf_op jit(solution)/shard_map/ppermute | solution.py:470
  65.9 1.5 collective-permute-done.9.refs_4_
  67.4 0.6 gathered_half.1.refs_1_
  68.0 2.6 %collective-permute-start.10 = (bf16[128,640]{1,0:T(8,128)(2,1)S(1)}, bf16[128,640]{1,0:T(8,128)(2,1)S(1)}, u32[]{:S(2)}, u32[]{:S(2)}) collective-permute-start(bf16[128,640]{1,0:T(8,128)(2,1)S(1)} %gathered_half.1.refs_1_), channel_id=1, source_target_pairs={{0,4},{4,0},{1,5},{5,1},{2,6},{6,2},{3,7},{7,3},{8,12},{12,8},{9,1... | collective-permute-start | bytes 491528 | tf_op jit(solution)/shard_map/ppermute | solution.py:474
  70.5 2.7 %inside.1.refs_8_ = f32[512,768]{1,0:T(8,128)S(1)} custom-call(bf16[512,256]{1,0:T(8,128)(2,1)} %refs_4_.5, bf16[512,256]{1,0:T(8,128)(2,1)} %refs_1_.3, bf16[512,512]{1,0:T(8,128)(2,1)} %refs_2_.3, f32[1,512]{1,0:T(1,128)} %refs_6_.3, bf16[512,128]{1,0:T(8,128)(2,1)} %refs_5_.5, bf16[512,128]{1,0:T(8,128)(2,1)} %refs_5_.4, bf16[512,256]{1,0:T(8,128)(2,1)} %refs_6_.2, ...), custom_call_target="tpu_custom_call" | custom-call | flops 805306368 | bytes 4000000 | tf_op jit(solution)/shard_map/inside/pallas_call | solution.py:70
  73.2 7.4 %heads_out.1 = (bf16[64,2048]{1,0:T(8,128)(2,1)}, bf16[64,2048]{1,0:T(8,128)(2,1)}, bf16[64,2048]{1,0:T(8,128)(2,1)}, bf16[64,2048]{1,0:T(8,128)(2,1)}, bf16[64,...) custom-call(s32[3]{0:T(128)S(1)} %pad_add_fusion.refs_0_, ...), custom_call_target="tpu_custom_call" | custom-call | flops 2147483648 | bytes 8000000 | tf_op jit(solution)/shard_map/heads_out/pallas_call | solution.py:70
  80.6 0.1 collective-permute-start.11
  80.7 2.7 %collective-permute-start.12 = (bf16[64,2048]{1,0:T(8,128)(2,1)}, bf16[64,2048]{1,0:T(8,128)(2,1)S(1)}, u32[]{:S(2)}, u32[]{:S(2)}) collective-permute-start(bf16[64,2048]{1,0:T(8,128)(2,1)} %get-tuple-element.39), channel_id=1, source_target_pairs={{0,3},{1,0},{2,1},{3,2},{4,7},{5,4},{6,5},{7,6},{8,11},{9,8},{10,9... | collective-permute-start | bytes 786440 | tf_op jit(solution)/shard_map/ppermute | solution.py:470
  83.4 0.0 collective-permute-start.14
  83.4 1.4 collective-permute-start.15
  84.9 5.2 %collective-permute-done.11.refs_1_ = bf16[64,2048]{1,0:T(8,128)(2,1)S(1)} collective-permute-done((bf16[64,2048]{1,0:T(8,128)(2,1)}, bf16[64,2048]{1,0:T(8,128)(2,1)S(1)}, u32[]{:S(2)}, u32[]{:S(2)}) %collective-permute-start.11) | collective-permute-done | bytes 262176 | tf_op jit(solution)/shard_map/ppermute | solution.py:470
  90.1 0.0 collective-permute-done.12.refs_3_
  90.1 1.9 %add_two.2 = (bf16[64,2048]{1,0:T(8,128)(2,1)}, bf16[64,2048]{1,0:T(8,128)(2,1)}) custom-call(bf16[64,2048]{1,0:T(8,128)(2,1)} %get-tuple-element.36.refs_0_, bf16[64,2048]{1,0:T(8,128)(2,1)S(1)} %collective-permute-done.11.refs_1_, bf16[64,2048]{1,0:T(8,128)(2,1)} %get-tuple-element.38.refs_2_, bf16[64,2048]{1,0:T(8,128)(2,1)S(1)} %collective-permute-done.12.refs_3_), custom_call_target="tpu_custom_call" | custom-call | tf_op jit(solution)/shard_map/add_two/pallas_call | solution.py:70
  92.0 0.1 collective-permute-start.13
  92.2 2.7 %collective-permute-start.16 = (bf16[64,2048]{1,0:T(8,128)(2,1)}, bf16[64,2048]{1,0:T(8,128)(2,1)S(1)}, u32[]{:S(2)}, u32[]{:S(2)}) collective-permute-start(bf16[64,2048]{1,0:T(8,128)(2,1)} %get-tuple-element.44), channel_id=1, source_target_pairs={{0,3},{1,0},{2,1},{3,2},{4,7},{5,4},{6,5},{7,6},{8,11},{9,8},{10,9... | collective-permute-start | bytes 786440 | tf_op jit(solution)/shard_map/ppermute | solution.py:470
  94.8 0.8 constant_dynamic-slice_fusion.refs_6_
  95.6 0.0 collective-permute-done.15.refs_4_
  95.7 4.5 %collective-permute-done.13.refs_1_ = bf16[64,2048]{1,0:T(8,128)(2,1)S(1)} collective-permute-done((bf16[64,2048]{1,0:T(8,128)(2,1)}, bf16[64,2048]{1,0:T(8,128)(2,1)S(1)}, u32[]{:S(2)}, u32[]{:S(2)}) %collective-permute-start.13) | collective-permute-done | bytes 262176 | tf_op jit(solution)/shard_map/ppermute | solution.py:470
  100.2 2.5 %rows_mid.1 = (bf16[64,2048]{1,0:T(8,128)(2,1)}, bf16[64,2048]{1,0:T(8,128)(2,1)}, bf16[64,2048]{1,0:T(8,128)(2,1)}, bf16[64,2048]{1,0:T(8,128)(2,1)}) custom-call(bf16[64,2048]{1,0:T(8,128)(2,1)} %get-tuple-element.35.refs_0_, bf16[64,2048]{1,0:T(8,128)(2,1)S(1)} %collective-permute-done.13.refs_1_, bf16[64,2048]{1,0:T(8,128)(2,1)S(1)} %collective-permute-done.14.refs_2_, ...), custom_call_target="tpu_custom_call" | custom-call | tf_op jit(solution)/shard_map/rows_mid/pallas_call | solution.py:70
  102.8 0.2 collective-permute-start.19
  103.0 2.6 %collective-permute-start.21 = (bf16[64,2048]{1,0:T(8,128)(2,1)}, bf16[64,2048]{1,0:T(8,128)(2,1)S(1)}, u32[]{:S(2)}, u32[]{:S(2)}) collective-permute-start(bf16[64,2048]{1,0:T(8,128)(2,1)} %get-tuple-element.55.refs_1_), channel_id=1, source_target_pairs={{0,3},{1,0},{2,1},{3,2},{4,7},{5,4},{6,5},{7,6},{8,11},{9,8},{10,9... | collective-permute-start | bytes 786440 | tf_op jit(solution)/shard_map/ppermute | solution.py:470
  105.6 4.6 %collective-permute-done.19.refs_3_ = bf16[64,2048]{1,0:T(8,128)(2,1)S(1)} collective-permute-done((bf16[64,2048]{1,0:T(8,128)(2,1)}, bf16[64,2048]{1,0:T(8,128)(2,1)S(1)}, u32[]{:S(2)}, u32[]{:S(2)}) %collective-permute-start.19) | collective-permute-done | bytes 262176 | tf_op jit(solution)/shard_map/ppermute | solution.py:470
  110.2 2.7 %collective-permute-start.22 = (bf16[64,2048]{1,0:T(8,128)(2,1)S(1)}, bf16[64,2048]{1,0:T(8,128)(2,1)}, u32[]{:S(2)}, u32[]{:S(2)}) collective-permute-start(bf16[64,2048]{1,0:T(8,128)(2,1)S(1)} %collective-permute-done.21.refs_2_), channel_id=1, source_target_pairs={{0,3},{1,0},{2,1},{3,2},{4,7},{5,4},{6,5},{7,6},{8,11},{9,8},{10,9... | collective-permute-start | bytes 786440 | tf_op jit(solution)/shard_map/ppermute | solution.py:470
  112.9 0.1 collective-permute-start.17
  113.0 1.3 collective-permute-start.18
  114.4 2.7 %collective-permute-done.20.refs_0_ = bf16[64,2048]{1,0:T(8,128)(2,1)S(1)} collective-permute-done((bf16[64,2048]{1,0:T(8,128)(2,1)S(1)}, bf16[64,2048]{1,0:T(8,128)(2,1)S(1)}, u32[]{:S(2)}, u32[]{:S(2)}) %collective-permute-start.20) | collective-permute-done | bytes 262176 | tf_op jit(solution)/shard_map/ppermute | solution.py:470
  117.1 18.8 %all-gather.2.cloned.1.call-done.refs_4_ = bf16[2048,4096]{1,0:T(8,128)(2,1)} async-done(((bf16[64,4096]{1,0:T(8,128)(2,1)}), bf16[2048,4096]{1,0:T(8,128)(2,1)}) %all-gather.2.cloned.1.call-update) | async-done | bytes 16777232 | tf_op jit(solution)/shard_map/all_gather | solution.py:522
  135.9 8.0 %first_rows.1 = (bf16[64,2048]{1,0:T(8,128)(2,1)S(1)}, bf16[64,2048]{1,0:T(8,128)(2,1)S(1)}, bf16[64,2048]{1,0:T(8,128)(2,1)S(1)}, bf16[64,2048]{1,0:T(8,128)(2,...) custom-call(bf16[64,2048]{1,0:T(8,128)(2,1)} %copy-done.5, ...), custom_call_target="tpu_custom_call" | custom-call | flops 4294967296 | bytes 16777216 | tf_op jit(solution)/shard_map/first_rows/pallas_call | solution.py:407
  143.9 1.2 collective-permute-start.23
  145.1 1.6 collective-permute-start.24
  146.7 1.3 collective-permute-start.26
  148.0 0.2 collective-permute-start.27
  148.2 4.5 %more_rows.2 = (bf16[64,2048]{1,0:T(8,128)(2,1)S(1)}, bf16[64,2048]{1,0:T(8,128)(2,1)S(1)}) custom-call(bf16[64,2048]{1,0:T(8,128)(2,1)S(1)} %collective-permute-done.17.refs_0_, bf16[64,2048]{1,0:T(8,128)(2,1)S(1)} %collective-permute-done.18.refs_1_, bf16[2048,2048]{1,0:T(8,128)(2,1)S(1)} %get-tuple-element.47.refs_2_, ...), custom_call_target="tpu_custom_call" | custom-call | flops 2147483648 | bytes 16777216 | tf_op jit(solution)/shard_map/more_rows/pallas_call | solution.py:438
  152.7 0.1 collective-permute-done.23.refs_1_
  152.9 0.1 add_two.3
  153.0 1.0 collective-permute-start.25
  154.0 1.8 %collective-permute-start.28 = (bf16[64,2048]{1,0:T(8,128)(2,1)S(1)}, bf16[64,2048]{1,0:T(8,128)(2,1)S(1)}, u32[]{:S(2)}, u32[]{:S(2)}) collective-permute-start(bf16[64,2048]{1,0:T(8,128)(2,1)S(1)} %get-tuple-element.64), channel_id=1, source_target_pairs={{0,3},{1,0},{2,1},{3,2},{4,7},{5,4},{6,5},{7,6},{8,11},{9,8},{10,9... | collective-permute-start | bytes 786440 | tf_op jit(solution)/shard_map/ppermute | solution.py:470
  155.8 4.5 %more_rows.3 = (bf16[64,2048]{1,0:T(8,128)(2,1)S(1)}, bf16[64,2048]{1,0:T(8,128)(2,1)S(1)}) custom-call(bf16[64,2048]{1,0:T(8,128)(2,1)S(1)} %copy-done.1, bf16[64,2048]{1,0:T(8,128)(2,1)S(1)} %copy-done.2, bf16[2048,2048]{1,0:T(8,128)(2,1)S(1)} %get-tuple-element.47.refs_2_, bf16[2048,2048]{1,0:T(8,128)(2,1)S(1)} %get-tuple-element.48.refs_3_), custom_call_target="tpu_custom_call" | custom-call | flops 2147483648 | bytes 16777216 | tf_op jit(solution)/shard_map/more_rows/pallas_call | solution.py:438
  160.3 1.2 with_middle.1
  161.5 2.6 %collective-permute-done.25.refs_1_ = bf16[64,2048]{1,0:T(8,128)(2,1)S(1)} collective-permute-done((bf16[64,2048]{1,0:T(8,128)(2,1)S(1)}, bf16[64,2048]{1,0:T(8,128)(2,1)S(1)}, u32[]{:S(2)}, u32[]{:S(2)}) %collective-permute-start.25) | collective-permute-done | bytes 262176 | tf_op jit(solution)/shard_map/ppermute | solution.py:470
  164.1 1.0 last_sum.1
  (29 shorter events, 0.1 us)
Async XLA Ops:
  6.5 88.3 %copy-start = (bf16[512,2048]{1,0:T(8,128)(2,1)S(1)}, bf16[512,2048]{1,0:T(8,128)(2,1)}, u32[]{:S(2)}) copy-start(bf16[512,2048]{1,0:T(8,128)(2,1)} %param.16) | copy-start | bytes 6291460
  6.6 129.3 %all-gather.2.cloned.1.call-start = ((), (), s32[]{:S(2)}) async-start(), calls=%async_computation | async-start | bytes 17301504 | tf_op jit(solution)/shard_map/all_gather | solution.py:522
  10.9 21.9 %collective-permute-start = (bf16[2,128,768]{2,1,0:T(8,128)(2,1)S(1)}, bf16[2,128,768]{2,1,0:T(8,128)(2,1)S(1)}, u32[]{:S(2)}, u32[]{:S(2)}) collective-permute-start(bf16[2,128,768]{2,1,0:T(8,128)(2,1)S(1)} %own_state.1.refs_1_), channel_id=1, source_target_pairs={{0,4},{4,0},{1,5},{5,1},{2,6},{6,2},{3,7},{7,3},{8,12},{12,8},{9,1... | collective-permute-start | bytes 1179656 | tf_op jit(solution)/shard_map/ppermute | solution.py:474
  33.7 4.9 %collective-permute-start.1 = (bf16[32,768]{1,0:T(8,128)(2,1)S(1)}, bf16[32,768]{1,0:T(8,128)(2,1)S(1)}, u32[]{:S(2)}, u32[]{:S(2)}) collective-permute-start(bf16[32,768]{1,0:T(8,128)(2,1)S(1)} %get-tuple-element.67), channel_id=1, source_target_pairs={{0,8},{8,16},{16,24},{24,0},{1,9},{9,17},{17,25},{25,1},{2,10},{10... | collective-permute-start | bytes 147464 | tf_op jit(solution)/shard_map/ppermute | solution.py:470
  33.9 4.8 %collective-permute-start.2 = (bf16[32,768]{1,0:T(8,128)(2,1)S(1)}, bf16[32,768]{1,0:T(8,128)(2,1)S(1)}, u32[]{:S(2)}, u32[]{:S(2)}) collective-permute-start(bf16[32,768]{1,0:T(8,128)(2,1)S(1)} %get-tuple-element.66), channel_id=1, source_target_pairs={{0,16},{8,24},{16,0},{24,8},{1,17},{9,25},{17,1},{25,9},{2,18},{10... | collective-permute-start | bytes 147464 | tf_op jit(solution)/shard_map/ppermute | solution.py:470
  34.0 5.7 %collective-permute-start.3 = (bf16[32,768]{1,0:T(8,128)(2,1)S(1)}, bf16[32,768]{1,0:T(8,128)(2,1)S(1)}, u32[]{:S(2)}, u32[]{:S(2)}) collective-permute-start(bf16[32,768]{1,0:T(8,128)(2,1)S(1)} %get-tuple-element.65), channel_id=1, source_target_pairs={{0,24},{8,0},{16,8},{24,16},{1,25},{9,1},{17,9},{25,17},{2,26},{10... | collective-permute-start | bytes 147464 | tf_op jit(solution)/shard_map/ppermute | solution.py:470
  40.5 7.8 %collective-permute-start.4 = (bf16[1,32,768]{2,1,0:T(8,128)(2,1)S(1)}, bf16[1,32,768]{2,1,0:T(8,128)(2,1)S(1)}, u32[]{:S(2)}, u32[]{:S(2)}) collective-permute-start(bf16[1,32,768]{2,1,0:T(8,128)(2,1)S(1)} %of_group.1), channel_id=1, source_target_pairs={{0,32},{32,64},{64,96},{1,33},{33,65},{65,97},{2,34},{34,66},{66,9... | collective-permute-start | bytes 147464 | tf_op jit(solution)/shard_map/ppermute | solution.py:470
  41.8 10.8 %collective-permute-start.6 = (bf16[1,32,768]{2,1,0:T(8,128)(2,1)S(1)}, bf16[1,32,768]{2,1,0:T(8,128)(2,1)S(1)}, u32[]{:S(2)}, u32[]{:S(2)}) collective-permute-start(bf16[1,32,768]{2,1,0:T(8,128)(2,1)S(1)} %of_group.1), channel_id=1, source_target_pairs={{0,96},{1,97},{2,98},{3,99},{4,100},{5,101},{6,102},{7,103},{8,104... | collective-permute-start | bytes 147464 | tf_op jit(solution)/shard_map/ppermute | solution.py:470
  48.3 6.4 %collective-permute-start.5 = (bf16[1,32,768]{2,1,0:T(8,128)(2,1)S(1)}, bf16[1,32,768]{2,1,0:T(8,128)(2,1)S(1)}, u32[]{:S(2)}, u32[]{:S(2)}) collective-permute-start(bf16[1,32,768]{2,1,0:T(8,128)(2,1)S(1)} %collective-permute-done.4.refs_5_), channel_id=1, source_target_pairs={{0,32},{32,64},{64,96},{1,33},{33,65},{65,97},{2,34},{34,66},{66,9... | collective-permute-start | bytes 147464 | tf_op jit(solution)/shard_map/ppermute | solution.py:470
  55.6 8.4 %collective-permute-start.7 = (bf16[32,640]{1,0:T(8,128)(2,1)S(1)}, bf16[32,640]{1,0:T(8,128)(2,1)S(1)}, u32[]{:S(2)}, u32[]{:S(2)}) collective-permute-start(bf16[32,640]{1,0:T(8,128)(2,1)S(1)} %get-tuple-element.71), channel_id=1, source_target_pairs={{0,8},{8,16},{16,24},{24,0},{1,9},{9,17},{17,25},{25,1},{2,10},{10... | collective-permute-start | bytes 122888 | tf_op jit(solution)/shard_map/ppermute | solution.py:470
  58.0 7.9 %collective-permute-start.8 = (bf16[32,640]{1,0:T(8,128)(2,1)S(1)}, bf16[32,640]{1,0:T(8,128)(2,1)S(1)}, u32[]{:S(2)}, u32[]{:S(2)}) collective-permute-start(bf16[32,640]{1,0:T(8,128)(2,1)S(1)} %get-tuple-element.70), channel_id=1, source_target_pairs={{0,16},{8,24},{16,0},{24,8},{1,17},{9,25},{17,1},{25,9},{2,18},{10... | collective-permute-start | bytes 122888 | tf_op jit(solution)/shard_map/ppermute | solution.py:470
  62.2 5.1 %collective-permute-start.9 = (bf16[32,640]{1,0:T(8,128)(2,1)S(1)}, bf16[32,640]{1,0:T(8,128)(2,1)S(1)}, u32[]{:S(2)}, u32[]{:S(2)}) collective-permute-start(bf16[32,640]{1,0:T(8,128)(2,1)S(1)} %get-tuple-element.69), channel_id=1, source_target_pairs={{0,24},{8,0},{16,8},{24,16},{1,25},{9,1},{17,9},{25,17},{2,26},{10... | collective-permute-start | bytes 122888 | tf_op jit(solution)/shard_map/ppermute | solution.py:470
  68.0 5.3 %collective-permute-start.10 = (bf16[128,640]{1,0:T(8,128)(2,1)S(1)}, bf16[128,640]{1,0:T(8,128)(2,1)S(1)}, u32[]{:S(2)}, u32[]{:S(2)}) collective-permute-start(bf16[128,640]{1,0:T(8,128)(2,1)S(1)} %gathered_half.1.refs_1_), channel_id=1, source_target_pairs={{0,4},{4,0},{1,5},{5,1},{2,6},{6,2},{3,7},{7,3},{8,12},{12,8},{9,1... | collective-permute-start | bytes 491528 | tf_op jit(solution)/shard_map/ppermute | solution.py:474
  80.6 9.5 %collective-permute-start.11 = (bf16[64,2048]{1,0:T(8,128)(2,1)}, bf16[64,2048]{1,0:T(8,128)(2,1)S(1)}, u32[]{:S(2)}, u32[]{:S(2)}) collective-permute-start(bf16[64,2048]{1,0:T(8,128)(2,1)} %get-tuple-element.37), channel_id=1, source_target_pairs={{0,1},{1,2},{2,3},{3,0},{4,5},{5,6},{6,7},{7,4},{8,9},{9,10},{10,1... | collective-permute-start | bytes 786440 | tf_op jit(solution)/shard_map/ppermute | solution.py:470
  80.7 9.3 %collective-permute-start.12 = (bf16[64,2048]{1,0:T(8,128)(2,1)}, bf16[64,2048]{1,0:T(8,128)(2,1)S(1)}, u32[]{:S(2)}, u32[]{:S(2)}) collective-permute-start(bf16[64,2048]{1,0:T(8,128)(2,1)} %get-tuple-element.39), channel_id=1, source_target_pairs={{0,3},{1,0},{2,1},{3,2},{4,7},{5,4},{6,5},{7,6},{8,11},{9,8},{10,9... | collective-permute-start | bytes 786440 | tf_op jit(solution)/shard_map/ppermute | solution.py:470
  83.4 12.3 %collective-permute-start.14 = (bf16[64,2048]{1,0:T(8,128)(2,1)}, bf16[64,2048]{1,0:T(8,128)(2,1)S(1)}, u32[]{:S(2)}, u32[]{:S(2)}) collective-permute-start(bf16[64,2048]{1,0:T(8,128)(2,1)} %get-tuple-element.41), channel_id=1, source_target_pairs={{0,3},{1,0},{2,1},{3,2},{4,7},{5,4},{6,5},{7,6},{8,11},{9,8},{10,9... | collective-permute-start | bytes 786440 | tf_op jit(solution)/shard_map/ppermute | solution.py:470
  83.4 12.3 %collective-permute-start.15 = (bf16[64,2048]{1,0:T(8,128)(2,1)}, bf16[64,2048]{1,0:T(8,128)(2,1)S(1)}, u32[]{:S(2)}, u32[]{:S(2)}) collective-permute-start(bf16[64,2048]{1,0:T(8,128)(2,1)} %get-tuple-element.43), channel_id=1, source_target_pairs={{0,1},{1,2},{2,3},{3,0},{4,5},{5,6},{6,7},{7,4},{8,9},{9,10},{10,1... | collective-permute-start | bytes 786440 | tf_op jit(solution)/shard_map/ppermute | solution.py:470
  92.0 8.2 %collective-permute-start.13 = (bf16[64,2048]{1,0:T(8,128)(2,1)}, bf16[64,2048]{1,0:T(8,128)(2,1)S(1)}, u32[]{:S(2)}, u32[]{:S(2)}) collective-permute-start(bf16[64,2048]{1,0:T(8,128)(2,1)} %get-tuple-element.40), channel_id=1, source_target_pairs={{0,1},{1,2},{2,3},{3,0},{4,5},{5,6},{6,7},{7,4},{8,9},{9,10},{10,1... | collective-permute-start | bytes 786440 | tf_op jit(solution)/shard_map/ppermute | solution.py:470
  92.2 8.1 %collective-permute-start.16 = (bf16[64,2048]{1,0:T(8,128)(2,1)}, bf16[64,2048]{1,0:T(8,128)(2,1)S(1)}, u32[]{:S(2)}, u32[]{:S(2)}) collective-permute-start(bf16[64,2048]{1,0:T(8,128)(2,1)} %get-tuple-element.44), channel_id=1, source_target_pairs={{0,3},{1,0},{2,1},{3,2},{4,7},{5,4},{6,5},{7,6},{8,11},{9,8},{10,9... | collective-permute-start | bytes 786440 | tf_op jit(solution)/shard_map/ppermute | solution.py:470
  102.8 7.4 %collective-permute-start.19 = (bf16[64,2048]{1,0:T(8,128)(2,1)}, bf16[64,2048]{1,0:T(8,128)(2,1)S(1)}, u32[]{:S(2)}, u32[]{:S(2)}) collective-permute-start(bf16[64,2048]{1,0:T(8,128)(2,1)} %get-tuple-element.54.refs_0_), channel_id=1, source_target_pairs={{0,1},{1,2},{2,3},{3,0},{4,5},{5,6},{6,7},{7,4},{8,9},{9,10},{10,1... | collective-permute-start | bytes 786440 | tf_op jit(solution)/shard_map/ppermute | solution.py:470
  103.0 7.3 %collective-permute-start.21 = (bf16[64,2048]{1,0:T(8,128)(2,1)}, bf16[64,2048]{1,0:T(8,128)(2,1)S(1)}, u32[]{:S(2)}, u32[]{:S(2)}) collective-permute-start(bf16[64,2048]{1,0:T(8,128)(2,1)} %get-tuple-element.55.refs_1_), channel_id=1, source_target_pairs={{0,3},{1,0},{2,1},{3,2},{4,7},{5,4},{6,5},{7,6},{8,11},{9,8},{10,9... | collective-permute-start | bytes 786440 | tf_op jit(solution)/shard_map/ppermute | solution.py:470
  110.2 25.7 %copy-start.3 = (bf16[64,2048]{1,0:T(8,128)(2,1)}, bf16[64,2048]{1,0:T(8,128)(2,1)S(1)}, u32[]{:S(2)}) copy-start(bf16[64,2048]{1,0:T(8,128)(2,1)S(1)} %collective-permute-done.19.refs_3_) | copy-start | bytes 786436
  110.2 6.8 %collective-permute-start.20 = (bf16[64,2048]{1,0:T(8,128)(2,1)S(1)}, bf16[64,2048]{1,0:T(8,128)(2,1)S(1)}, u32[]{:S(2)}, u32[]{:S(2)}) collective-permute-start(bf16[64,2048]{1,0:T(8,128)(2,1)S(1)} %collective-permute-done.19.refs_3_), channel_id=1, source_target_pairs={{0,1},{1,2},{2,3},{3,0},{4,5},{5,6},{6,7},{7,4},{8,9},{9,10},{10,1... | collective-permute-start | bytes 786440 | tf_op jit(solution)/shard_map/ppermute | solution.py:470
  110.2 25.7 %copy-start.4 = (bf16[64,2048]{1,0:T(8,128)(2,1)}, bf16[64,2048]{1,0:T(8,128)(2,1)S(1)}, u32[]{:S(2)}) copy-start(bf16[64,2048]{1,0:T(8,128)(2,1)S(1)} %collective-permute-done.21.refs_2_) | copy-start | bytes 786436
  110.2 6.8 %collective-permute-start.22 = (bf16[64,2048]{1,0:T(8,128)(2,1)S(1)}, bf16[64,2048]{1,0:T(8,128)(2,1)}, u32[]{:S(2)}, u32[]{:S(2)}) collective-permute-start(bf16[64,2048]{1,0:T(8,128)(2,1)S(1)} %collective-permute-done.21.refs_2_), channel_id=1, source_target_pairs={{0,3},{1,0},{2,1},{3,2},{4,7},{5,4},{6,5},{7,6},{8,11},{9,8},{10,9... | collective-permute-start | bytes 786440 | tf_op jit(solution)/shard_map/ppermute | solution.py:470
  112.9 35.1 %collective-permute-start.17 = (bf16[64,2048]{1,0:T(8,128)(2,1)}, bf16[64,2048]{1,0:T(8,128)(2,1)S(1)}, u32[]{:S(2)}, u32[]{:S(2)}) collective-permute-start(bf16[64,2048]{1,0:T(8,128)(2,1)} %get-tuple-element.54.refs_0_), channel_id=1, source_target_pairs={{0,3},{1,0},{2,1},{3,2},{4,7},{5,4},{6,5},{7,6},{8,11},{9,8},{10,9... | collective-permute-start | bytes 786440 | tf_op jit(solution)/shard_map/ppermute | solution.py:470
  113.0 35.2 %collective-permute-start.18 = (bf16[64,2048]{1,0:T(8,128)(2,1)}, bf16[64,2048]{1,0:T(8,128)(2,1)S(1)}, u32[]{:S(2)}, u32[]{:S(2)}) collective-permute-start(bf16[64,2048]{1,0:T(8,128)(2,1)} %get-tuple-element.55.refs_1_), channel_id=1, source_target_pairs={{0,1},{1,2},{2,3},{3,0},{4,5},{5,6},{6,7},{7,4},{8,9},{9,10},{10,1... | collective-permute-start | bytes 786440 | tf_op jit(solution)/shard_map/ppermute | solution.py:470
  117.0 18.8 %copy-start.5 = (bf16[64,2048]{1,0:T(8,128)(2,1)}, bf16[64,2048]{1,0:T(8,128)(2,1)S(1)}, u32[]{:S(2)}) copy-start(bf16[64,2048]{1,0:T(8,128)(2,1)S(1)} %collective-permute-done.20.refs_0_) | copy-start | bytes 786436
  143.9 8.9 %collective-permute-start.23 = (bf16[64,2048]{1,0:T(8,128)(2,1)S(1)}, bf16[64,2048]{1,0:T(8,128)(2,1)S(1)}, u32[]{:S(2)}, u32[]{:S(2)}) collective-permute-start(bf16[64,2048]{1,0:T(8,128)(2,1)S(1)} %get-tuple-element.50), channel_id=1, source_target_pairs={{0,1},{1,2},{2,3},{3,0},{4,5},{5,6},{6,7},{7,4},{8,9},{9,10},{10,1... | collective-permute-start | bytes 786440 | tf_op jit(solution)/shard_map/ppermute | solution.py:470
  145.1 7.8 %collective-permute-start.24 = (bf16[64,2048]{1,0:T(8,128)(2,1)S(1)}, bf16[64,2048]{1,0:T(8,128)(2,1)S(1)}, u32[]{:S(2)}, u32[]{:S(2)}) collective-permute-start(bf16[64,2048]{1,0:T(8,128)(2,1)S(1)} %get-tuple-element.52), channel_id=1, source_target_pairs={{0,3},{1,0},{2,1},{3,2},{4,7},{5,4},{6,5},{7,6},{8,11},{9,8},{10,9... | collective-permute-start | bytes 786440 | tf_op jit(solution)/shard_map/ppermute | solution.py:470
  146.7 14.8 %collective-permute-start.26 = (bf16[64,2048]{1,0:T(8,128)(2,1)S(1)}, bf16[64,2048]{1,0:T(8,128)(2,1)S(1)}, u32[]{:S(2)}, u32[]{:S(2)}) collective-permute-start(bf16[64,2048]{1,0:T(8,128)(2,1)S(1)} %get-tuple-element.61), channel_id=1, source_target_pairs={{0,3},{1,0},{2,1},{3,2},{4,7},{5,4},{6,5},{7,6},{8,11},{9,8},{10,9... | collective-permute-start | bytes 786440 | tf_op jit(solution)/shard_map/ppermute | solution.py:470
  148.0 13.5 %collective-permute-start.27 = (bf16[64,2048]{1,0:T(8,128)(2,1)S(1)}, bf16[64,2048]{1,0:T(8,128)(2,1)S(1)}, u32[]{:S(2)}, u32[]{:S(2)}) collective-permute-start(bf16[64,2048]{1,0:T(8,128)(2,1)S(1)} %get-tuple-element.63), channel_id=1, source_target_pairs={{0,1},{1,2},{2,3},{3,0},{4,5},{5,6},{6,7},{7,4},{8,9},{9,10},{10,1... | collective-permute-start | bytes 786440 | tf_op jit(solution)/shard_map/ppermute | solution.py:470
  148.2 7.6 %copy-start.1 = (bf16[64,2048]{1,0:T(8,128)(2,1)S(1)}, bf16[64,2048]{1,0:T(8,128)(2,1)}, u32[]{:S(2)}) copy-start(bf16[64,2048]{1,0:T(8,128)(2,1)} %get-tuple-element.54.refs_0_) | copy-start | bytes 786436
  148.2 7.6 %copy-start.2 = (bf16[64,2048]{1,0:T(8,128)(2,1)S(1)}, bf16[64,2048]{1,0:T(8,128)(2,1)}, u32[]{:S(2)}) copy-start(bf16[64,2048]{1,0:T(8,128)(2,1)} %get-tuple-element.55.refs_1_) | copy-start | bytes 786436
  153.0 11.1 %collective-permute-start.25 = (bf16[64,2048]{1,0:T(8,128)(2,1)S(1)}, bf16[64,2048]{1,0:T(8,128)(2,1)S(1)}, u32[]{:S(2)}, u32[]{:S(2)}) collective-permute-start(bf16[64,2048]{1,0:T(8,128)(2,1)S(1)} %get-tuple-element.53), channel_id=1, source_target_pairs={{0,1},{1,2},{2,3},{3,0},{4,5},{5,6},{6,7},{7,4},{8,9},{9,10},{10,1... | collective-permute-start | bytes 786440 | tf_op jit(solution)/shard_map/ppermute | solution.py:470
  154.0 10.1 %collective-permute-start.28 = (bf16[64,2048]{1,0:T(8,128)(2,1)S(1)}, bf16[64,2048]{1,0:T(8,128)(2,1)S(1)}, u32[]{:S(2)}, u32[]{:S(2)}) collective-permute-start(bf16[64,2048]{1,0:T(8,128)(2,1)S(1)} %get-tuple-element.64), channel_id=1, source_target_pairs={{0,3},{1,0},{2,1},{3,2},{4,7},{5,4},{6,5},{7,6},{8,11},{9,8},{10,9... | collective-permute-start | bytes 786440 | tf_op jit(solution)/shard_map/ppermute | solution.py:470
Sparse Core Ops, SparseCore 0:
  9.2 126.6 all-gather.1

commit v7 on v6

--- a/solution.py
+++ b/solution.py
@@ -285,7 +285,7 @@
         start = pl.multiple_of(order * 2 * rows, 2 * rows)
         turned_wide[pl.ds(start, 2 * rows), :] = wide[m * 2 * rows : (m + 1) * 2 * rows]
         turned_thin[pl.ds(start, 2 * rows), :] = thin[m * 2 * rows : (m + 1) * 2 * rows]
-    step = 1024
+    step = 512
 
     @pl.loop(0, ow.shape[1] // step)
     def _(n):
@@ -337,52 +337,51 @@
     number = len(ends) // 2
     parts, weights, outs = ends[:number], ends[number], ends[number + 1 :]
     size = parts[0].shape[0]
-    units, block = up.shape[1], 512
-    count = up.shape[0] // block
-
-    def fetch(k, column, to, sems):
+    units, block, wide = up.shape[1], 512, 1024
+
+    def fetch(k, column, to, sems, block):
         span = pl.ds(pl.multiple_of(k * block, block), block)
         source = weights.at[span, pl.ds(column * units, units)]
         return pltpu.make_async_copy(source, to.at[span, :], sems.at[k])
 
     copies = fetched(list(zip(parts, stacked(parts, rows))), row_sems)
 
-    @pl.loop(0, count)
+    @pl.loop(0, up.shape[0] // block)
     def _(k):
-        fetch(k, 0, up, up_sems).start()
-
-    @pl.loop(0, count)
+        fetch(k, 0, up, up_sems, block).start()
+
+    @pl.loop(0, down.shape[0] // wide)
     def _(k):
-        fetch(k, 1, down, down_sems).start()
+        fetch(k, 1, down, down_sems, wide).start()
 
     for copy in copies:
         copy.wait()
     total[...] = jnp.zeros_like(total)
 
-    @pl.loop(0, count)
+    @pl.loop(0, up.shape[0] // block)
     def _(k):
-        fetch(k, 0, up, up_sems).wait()
+        fetch(k, 0, up, up_sems, block).wait()
         span = pl.ds(pl.multiple_of(k * block, block), block)
         total[...] += mm(rows[:, span], up[span, :])
 
     hidden[...] = squared(total[...])
 
-    @pl.loop(0, count)
+    @pl.loop(0, down.shape[0] // wide)
     def _(k):
-        fetch(k, 1, down, down_sems).wait()
-        span = pl.ds(pl.multiple_of(k * block, block), block)
+        fetch(k, 1, down, down_sems, wide).wait()
+        span = pl.ds(pl.multiple_of(k * wide, wide), wide)
         done = mm(hidden[...], down[span, :], ((1,), (1,))).astype(BF16)
         for m, out in enumerate(outs):
             out[:, span] = done[m * size : (m + 1) * size]
 
 
 def more_rows(*refs):
-    *ends, rows, hidden, row_sems = refs
+    *ends, rows, hidden = refs
     number = (len(ends) - 2) // 2
     parts, (up, down), outs = ends[:number], ends[number : number + 2], ends[number + 2 :]
     size, block = parts[0].shape[0], 1024
-    for copy in fetched(list(zip(parts, stacked(parts, rows))), row_sems):
-        copy.wait()
+    for n, part in enumerate(parts):
+        rows[n * size : (n + 1) * size, :] = part[...]
 
     @pl.loop(0, up.shape[1] // block)
     def _(n):
@@ -401,7 +400,7 @@
     size, width = parts[0].shape
     units = weights.shape[1] // 2
     number = len(parts)
-    count, total = width // 512, number * size
+    total = number * size
     far = pl.BlockSpec(memory_space=pltpu.HBM)
     held = [pltpu.with_memory_space_constraint(p, pltpu.HBM) for p in (*parts, weights)]
     *done, up, down = pl.pallas_call(
@@ -415,8 +414,8 @@
             pltpu.VMEM((total, units), F32),
             pltpu.VMEM((total, units), BF16),
             pltpu.SemaphoreType.DMA((number,)),
-            pltpu.SemaphoreType.DMA((count,)),
-            pltpu.SemaphoreType.DMA((count,)),
+            pltpu.SemaphoreType.DMA((width // 512,)),
+            pltpu.SemaphoreType.DMA((width // 1024,)),
         ],
         compiler_params=pltpu.CompilerParams(vmem_limit_bytes=20 * 2**20),
         cost_estimate=pl.CostEstimate(
@@ -432,18 +431,16 @@
     units = weights[0].shape[1]
     number = len(parts)
     total = number * size
-    far = pl.BlockSpec(memory_space=pltpu.HBM)
     held = list(parts)
     held += [pltpu.with_memory_space_constraint(w, pltpu.VMEM) for w in weights]
     return pl.pallas_call(
         more_rows,
         out_shape=[shaped((size, width), BF16)] * number,
-        in_specs=[pl.BlockSpec(memory_space=pl.ANY)] * number + [vmem()] * 2,
+        in_specs=[vmem()] * (number + 2),
         out_specs=[vmem()] * number,
         scratch_shapes=[
             pltpu.VMEM((total, width), BF16),
             pltpu.VMEM((total, units), BF16),
-            pltpu.SemaphoreType.DMA((number,)),
         ],
         compiler_params=pltpu.CompilerParams(vmem_limit_bytes=24 * 2**20),
         cost_estimate=pl.CostEstimate(

time: 172 us -> 172 us (level)
  no operation moved by 1% of the time
where the time goes in v7:
time: 172 us
  starting transfers between devices  66.2 us (38%)
  waiting for transfers between devices  49.6 us (29%)
  Pallas kernels  39.1 us (23%)
  between operations  13.7 us (8%)
  other arithmetic  2.09 us (1%)
    ppermute x27, starting transfers between devices, shift(): return lax.ppermute(x, axis, pairs)  43 us
    ppermute x27, waiting for transfers between devices, shift(): return lax.ppermute(x, axis, pairs)  29.8 us
    ppermute x2, starting transfers between devices, swap(): return lax.ppermute(x, 'core', [(0, 1), (1, 0)])  23.1 us
    pallas_call x12, Pallas kernels, call(): pl.pallas_call(inner, out_shape=[pltpu.HBM(o.shape, o.dtype) for o in out...  22.4 us
    all_gather x1, waiting for transfers between devices, on_device(): weights = lax.all_gather(both, SP, axis=0, tiled=True)  18.5 us
    pallas_call x2, Pallas kernels, more_forward(): pl.pallas_call(more_rows, out_shape=[shaped((size, width), BF16)] * numbe...  9 us
    pallas_call x1, Pallas kernels, first_forward(): pl.pallas_call(first_rows, out_shape=[pltpu.VMEM((size, width), BF16)] *...  7.64 us
  transfers between devices with their start and end apart: 30, of which 14 were waited for; matrix products, arithmetic and copies ran while one was open for 1% of the time, Pallas kernels for 22%

profile of v7, /device:TPU:33, one launch (start us, length us, event | category | flops | bytes accessed | tf_op | source)
XLA Modules:
  0.0 171.5 jit_solution(4453802520609116776)
XLA Ops:
  6.6 2.0 %pad_maximum_fusion = bf16[64,4096]{1,0:T(8,128)(2,1)} fusion(bf16[64,2048]{1,0:T(8,128)(2,1)} %bitcast.23, bf16[64,2048]{1,0:T(8,128)(2,1)} %param.30), kind=kLoop, calls=%fused_computation | loop fusion | flops 1048576 | bytes 1048576 | tf_op jit(solution)/shard_map/concatenate | solution.py:518
  8.6 0.1 all-gather.2.cloned.1.call-update
  8.6 2.3 %own_state.1.refs_1_ = bf16[2,128,768]{2,1,0:T(8,128)(2,1)S(1)} custom-call(bf16[512,256]{1,0:T(8,128)(2,1)} %refs_1_.3, bf16[512,512]{1,0:T(8,128)(2,1)} %refs_2_.3, f32[1,512]{1,0:T(1,128)} %refs_6_.3, bf16[512,128]{1,0:T(8,128)(2,1)} %refs_5_.4, bf16[512,256]{1,0:T(8,128)(2,1)} %refs_6_.2, f32[1,512]{1,0:T(1,128)} %refs_7_.3), custom_call_target="tpu_custom_call" | custom-call | flops 134217728 | bytes 1000000 | tf_op jit(solution)/shard_map/own_state/pallas_call | solution.py:70
  10.9 20.5 %collective-permute-start = (bf16[2,128,768]{2,1,0:T(8,128)(2,1)S(1)}, bf16[2,128,768]{2,1,0:T(8,128)(2,1)S(1)}, u32[]{:S(2)}, u32[]{:S(2)}) collective-permute-start(bf16[2,128,768]{2,1,0:T(8,128)(2,1)S(1)} %own_state.1.refs_1_), channel_id=1, source_target_pairs={{0,4},{4,0},{1,5},{5,1},{2,6},{6,2},{3,7},{7,3},{8,12},{12,8},{9,1... | collective-permute-start | bytes 1179656 | tf_op jit(solution)/shard_map/ppermute | solution.py:471
  31.4 0.1 pad_add_fusion.refs_0_
  31.5 1.3 collective-permute-done.refs_2_.refs_3_
  32.8 0.9 of_chip.1
  33.7 0.1 collective-permute-start.1
  33.9 0.1 collective-permute-start.2
  34.0 3.1 %collective-permute-start.3 = (bf16[32,768]{1,0:T(8,128)(2,1)S(1)}, bf16[32,768]{1,0:T(8,128)(2,1)S(1)}, u32[]{:S(2)}, u32[]{:S(2)}) collective-permute-start(bf16[32,768]{1,0:T(8,128)(2,1)S(1)} %get-tuple-element.65), channel_id=1, source_target_pairs={{0,24},{8,0},{16,8},{24,16},{1,25},{9,1},{17,9},{25,17},{2,26},{10... | collective-permute-start | bytes 147464 | tf_op jit(solution)/shard_map/ppermute | solution.py:467
  37.1 1.5 collective-permute-done.1.refs_2_
  38.7 0.0 collective-permute-done.2.refs_3_
  38.7 1.1 collective-permute-done.3.refs_4_
  39.7 0.8 of_group.1
  40.5 1.3 collective-permute-start.4
  41.8 6.5 %collective-permute-start.6 = (bf16[1,32,768]{2,1,0:T(8,128)(2,1)S(1)}, bf16[1,32,768]{2,1,0:T(8,128)(2,1)S(1)}, u32[]{:S(2)}, u32[]{:S(2)}) collective-permute-start(bf16[1,32,768]{2,1,0:T(8,128)(2,1)S(1)} %of_group.1), channel_id=1, source_target_pairs={{0,96},{1,97},{2,98},{3,99},{4,100},{5,101},{6,102},{7,103},{8,104... | collective-permute-start | bytes 147464 | tf_op jit(solution)/shard_map/ppermute | solution.py:467
  48.3 4.2 %collective-permute-start.5 = (bf16[1,32,768]{2,1,0:T(8,128)(2,1)S(1)}, bf16[1,32,768]{2,1,0:T(8,128)(2,1)S(1)}, u32[]{:S(2)}, u32[]{:S(2)}) collective-permute-start(bf16[1,32,768]{2,1,0:T(8,128)(2,1)S(1)} %collective-permute-done.4.refs_5_), channel_id=1, source_target_pairs={{0,32},{32,64},{64,96},{1,33},{33,65},{65,97},{2,34},{34,66},{66,9... | collective-permute-start | bytes 147464 | tf_op jit(solution)/shard_map/ppermute | solution.py:467
  52.6 2.2 %collective-permute-done.5.refs_6_ = bf16[1,32,768]{2,1,0:T(8,128)(2,1)S(1)} collective-permute-done((bf16[1,32,768]{2,1,0:T(8,128)(2,1)S(1)}, bf16[1,32,768]{2,1,0:T(8,128)(2,1)S(1)}, u32[]{:S(2)}, u32[]{:S(2)}) %collective-permute-start.5) | collective-permute-done | bytes 49184 | tf_op jit(solution)/shard_map/ppermute | solution.py:467
  54.8 0.8 before_each.1
  55.6 2.4 %collective-permute-start.7 = (bf16[32,640]{1,0:T(8,128)(2,1)S(1)}, bf16[32,640]{1,0:T(8,128)(2,1)S(1)}, u32[]{:S(2)}, u32[]{:S(2)}) collective-permute-start(bf16[32,640]{1,0:T(8,128)(2,1)S(1)} %get-tuple-element.71), channel_id=1, source_target_pairs={{0,8},{8,16},{16,24},{24,0},{1,9},{9,17},{17,25},{25,1},{2,10},{10... | collective-permute-start | bytes 122888 | tf_op jit(solution)/shard_map/ppermute | solution.py:467
  58.0 4.2 %collective-permute-start.8 = (bf16[32,640]{1,0:T(8,128)(2,1)S(1)}, bf16[32,640]{1,0:T(8,128)(2,1)S(1)}, u32[]{:S(2)}, u32[]{:S(2)}) collective-permute-start(bf16[32,640]{1,0:T(8,128)(2,1)S(1)} %get-tuple-element.70), channel_id=1, source_target_pairs={{0,16},{8,24},{16,0},{24,8},{1,17},{9,25},{17,1},{25,9},{2,18},{10... | collective-permute-start | bytes 122888 | tf_op jit(solution)/shard_map/ppermute | solution.py:467
  62.2 0.0 collective-permute-start.9
  62.2 1.7 collective-permute-done.7.refs_2_
  63.9 2.0 %collective-permute-done.8.refs_3_ = bf16[32,640]{1,0:T(8,128)(2,1)S(1)} collective-permute-done((bf16[32,640]{1,0:T(8,128)(2,1)S(1)}, bf16[32,640]{1,0:T(8,128)(2,1)S(1)}, u32[]{:S(2)}, u32[]{:S(2)}) %collective-permute-start.8) | collective-permute-done | bytes 40992 | tf_op jit(solution)/shard_map/ppermute | solution.py:467
  65.9 1.5 collective-permute-done.9.refs_4_
  67.4 0.6 gathered_half.1.refs_1_
  68.0 2.6 %collective-permute-start.10 = (bf16[128,640]{1,0:T(8,128)(2,1)S(1)}, bf16[128,640]{1,0:T(8,128)(2,1)S(1)}, u32[]{:S(2)}, u32[]{:S(2)}) collective-permute-start(bf16[128,640]{1,0:T(8,128)(2,1)S(1)} %gathered_half.1.refs_1_), channel_id=1, source_target_pairs={{0,4},{4,0},{1,5},{5,1},{2,6},{6,2},{3,7},{7,3},{8,12},{12,8},{9,1... | collective-permute-start | bytes 491528 | tf_op jit(solution)/shard_map/ppermute | solution.py:471
  70.5 2.7 %inside.1.refs_8_ = f32[512,768]{1,0:T(8,128)S(1)} custom-call(bf16[512,256]{1,0:T(8,128)(2,1)} %refs_4_.5, bf16[512,256]{1,0:T(8,128)(2,1)} %refs_1_.3, bf16[512,512]{1,0:T(8,128)(2,1)} %refs_2_.3, f32[1,512]{1,0:T(1,128)} %refs_6_.3, bf16[512,128]{1,0:T(8,128)(2,1)} %refs_5_.5, bf16[512,128]{1,0:T(8,128)(2,1)} %refs_5_.4, bf16[512,256]{1,0:T(8,128)(2,1)} %refs_6_.2, ...), custom_call_target="tpu_custom_call" | custom-call | flops 805306368 | bytes 4000000 | tf_op jit(solution)/shard_map/inside/pallas_call | solution.py:70
  73.2 7.7 %heads_out.1 = (bf16[64,2048]{1,0:T(8,128)(2,1)}, bf16[64,2048]{1,0:T(8,128)(2,1)}, bf16[64,2048]{1,0:T(8,128)(2,1)}, bf16[64,2048]{1,0:T(8,128)(2,1)}, bf16[64,...) custom-call(s32[3]{0:T(128)S(1)} %pad_add_fusion.refs_0_, ...), custom_call_target="tpu_custom_call" | custom-call | flops 2147483648 | bytes 8000000 | tf_op jit(solution)/shard_map/heads_out/pallas_call | solution.py:70
  80.9 0.1 collective-permute-start.11
  81.1 2.7 %collective-permute-start.12 = (bf16[64,2048]{1,0:T(8,128)(2,1)}, bf16[64,2048]{1,0:T(8,128)(2,1)S(1)}, u32[]{:S(2)}, u32[]{:S(2)}) collective-permute-start(bf16[64,2048]{1,0:T(8,128)(2,1)} %get-tuple-element.39), channel_id=1, source_target_pairs={{0,3},{1,0},{2,1},{3,2},{4,7},{5,4},{6,5},{7,6},{8,11},{9,8},{10,9... | collective-permute-start | bytes 786440 | tf_op jit(solution)/shard_map/ppermute | solution.py:467
  83.7 0.0 collective-permute-start.14
  83.7 1.4 collective-permute-start.15
  85.2 5.2 %collective-permute-done.11.refs_1_ = bf16[64,2048]{1,0:T(8,128)(2,1)S(1)} collective-permute-done((bf16[64,2048]{1,0:T(8,128)(2,1)}, bf16[64,2048]{1,0:T(8,128)(2,1)S(1)}, u32[]{:S(2)}, u32[]{:S(2)}) %collective-permute-start.11) | collective-permute-done | bytes 262176 | tf_op jit(solution)/shard_map/ppermute | solution.py:467
  90.4 0.0 collective-permute-done.12.refs_3_
  90.4 1.9 %add_two.2 = (bf16[64,2048]{1,0:T(8,128)(2,1)}, bf16[64,2048]{1,0:T(8,128)(2,1)}) custom-call(bf16[64,2048]{1,0:T(8,128)(2,1)} %get-tuple-element.36.refs_0_, bf16[64,2048]{1,0:T(8,128)(2,1)S(1)} %collective-permute-done.11.refs_1_, bf16[64,2048]{1,0:T(8,128)(2,1)} %get-tuple-element.38.refs_2_, bf16[64,2048]{1,0:T(8,128)(2,1)S(1)} %collective-permute-done.12.refs_3_), custom_call_target="tpu_custom_call" | custom-call | tf_op jit(solution)/shard_map/add_two/pallas_call | solution.py:70
  92.3 0.1 collective-permute-start.13
  92.5 2.7 %collective-permute-start.16 = (bf16[64,2048]{1,0:T(8,128)(2,1)}, bf16[64,2048]{1,0:T(8,128)(2,1)S(1)}, u32[]{:S(2)}, u32[]{:S(2)}) collective-permute-start(bf16[64,2048]{1,0:T(8,128)(2,1)} %get-tuple-element.44), channel_id=1, source_target_pairs={{0,3},{1,0},{2,1},{3,2},{4,7},{5,4},{6,5},{7,6},{8,11},{9,8},{10,9... | collective-permute-start | bytes 786440 | tf_op jit(solution)/shard_map/ppermute | solution.py:467
  95.1 0.8 constant_dynamic-slice_fusion.refs_6_
  96.0 0.0 collective-permute-done.15.refs_4_
  96.0 4.5 %collective-permute-done.13.refs_1_ = bf16[64,2048]{1,0:T(8,128)(2,1)S(1)} collective-permute-done((bf16[64,2048]{1,0:T(8,128)(2,1)}, bf16[64,2048]{1,0:T(8,128)(2,1)S(1)}, u32[]{:S(2)}, u32[]{:S(2)}) %collective-permute-start.13) | collective-permute-done | bytes 262176 | tf_op jit(solution)/shard_map/ppermute | solution.py:467
  100.5 2.6 %rows_mid.1 = (bf16[64,2048]{1,0:T(8,128)(2,1)}, bf16[64,2048]{1,0:T(8,128)(2,1)}, bf16[64,2048]{1,0:T(8,128)(2,1)}, bf16[64,2048]{1,0:T(8,128)(2,1)}) custom-call(bf16[64,2048]{1,0:T(8,128)(2,1)} %get-tuple-element.35.refs_0_, bf16[64,2048]{1,0:T(8,128)(2,1)S(1)} %collective-permute-done.13.refs_1_, bf16[64,2048]{1,0:T(8,128)(2,1)S(1)} %collective-permute-done.14.refs_2_, ...), custom_call_target="tpu_custom_call" | custom-call | tf_op jit(solution)/shard_map/rows_mid/pallas_call | solution.py:70
  103.1 0.2 collective-permute-start.19
  103.3 2.6 %collective-permute-start.21 = (bf16[64,2048]{1,0:T(8,128)(2,1)}, bf16[64,2048]{1,0:T(8,128)(2,1)S(1)}, u32[]{:S(2)}, u32[]{:S(2)}) collective-permute-start(bf16[64,2048]{1,0:T(8,128)(2,1)} %get-tuple-element.55.refs_1_), channel_id=1, source_target_pairs={{0,3},{1,0},{2,1},{3,2},{4,7},{5,4},{6,5},{7,6},{8,11},{9,8},{10,9... | collective-permute-start | bytes 786440 | tf_op jit(solution)/shard_map/ppermute | solution.py:467
  105.9 4.7 %collective-permute-done.19.refs_3_ = bf16[64,2048]{1,0:T(8,128)(2,1)S(1)} collective-permute-done((bf16[64,2048]{1,0:T(8,128)(2,1)}, bf16[64,2048]{1,0:T(8,128)(2,1)S(1)}, u32[]{:S(2)}, u32[]{:S(2)}) %collective-permute-start.19) | collective-permute-done | bytes 262176 | tf_op jit(solution)/shard_map/ppermute | solution.py:467
  110.6 2.7 %collective-permute-start.22 = (bf16[64,2048]{1,0:T(8,128)(2,1)S(1)}, bf16[64,2048]{1,0:T(8,128)(2,1)}, u32[]{:S(2)}, u32[]{:S(2)}) collective-permute-start(bf16[64,2048]{1,0:T(8,128)(2,1)S(1)} %collective-permute-done.21.refs_2_), channel_id=1, source_target_pairs={{0,3},{1,0},{2,1},{3,2},{4,7},{5,4},{6,5},{7,6},{8,11},{9,8},{10,9... | collective-permute-start | bytes 786440 | tf_op jit(solution)/shard_map/ppermute | solution.py:467
  113.2 0.1 collective-permute-start.17
  113.4 1.3 collective-permute-start.18
  114.7 2.7 %collective-permute-done.20.refs_0_ = bf16[64,2048]{1,0:T(8,128)(2,1)S(1)} collective-permute-done((bf16[64,2048]{1,0:T(8,128)(2,1)S(1)}, bf16[64,2048]{1,0:T(8,128)(2,1)S(1)}, u32[]{:S(2)}, u32[]{:S(2)}) %collective-permute-start.20) | collective-permute-done | bytes 262176 | tf_op jit(solution)/shard_map/ppermute | solution.py:467
  117.4 18.5 %all-gather.2.cloned.1.call-done.refs_4_ = bf16[2048,4096]{1,0:T(8,128)(2,1)} async-done(((bf16[64,4096]{1,0:T(8,128)(2,1)}), bf16[2048,4096]{1,0:T(8,128)(2,1)}) %all-gather.2.cloned.1.call-update) | async-done | bytes 16777232 | tf_op jit(solution)/shard_map/all_gather | solution.py:519
  135.9 7.6 %first_rows.1 = (bf16[64,2048]{1,0:T(8,128)(2,1)S(1)}, bf16[64,2048]{1,0:T(8,128)(2,1)S(1)}, bf16[64,2048]{1,0:T(8,128)(2,1)S(1)}, bf16[64,2048]{1,0:T(8,128)(2,...) custom-call(bf16[64,2048]{1,0:T(8,128)(2,1)} %copy-done.5, ...), custom_call_target="tpu_custom_call" | custom-call | flops 4294967296 | bytes 16777216 | tf_op jit(solution)/shard_map/first_rows/pallas_call | solution.py:406
  143.5 1.2 collective-permute-start.23
  144.7 1.6 collective-permute-start.24
  146.3 1.3 collective-permute-start.26
  147.6 0.2 collective-permute-start.27
  147.8 4.5 %more_rows.2 = (bf16[64,2048]{1,0:T(8,128)(2,1)S(1)}, bf16[64,2048]{1,0:T(8,128)(2,1)S(1)}) custom-call(bf16[64,2048]{1,0:T(8,128)(2,1)S(1)} %collective-permute-done.17.refs_0_, bf16[64,2048]{1,0:T(8,128)(2,1)S(1)} %collective-permute-done.18.refs_1_, bf16[2048,2048]{1,0:T(8,128)(2,1)S(1)} %get-tuple-element.47.refs_2_, ...), custom_call_target="tpu_custom_call" | custom-call | flops 2147483648 | bytes 16777216 | tf_op jit(solution)/shard_map/more_rows/pallas_call | solution.py:436
  152.3 0.1 collective-permute-done.23.refs_1_
  152.4 0.1 add_two.3
  152.6 1.2 collective-permute-start.25
  153.7 1.6 collective-permute-start.28
  155.4 4.5 %more_rows.3 = (bf16[64,2048]{1,0:T(8,128)(2,1)S(1)}, bf16[64,2048]{1,0:T(8,128)(2,1)S(1)}) custom-call(bf16[64,2048]{1,0:T(8,128)(2,1)S(1)} %copy-done.1, bf16[64,2048]{1,0:T(8,128)(2,1)S(1)} %copy-done.2, bf16[2048,2048]{1,0:T(8,128)(2,1)S(1)} %get-tuple-element.47.refs_2_, bf16[2048,2048]{1,0:T(8,128)(2,1)S(1)} %get-tuple-element.48.refs_3_), custom_call_target="tpu_custom_call" | custom-call | flops 2147483648 | bytes 16777216 | tf_op jit(solution)/shard_map/more_rows/pallas_call | solution.py:436
  159.9 1.2 with_middle.1
  161.1 2.6 %collective-permute-done.25.refs_1_ = bf16[64,2048]{1,0:T(8,128)(2,1)S(1)} collective-permute-done((bf16[64,2048]{1,0:T(8,128)(2,1)S(1)}, bf16[64,2048]{1,0:T(8,128)(2,1)S(1)}, u32[]{:S(2)}, u32[]{:S(2)}) %collective-permute-start.25) | collective-permute-done | bytes 262176 | tf_op jit(solution)/shard_map/ppermute | solution.py:467
  163.7 1.0 last_sum.1
  (29 shorter events, 0.1 us)
Async XLA Ops:
  6.5 88.6 %copy-start = (bf16[512,2048]{1,0:T(8,128)(2,1)S(1)}, bf16[512,2048]{1,0:T(8,128)(2,1)}, u32[]{:S(2)}) copy-start(bf16[512,2048]{1,0:T(8,128)(2,1)} %param.16) | copy-start | bytes 6291460
  6.6 129.3 %all-gather.2.cloned.1.call-start = ((), (), s32[]{:S(2)}) async-start(), calls=%async_computation | async-start | bytes 17301504 | tf_op jit(solution)/shard_map/all_gather | solution.py:519
  10.9 21.9 %collective-permute-start = (bf16[2,128,768]{2,1,0:T(8,128)(2,1)S(1)}, bf16[2,128,768]{2,1,0:T(8,128)(2,1)S(1)}, u32[]{:S(2)}, u32[]{:S(2)}) collective-permute-start(bf16[2,128,768]{2,1,0:T(8,128)(2,1)S(1)} %own_state.1.refs_1_), channel_id=1, source_target_pairs={{0,4},{4,0},{1,5},{5,1},{2,6},{6,2},{3,7},{7,3},{8,12},{12,8},{9,1... | collective-permute-start | bytes 1179656 | tf_op jit(solution)/shard_map/ppermute | solution.py:471
  33.7 4.9 %collective-permute-start.1 = (bf16[32,768]{1,0:T(8,128)(2,1)S(1)}, bf16[32,768]{1,0:T(8,128)(2,1)S(1)}, u32[]{:S(2)}, u32[]{:S(2)}) collective-permute-start(bf16[32,768]{1,0:T(8,128)(2,1)S(1)} %get-tuple-element.67), channel_id=1, source_target_pairs={{0,8},{8,16},{16,24},{24,0},{1,9},{9,17},{17,25},{25,1},{2,10},{10... | collective-permute-start | bytes 147464 | tf_op jit(solution)/shard_map/ppermute | solution.py:467
  33.9 4.8 %collective-permute-start.2 = (bf16[32,768]{1,0:T(8,128)(2,1)S(1)}, bf16[32,768]{1,0:T(8,128)(2,1)S(1)}, u32[]{:S(2)}, u32[]{:S(2)}) collective-permute-start(bf16[32,768]{1,0:T(8,128)(2,1)S(1)} %get-tuple-element.66), channel_id=1, source_target_pairs={{0,16},{8,24},{16,0},{24,8},{1,17},{9,25},{17,1},{25,9},{2,18},{10... | collective-permute-start | bytes 147464 | tf_op jit(solution)/shard_map/ppermute | solution.py:467
  34.0 5.7 %collective-permute-start.3 = (bf16[32,768]{1,0:T(8,128)(2,1)S(1)}, bf16[32,768]{1,0:T(8,128)(2,1)S(1)}, u32[]{:S(2)}, u32[]{:S(2)}) collective-permute-start(bf16[32,768]{1,0:T(8,128)(2,1)S(1)} %get-tuple-element.65), channel_id=1, source_target_pairs={{0,24},{8,0},{16,8},{24,16},{1,25},{9,1},{17,9},{25,17},{2,26},{10... | collective-permute-start | bytes 147464 | tf_op jit(solution)/shard_map/ppermute | solution.py:467
  40.5 7.8 %collective-permute-start.4 = (bf16[1,32,768]{2,1,0:T(8,128)(2,1)S(1)}, bf16[1,32,768]{2,1,0:T(8,128)(2,1)S(1)}, u32[]{:S(2)}, u32[]{:S(2)}) collective-permute-start(bf16[1,32,768]{2,1,0:T(8,128)(2,1)S(1)} %of_group.1), channel_id=1, source_target_pairs={{0,32},{32,64},{64,96},{1,33},{33,65},{65,97},{2,34},{34,66},{66,9... | collective-permute-start | bytes 147464 | tf_op jit(solution)/shard_map/ppermute | solution.py:467
  41.8 10.8 %collective-permute-start.6 = (bf16[1,32,768]{2,1,0:T(8,128)(2,1)S(1)}, bf16[1,32,768]{2,1,0:T(8,128)(2,1)S(1)}, u32[]{:S(2)}, u32[]{:S(2)}) collective-permute-start(bf16[1,32,768]{2,1,0:T(8,128)(2,1)S(1)} %of_group.1), channel_id=1, source_target_pairs={{0,96},{1,97},{2,98},{3,99},{4,100},{5,101},{6,102},{7,103},{8,104... | collective-permute-start | bytes 147464 | tf_op jit(solution)/shard_map/ppermute | solution.py:467
  48.3 6.4 %collective-permute-start.5 = (bf16[1,32,768]{2,1,0:T(8,128)(2,1)S(1)}, bf16[1,32,768]{2,1,0:T(8,128)(2,1)S(1)}, u32[]{:S(2)}, u32[]{:S(2)}) collective-permute-start(bf16[1,32,768]{2,1,0:T(8,128)(2,1)S(1)} %collective-permute-done.4.refs_5_), channel_id=1, source_target_pairs={{0,32},{32,64},{64,96},{1,33},{33,65},{65,97},{2,34},{34,66},{66,9... | collective-permute-start | bytes 147464 | tf_op jit(solution)/shard_map/ppermute | solution.py:467
  55.6 8.4 %collective-permute-start.7 = (bf16[32,640]{1,0:T(8,128)(2,1)S(1)}, bf16[32,640]{1,0:T(8,128)(2,1)S(1)}, u32[]{:S(2)}, u32[]{:S(2)}) collective-permute-start(bf16[32,640]{1,0:T(8,128)(2,1)S(1)} %get-tuple-element.71), channel_id=1, source_target_pairs={{0,8},{8,16},{16,24},{24,0},{1,9},{9,17},{17,25},{25,1},{2,10},{10... | collective-permute-start | bytes 122888 | tf_op jit(solution)/shard_map/ppermute | solution.py:467
  58.0 7.9 %collective-permute-start.8 = (bf16[32,640]{1,0:T(8,128)(2,1)S(1)}, bf16[32,640]{1,0:T(8,128)(2,1)S(1)}, u32[]{:S(2)}, u32[]{:S(2)}) collective-permute-start(bf16[32,640]{1,0:T(8,128)(2,1)S(1)} %get-tuple-element.70), channel_id=1, source_target_pairs={{0,16},{8,24},{16,0},{24,8},{1,17},{9,25},{17,1},{25,9},{2,18},{10... | collective-permute-start | bytes 122888 | tf_op jit(solution)/shard_map/ppermute | solution.py:467
  62.2 5.1 %collective-permute-start.9 = (bf16[32,640]{1,0:T(8,128)(2,1)S(1)}, bf16[32,640]{1,0:T(8,128)(2,1)S(1)}, u32[]{:S(2)}, u32[]{:S(2)}) collective-permute-start(bf16[32,640]{1,0:T(8,128)(2,1)S(1)} %get-tuple-element.69), channel_id=1, source_target_pairs={{0,24},{8,0},{16,8},{24,16},{1,25},{9,1},{17,9},{25,17},{2,26},{10... | collective-permute-start | bytes 122888 | tf_op jit(solution)/shard_map/ppermute | solution.py:467
  68.0 5.3 %collective-permute-start.10 = (bf16[128,640]{1,0:T(8,128)(2,1)S(1)}, bf16[128,640]{1,0:T(8,128)(2,1)S(1)}, u32[]{:S(2)}, u32[]{:S(2)}) collective-permute-start(bf16[128,640]{1,0:T(8,128)(2,1)S(1)} %gathered_half.1.refs_1_), channel_id=1, source_target_pairs={{0,4},{4,0},{1,5},{5,1},{2,6},{6,2},{3,7},{7,3},{8,12},{12,8},{9,1... | collective-permute-start | bytes 491528 | tf_op jit(solution)/shard_map/ppermute | solution.py:471
  80.9 9.5 %collective-permute-start.11 = (bf16[64,2048]{1,0:T(8,128)(2,1)}, bf16[64,2048]{1,0:T(8,128)(2,1)S(1)}, u32[]{:S(2)}, u32[]{:S(2)}) collective-permute-start(bf16[64,2048]{1,0:T(8,128)(2,1)} %get-tuple-element.37), channel_id=1, source_target_pairs={{0,1},{1,2},{2,3},{3,0},{4,5},{5,6},{6,7},{7,4},{8,9},{9,10},{10,1... | collective-permute-start | bytes 786440 | tf_op jit(solution)/shard_map/ppermute | solution.py:467
  81.1 9.3 %collective-permute-start.12 = (bf16[64,2048]{1,0:T(8,128)(2,1)}, bf16[64,2048]{1,0:T(8,128)(2,1)S(1)}, u32[]{:S(2)}, u32[]{:S(2)}) collective-permute-start(bf16[64,2048]{1,0:T(8,128)(2,1)} %get-tuple-element.39), channel_id=1, source_target_pairs={{0,3},{1,0},{2,1},{3,2},{4,7},{5,4},{6,5},{7,6},{8,11},{9,8},{10,9... | collective-permute-start | bytes 786440 | tf_op jit(solution)/shard_map/ppermute | solution.py:467
  83.7 12.2 %collective-permute-start.14 = (bf16[64,2048]{1,0:T(8,128)(2,1)}, bf16[64,2048]{1,0:T(8,128)(2,1)S(1)}, u32[]{:S(2)}, u32[]{:S(2)}) collective-permute-start(bf16[64,2048]{1,0:T(8,128)(2,1)} %get-tuple-element.41), channel_id=1, source_target_pairs={{0,3},{1,0},{2,1},{3,2},{4,7},{5,4},{6,5},{7,6},{8,11},{9,8},{10,9... | collective-permute-start | bytes 786440 | tf_op jit(solution)/shard_map/ppermute | solution.py:467
  83.7 12.3 %collective-permute-start.15 = (bf16[64,2048]{1,0:T(8,128)(2,1)}, bf16[64,2048]{1,0:T(8,128)(2,1)S(1)}, u32[]{:S(2)}, u32[]{:S(2)}) collective-permute-start(bf16[64,2048]{1,0:T(8,128)(2,1)} %get-tuple-element.43), channel_id=1, source_target_pairs={{0,1},{1,2},{2,3},{3,0},{4,5},{5,6},{6,7},{7,4},{8,9},{9,10},{10,1... | collective-permute-start | bytes 786440 | tf_op jit(solution)/shard_map/ppermute | solution.py:467
  92.3 8.2 %collective-permute-start.13 = (bf16[64,2048]{1,0:T(8,128)(2,1)}, bf16[64,2048]{1,0:T(8,128)(2,1)S(1)}, u32[]{:S(2)}, u32[]{:S(2)}) collective-permute-start(bf16[64,2048]{1,0:T(8,128)(2,1)} %get-tuple-element.40), channel_id=1, source_target_pairs={{0,1},{1,2},{2,3},{3,0},{4,5},{5,6},{6,7},{7,4},{8,9},{9,10},{10,1... | collective-permute-start | bytes 786440 | tf_op jit(solution)/shard_map/ppermute | solution.py:467
  92.5 8.1 %collective-permute-start.16 = (bf16[64,2048]{1,0:T(8,128)(2,1)}, bf16[64,2048]{1,0:T(8,128)(2,1)S(1)}, u32[]{:S(2)}, u32[]{:S(2)}) collective-permute-start(bf16[64,2048]{1,0:T(8,128)(2,1)} %get-tuple-element.44), channel_id=1, source_target_pairs={{0,3},{1,0},{2,1},{3,2},{4,7},{5,4},{6,5},{7,6},{8,11},{9,8},{10,9... | collective-permute-start | bytes 786440 | tf_op jit(solution)/shard_map/ppermute | solution.py:467
  103.1 7.5 %collective-permute-start.19 = (bf16[64,2048]{1,0:T(8,128)(2,1)}, bf16[64,2048]{1,0:T(8,128)(2,1)S(1)}, u32[]{:S(2)}, u32[]{:S(2)}) collective-permute-start(bf16[64,2048]{1,0:T(8,128)(2,1)} %get-tuple-element.54.refs_0_), channel_id=1, source_target_pairs={{0,1},{1,2},{2,3},{3,0},{4,5},{5,6},{6,7},{7,4},{8,9},{9,10},{10,1... | collective-permute-start | bytes 786440 | tf_op jit(solution)/shard_map/ppermute | solution.py:467
  103.3 7.3 %collective-permute-start.21 = (bf16[64,2048]{1,0:T(8,128)(2,1)}, bf16[64,2048]{1,0:T(8,128)(2,1)S(1)}, u32[]{:S(2)}, u32[]{:S(2)}) collective-permute-start(bf16[64,2048]{1,0:T(8,128)(2,1)} %get-tuple-element.55.refs_1_), channel_id=1, source_target_pairs={{0,3},{1,0},{2,1},{3,2},{4,7},{5,4},{6,5},{7,6},{8,11},{9,8},{10,9... | collective-permute-start | bytes 786440 | tf_op jit(solution)/shard_map/ppermute | solution.py:467
  110.6 25.3 %copy-start.3 = (bf16[64,2048]{1,0:T(8,128)(2,1)}, bf16[64,2048]{1,0:T(8,128)(2,1)S(1)}, u32[]{:S(2)}) copy-start(bf16[64,2048]{1,0:T(8,128)(2,1)S(1)} %collective-permute-done.19.refs_3_) | copy-start | bytes 786436
  110.6 6.8 %collective-permute-start.20 = (bf16[64,2048]{1,0:T(8,128)(2,1)S(1)}, bf16[64,2048]{1,0:T(8,128)(2,1)S(1)}, u32[]{:S(2)}, u32[]{:S(2)}) collective-permute-start(bf16[64,2048]{1,0:T(8,128)(2,1)S(1)} %collective-permute-done.19.refs_3_), channel_id=1, source_target_pairs={{0,1},{1,2},{2,3},{3,0},{4,5},{5,6},{6,7},{7,4},{8,9},{9,10},{10,1... | collective-permute-start | bytes 786440 | tf_op jit(solution)/shard_map/ppermute | solution.py:467
  110.6 25.3 %copy-start.4 = (bf16[64,2048]{1,0:T(8,128)(2,1)}, bf16[64,2048]{1,0:T(8,128)(2,1)S(1)}, u32[]{:S(2)}) copy-start(bf16[64,2048]{1,0:T(8,128)(2,1)S(1)} %collective-permute-done.21.refs_2_) | copy-start | bytes 786436
  110.6 6.8 %collective-permute-start.22 = (bf16[64,2048]{1,0:T(8,128)(2,1)S(1)}, bf16[64,2048]{1,0:T(8,128)(2,1)}, u32[]{:S(2)}, u32[]{:S(2)}) collective-permute-start(bf16[64,2048]{1,0:T(8,128)(2,1)S(1)} %collective-permute-done.21.refs_2_), channel_id=1, source_target_pairs={{0,3},{1,0},{2,1},{3,2},{4,7},{5,4},{6,5},{7,6},{8,11},{9,8},{10,9... | collective-permute-start | bytes 786440 | tf_op jit(solution)/shard_map/ppermute | solution.py:467
  113.2 34.4 %collective-permute-start.17 = (bf16[64,2048]{1,0:T(8,128)(2,1)}, bf16[64,2048]{1,0:T(8,128)(2,1)S(1)}, u32[]{:S(2)}, u32[]{:S(2)}) collective-permute-start(bf16[64,2048]{1,0:T(8,128)(2,1)} %get-tuple-element.54.refs_0_), channel_id=1, source_target_pairs={{0,3},{1,0},{2,1},{3,2},{4,7},{5,4},{6,5},{7,6},{8,11},{9,8},{10,9... | collective-permute-start | bytes 786440 | tf_op jit(solution)/shard_map/ppermute | solution.py:467
  113.4 34.4 %collective-permute-start.18 = (bf16[64,2048]{1,0:T(8,128)(2,1)}, bf16[64,2048]{1,0:T(8,128)(2,1)S(1)}, u32[]{:S(2)}, u32[]{:S(2)}) collective-permute-start(bf16[64,2048]{1,0:T(8,128)(2,1)} %get-tuple-element.55.refs_1_), channel_id=1, source_target_pairs={{0,1},{1,2},{2,3},{3,0},{4,5},{5,6},{6,7},{7,4},{8,9},{9,10},{10,1... | collective-permute-start | bytes 786440 | tf_op jit(solution)/shard_map/ppermute | solution.py:467
  117.4 18.5 %copy-start.5 = (bf16[64,2048]{1,0:T(8,128)(2,1)}, bf16[64,2048]{1,0:T(8,128)(2,1)S(1)}, u32[]{:S(2)}) copy-start(bf16[64,2048]{1,0:T(8,128)(2,1)S(1)} %collective-permute-done.20.refs_0_) | copy-start | bytes 786436
  143.5 8.9 %collective-permute-start.23 = (bf16[64,2048]{1,0:T(8,128)(2,1)S(1)}, bf16[64,2048]{1,0:T(8,128)(2,1)S(1)}, u32[]{:S(2)}, u32[]{:S(2)}) collective-permute-start(bf16[64,2048]{1,0:T(8,128)(2,1)S(1)} %get-tuple-element.50), channel_id=1, source_target_pairs={{0,1},{1,2},{2,3},{3,0},{4,5},{5,6},{6,7},{7,4},{8,9},{9,10},{10,1... | collective-permute-start | bytes 786440 | tf_op jit(solution)/shard_map/ppermute | solution.py:467
  144.7 7.8 %collective-permute-start.24 = (bf16[64,2048]{1,0:T(8,128)(2,1)S(1)}, bf16[64,2048]{1,0:T(8,128)(2,1)S(1)}, u32[]{:S(2)}, u32[]{:S(2)}) collective-permute-start(bf16[64,2048]{1,0:T(8,128)(2,1)S(1)} %get-tuple-element.52), channel_id=1, source_target_pairs={{0,3},{1,0},{2,1},{3,2},{4,7},{5,4},{6,5},{7,6},{8,11},{9,8},{10,9... | collective-permute-start | bytes 786440 | tf_op jit(solution)/shard_map/ppermute | solution.py:467
  146.3 14.7 %collective-permute-start.26 = (bf16[64,2048]{1,0:T(8,128)(2,1)S(1)}, bf16[64,2048]{1,0:T(8,128)(2,1)S(1)}, u32[]{:S(2)}, u32[]{:S(2)}) collective-permute-start(bf16[64,2048]{1,0:T(8,128)(2,1)S(1)} %get-tuple-element.61), channel_id=1, source_target_pairs={{0,3},{1,0},{2,1},{3,2},{4,7},{5,4},{6,5},{7,6},{8,11},{9,8},{10,9... | collective-permute-start | bytes 786440 | tf_op jit(solution)/shard_map/ppermute | solution.py:467
  147.6 13.4 %collective-permute-start.27 = (bf16[64,2048]{1,0:T(8,128)(2,1)S(1)}, bf16[64,2048]{1,0:T(8,128)(2,1)S(1)}, u32[]{:S(2)}, u32[]{:S(2)}) collective-permute-start(bf16[64,2048]{1,0:T(8,128)(2,1)S(1)} %get-tuple-element.63), channel_id=1, source_target_pairs={{0,1},{1,2},{2,3},{3,0},{4,5},{5,6},{6,7},{7,4},{8,9},{9,10},{10,1... | collective-permute-start | bytes 786440 | tf_op jit(solution)/shard_map/ppermute | solution.py:467
  147.8 7.6 %copy-start.1 = (bf16[64,2048]{1,0:T(8,128)(2,1)S(1)}, bf16[64,2048]{1,0:T(8,128)(2,1)}, u32[]{:S(2)}) copy-start(bf16[64,2048]{1,0:T(8,128)(2,1)} %get-tuple-element.54.refs_0_) | copy-start | bytes 786436
  147.8 7.6 %copy-start.2 = (bf16[64,2048]{1,0:T(8,128)(2,1)S(1)}, bf16[64,2048]{1,0:T(8,128)(2,1)}, u32[]{:S(2)}) copy-start(bf16[64,2048]{1,0:T(8,128)(2,1)} %get-tuple-element.55.refs_1_) | copy-start | bytes 786436
  152.6 11.1 %collective-permute-start.25 = (bf16[64,2048]{1,0:T(8,128)(2,1)S(1)}, bf16[64,2048]{1,0:T(8,128)(2,1)S(1)}, u32[]{:S(2)}, u32[]{:S(2)}) collective-permute-start(bf16[64,2048]{1,0:T(8,128)(2,1)S(1)} %get-tuple-element.53), channel_id=1, source_target_pairs={{0,1},{1,2},{2,3},{3,0},{4,5},{5,6},{6,7},{7,4},{8,9},{9,10},{10,1... | collective-permute-start | bytes 786440 | tf_op jit(solution)/shard_map/ppermute | solution.py:467
  153.7 9.9 %collective-permute-start.28 = (bf16[64,2048]{1,0:T(8,128)(2,1)S(1)}, bf16[64,2048]{1,0:T(8,128)(2,1)S(1)}, u32[]{:S(2)}, u32[]{:S(2)}) collective-permute-start(bf16[64,2048]{1,0:T(8,128)(2,1)S(1)} %get-tuple-element.64), channel_id=1, source_target_pairs={{0,3},{1,0},{2,1},{3,2},{4,7},{5,4},{6,5},{7,6},{8,11},{9,8},{10,9... | collective-permute-start | bytes 786440 | tf_op jit(solution)/shard_map/ppermute | solution.py:467
Sparse Core Ops, SparseCore 0:
  9.2 126.6 all-gather.1
